TPU v7x, 256 devices: a whole 4x4x8 slice. The times are simulated.
256 devices in a mesh: sp: 16 (over y, x), tp: 16 (over z, core).
Axes of the slice: x: 4, y: 4, z: 8, core: 2. Of those that a mesh axis runs over, the one named last changes fastest.
Arguments:
- conv_value: bfloat16 [1024, 16384], P('tp', 'sp'), may hold values from -6 to 6
- conv_gate: bfloat16 [1024, 16384], P('tp', 'sp'), may hold values from -6 to 6
- conv_taps: float32 [1024, 31], P('tp'), may hold values from -2.2 to 2.2
- norm_gain: float32 [1024], replicated, may hold values from 0.1 to 1.9
- norm_bias: float32 [1024], replicated, may hold values from -3 to 3
- out_weight: bfloat16 [1024, 2048], replicated, may hold values from -0.1875 to 0.1875
- stream: bfloat16 [16384, 2048], P(('sp', 'tp')), may hold values from -6 to 6
- routes: int32 [16384, 2], P(('sp', 'tp')), may hold values from 0 to 15, all different within a row; in each aligned block of 64 rows (0 to 63, 64 to 127, ...) at most 8 rows name the same one
- route_weights: float32 [16384, 2], P(('sp', 'tp')), may hold values from 0.2 to 1
- expert_gain: float32 [2048], replicated, may hold values from 0.1 to 1.9
- expert_gate: bfloat16 [16, 2048, 7168], P('sp', None, 'tp'), may hold values from -0.125 to 0.125
- expert_up: bfloat16 [16, 2048, 7168], P('sp', None, 'tp'), may hold values from -0.125 to 0.125
- expert_down: bfloat16 [16, 7168, 2048], P('sp', 'tp'), may hold values from -0.0625 to 0.0625
Outputs:
- mixed: bfloat16 [16384, 2048], P(('sp', 'tp'))
Inputs may be any that keep to these rules, and one draw needn't show every extreme that they name: `routes`: within each device's 64 rows every expert is named exactly 8 times; a row names distinct experts.
All inputs are finite; a program needn't handle non-finite values.
Results may differ from a plain program's by a relative error of at most 0.014.
Values may be sent and summed in bfloat16 or wider, within the bound.
No kernel may reach another device: no remote copies, remote signals or barrier semaphores. Data moves between devices by JAX's collectives and lax.ppermute only.
A program may use at most 64 MiB of HBM per device.

v0:
```python
import jax
import jax.numpy as jnp
from jax import lax
from jax.sharding import PartitionSpec as P

epsilon = 1e-06


def shifted(value, axis, steps):
    count = lax.axis_size(axis)
    initial, last = (max(0, -steps), min(count, count - steps))
    return lax.ppermute(value, axis, [(source, source + steps) for source in range(initial, last)])


def per_device(
    conv_value,
    conv_gate,
    conv_taps,
    norm_gain,
    norm_bias,
    out_weight,
    stream,
    routes,
    route_weights,
    expert_gain,
    expert_gate,
    expert_up,
    expert_down,
):
    f32 = jnp.float32
    local_ch = conv_value.shape[0]
    run_len = conv_value.shape[1]
    kernel_len = conv_taps.shape[1]
    gated_input = (conv_value.astype(f32) * jax.nn.sigmoid(conv_gate.astype(f32))).astype(
        jnp.bfloat16
    )
    left_rim = shifted(gated_input[:, run_len - (kernel_len - 1) :], "sp", 1)
    padded = jnp.concatenate([left_rim, gated_input], axis=1).astype(f32)
    conv_sum = jnp.zeros((local_ch, run_len), f32)
    for offset in range(kernel_len):
        conv_sum = (
            conv_sum + conv_taps[:, offset : offset + 1] * padded[:, offset : offset + run_len]
        )
    conv_out = conv_sum.astype(jnp.bfloat16)
    whole_conv = lax.all_to_all(conv_out, "tp", split_axis=1, concat_axis=0, tiled=True).astype(f32)
    center = jnp.mean(whole_conv, axis=0, keepdims=True)
    spread = jnp.mean((whole_conv - center) ** 2, axis=0, keepdims=True)
    scaled = (whole_conv - center) * lax.rsqrt(spread + epsilon) * norm_gain[:, None] + norm_bias[
        :, None
    ]
    token_major = jax.nn.silu(scaled).astype(jnp.bfloat16)
    projected = lax.dot_general(
        token_major, out_weight, (((0,), (0,)), ((), ())), preferred_element_type=f32
    )
    residual = (stream.astype(f32) + projected).astype(jnp.bfloat16)
    res_float = residual.astype(f32)
    normed = (
        res_float
        * lax.rsqrt(jnp.mean(res_float * res_float, axis=1, keepdims=True) + epsilon)
        * expert_gain
    ).astype(jnp.bfloat16)
    tok_rows = stream.shape[0]
    width = stream.shape[1]
    top_count = routes.shape[1]
    experts = lax.axis_size("sp")
    capacity = top_count * tok_rows // experts
    flat_ids = routes.reshape(-1)
    onehot = (flat_ids[:, None] == jnp.arange(experts, dtype=jnp.int32)[None, :]).astype(jnp.int32)
    before = jnp.cumsum(onehot, axis=0) - onehot
    rank = jnp.sum(before * onehot, axis=1)
    slots = flat_ids * capacity + rank
    chooser = jnp.any(
        slots.reshape(tok_rows, top_count)[None, :, :]
        == jnp.arange(experts * capacity, dtype=jnp.int32)[:, None, None],
        axis=2,
    ).astype(jnp.bfloat16)
    send_rows = (
        jnp.dot(chooser, normed, preferred_element_type=f32)
        .astype(jnp.bfloat16)
        .reshape(experts, capacity, width)
    )
    gate_w = expert_gate[0]
    up_w = expert_up[0]
    down_w = expert_down[0]
    received = lax.all_to_all(send_rows, "sp", split_axis=0, concat_axis=0, tiled=True)
    flat_recv = received.reshape(-1, width)
    piece = lax.all_gather(flat_recv, "tp", axis=0, tiled=True)
    gate_val = jnp.dot(piece, gate_w, preferred_element_type=f32)
    up_val = jnp.dot(piece, up_w, preferred_element_type=f32)
    hidden = (jax.nn.silu(gate_val) * up_val).astype(jnp.bfloat16)
    summed = lax.psum_scatter(
        jnp.dot(hidden, down_w, preferred_element_type=f32).astype(jnp.bfloat16),
        "tp",
        scatter_dimension=0,
        tiled=True,
    )
    result = summed.reshape(received.shape)
    returned = lax.all_to_all(result, "sp", split_axis=0, concat_axis=0, tiled=True)
    picked = returned.reshape(experts * capacity, width)[slots].reshape(tok_rows, top_count, width)
    expert_sum = jnp.sum(picked.astype(f32) * route_weights[:, :, None], axis=1)
    return (res_float + expert_sum).astype(jnp.bfloat16)


def solution(mesh):
    return jax.shard_map(
        per_device,
        mesh=mesh,
        in_specs=(
            P("tp", "sp"),
            P("tp", "sp"),
            P("tp", None),
            P(),
            P(),
            P(),
            P(("sp", "tp"), None),
            P(("sp", "tp"), None),
            P(("sp", "tp"), None),
            P(),
            P("sp", None, "tp"),
            P("sp", None, "tp"),
            P("sp", "tp", None),
        ),
        out_specs=P(("sp", "tp"), None),
        check_vma=False,
    )
```

profile of v0, /device:TPU:2, one launch (start us, length us, event | category | flops | bytes accessed | tf_op | source)
XLA Modules:
  0.0 225.3 jit_solution(4182957621673231946)
XLA Ops:
  6.5 1.2 multiply_convert_fusion.4
  7.7 0.1 slice.254
  7.8 3.4 %collective-permute-start = (bf16[64,30]{1,0:T(8,128)(2,1)S(1)}, bf16[64,30]{1,0:T(8,128)(2,1)S(1)}, u32[]{:S(2)}, u32[]{:S(2)}) collective-permute-start(bf16[64,30]{1,0:T(8,128)(2,1)S(1)} %slice.254), channel_id=1, source_target_pairs={{0,16},{16,32},{32,48},{48,64},{64,80},{80,96},{96,112},{112,128},... | collective-permute-start | bytes 11528 | tf_op jit(solution)/shard_map/ppermute | solution.py:12
  11.2 1.0 slice_bitcast_fusion.30
  12.2 1.0 slice_bitcast_fusion.29
  13.2 0.8 copy.28
  14.0 0.1 eq.28
  14.1 0.1 fusion.47
  14.2 0.2 reduce_window_sum.11
  14.4 0.2 select_reduce_fusion
  14.6 0.1 reduce_sum.52
  14.7 0.0 collective-permute-done
  14.7 0.1 maximum_convert_fusion
  14.8 2.7 %fusion.10 = bf16[64,1024]{1,0:T(8,128)(2,1)S(1)} fusion(f32[64,1054]{1,0:T(8,128)S(1)} %maximum_convert_fusion, f32[64]{0:T(128)S(1)} %get-tuple-element.36, f32[64]{0:T(128)S(1)} %get-tuple-element.37, f32[64]{0:T(128)S(1)} %get-tuple-element.8, f32[64]{0:T(128)S(1)} %get-tuple-element.9, f32[64]{0:T(128)S(1)} %get-tuple-element.10, ...), kind=kLoop, calls=%fused_computation.23 | loop fusion | flops 4063232 | bytes 8265472 | tf_op jit(solution)/shard_map/convert_element_type | solution.py:44
  17.5 0.0 copy-start.1
  17.5 0.0 copy-start.3
  17.5 0.0 copy-start.4
  17.5 0.2 copy.26
  17.7 0.9 reshape.99
  18.6 8.6 %all-to-all-start = ((bf16[16,2,2048]{2,1,0:T(2,128)(2,1)}), bf16[16,2,2048]{2,1,0:T(2,128)(2,1)S(1)}, u32[]{:S(2)}, u32[]{:S(2)}) async-start(bf16[16,2,2048]{2,1,0:T(2,128)(2,1)} %reshape.99), calls=%async_computation | async-start | bytes 262144 | tf_op jit(solution)/shard_map/all_to_all | solution.py:45
  27.2 0.0 all-gather.2.cloned.1.call-start
  27.3 0.1 copy.30
  27.3 0.1 fusion.48
  27.4 8.4 %all-to-all-done = bf16[16,2,2048]{2,1,0:T(2,128)(2,1)S(1)} async-done(((bf16[16,2,2048]{2,1,0:T(2,128)(2,1)}), bf16[16,2,2048]{2,1,0:T(2,128)(2,1)S(1)}, u32[]{:S(2)}, u32[]{:S(2)}) %all-to-all-start) | async-done | bytes 131104 | tf_op jit(solution)/shard_map/all_to_all | solution.py:45
  35.8 0.2 reshape.100
  36.1 0.2 convert_reduce_fusion
  36.3 0.3 copy.27
  36.6 0.2 reshape.89
  36.8 0.3 fusion.8
  37.1 3.3 %multiply_reduce_fusion.1 = (f32[64]{0:T(128)S(1)}, f32[64,2048]{1,0:T(8,128)S(1)}) fusion(bf16[1024,2048]{1,0:T(8,128)(2,1)} %param.18, f32[1024,64]{0,1:T(8,128)S(1)} %reshape.89, f32[1024]{0:T(1024)S(1)} %copy-done.3, f32[1024]{0:T(1024)S(1)} %copy-done.4, f32[64]{0:T(128)S(1)} %add_rsqrt_fusion.1, f32[64]{0:T(128)S(1)} %broadcast_multiply_fusion.1, ...), kind=kOutput, calls=%fused_computation.20 | convolution fusion | flops 269811648 | bytes 5251840 | tf_op jit(solution)/shard_map/dot_general | solution.py:52
  40.4 0.4 fusion
  40.7 18.1 %all_to_all.23 = bf16[16,8,2048]{2,1,0:T(8,128)(2,1)} all-to-all(bf16[16,8,2048]{2,1,0:T(8,128)(2,1)S(1)} %fusion), channel_id=1, replica_groups=mesh['sp'=16,'tp'=16] {'sp'}, dimensions={0} | all-to-all | bytes 1048576 | tf_op jit(solution)/shard_map/all_to_all | solution.py:85
  58.8 0.0 all-gather.2.cloned.1.call-update
  58.8 0.2 reduce-scatter.2.cloned.1.call-start
  59.1 49.8 %all-gather.2.cloned.1.call-done = bf16[2048,2048]{1,0:T(8,128)(2,1)} async-done(((bf16[128,2048]{1,0:T(8,128)(2,1)}), bf16[2048,2048]{1,0:T(8,128)(2,1)}) %all-gather.2.cloned.1.call-update) | async-done | bytes 8388624 | tf_op jit(solution)/shard_map/all_gather | solution.py:87
  108.8 7.2 %fusion.5 = f32[2048,448]{0,1:T(8,128)S(1)} fusion(bf16[2048,2048]{1,0:T(8,128)(2,1)} %all-gather.2.cloned.1.call-done, bf16[1,2048,448]{1,2,0:T(8,128)(2,1)} %param.23), kind=kOutput, calls=%fused_computation.10 | convolution fusion | flops 3758096384 | bytes 13893632 | tf_op jit(solution)/shard_map/dot_general | solution.py:88
  116.0 4.3 %multiply_convert_fusion = bf16[2048,448]{0,1:T(8,128)(2,1)S(1)} fusion(f32[2048,448]{0,1:T(8,128)S(1)} %fusion.5, bf16[2048,2048]{1,0:T(8,128)(2,1)S(1)} %copy-done.6, bf16[1,2048,448]{1,2,0:T(8,128)(2,1)S(1)} %copy-done.7), kind=kOutput, calls=%fused_computation.2 | convolution fusion | flops 3763601408 | bytes 15728640 | tf_op jit(solution)/shard_map/dot_general | solution.py:89
  120.3 6.9 %convolution_convert_fusion = bf16[2048,2048]{1,0:T(8,128)(2,1)} fusion(bf16[2048,448]{0,1:T(8,128)(2,1)S(1)} %multiply_convert_fusion, bf16[1,448,2048]{2,1,0:T(8,128)(2,1)S(1)} %copy-done), kind=kOutput, calls=%fused_computation.1 | convolution fusion | flops 3762290688 | bytes 12058624 | tf_op jit(solution)/shard_map/dot_general | solution.py:92
  127.2 0.0 reduce-scatter.2.cloned.1.call-update
  127.2 69.5 %reduce-scatter.2.cloned.1.call-done = bf16[128,2048]{1,0:T(8,128)(2,1)} async-done(((bf16[2048,2048]{1,0:T(8,128)(2,1)}), bf16[128,2048]{1,0:T(8,128)(2,1)}) %reduce-scatter.2.cloned.1.call-update) | async-done | bytes 524304 | tf_op jit(solution)/shard_map/reduce_scatter | solution.py:91
  196.8 7.1 %all-to-all-start.2 = ((bf16[16,8,2048]{2,1,0:T(8,128)(2,1)}), bf16[16,8,2048]{2,1,0:T(8,128)(2,1)S(1)}, u32[]{:S(2)}, u32[]{:S(2)}) async-start(bf16[16,8,2048]{2,1,0:T(8,128)(2,1)} %bitcast.100), calls=%async_computation.3 | async-start | bytes 1048576 | tf_op jit(solution)/shard_map/all_to_all | solution.py:98
  203.9 0.1 mul.497
  204.0 0.1 copy.31
  204.2 8.5 %all-to-all-done.2 = bf16[16,8,2048]{2,1,0:T(8,128)(2,1)S(1)} async-done(((bf16[16,8,2048]{2,1,0:T(8,128)(2,1)}), bf16[16,8,2048]{2,1,0:T(8,128)(2,1)S(1)}, u32[]{:S(2)}, u32[]{:S(2)}) %all-to-all-start.2) | async-done | bytes 524320 | tf_op jit(solution)/shard_map/all_to_all | solution.py:98
  212.7 1.7 gather_fusion
  214.4 1.7 reshape.90
  216.1 1.6 multiply_reduce_fusion
  217.7 0.8 add_convert_fusion
  (20 shorter events, 0.1 us)
Async XLA Ops:
  6.5 113.8 %copy-start = (bf16[1,448,2048]{2,1,0:T(8,128)(2,1)S(1)}, bf16[1,448,2048]{2,1,0:T(8,128)(2,1)}, u32[]{:S(2)}) copy-start(bf16[1,448,2048]{2,1,0:T(8,128)(2,1)} %param.25) | copy-start | bytes 5505028
  7.8 6.9 %collective-permute-start = (bf16[64,30]{1,0:T(8,128)(2,1)S(1)}, bf16[64,30]{1,0:T(8,128)(2,1)S(1)}, u32[]{:S(2)}, u32[]{:S(2)}) collective-permute-start(bf16[64,30]{1,0:T(8,128)(2,1)S(1)} %slice.254), channel_id=1, source_target_pairs={{0,16},{16,32},{32,48},{48,64},{64,80},{80,96},{96,112},{112,128},... | collective-permute-start | bytes 11528 | tf_op jit(solution)/shard_map/ppermute | solution.py:12
  17.5 19.5 %copy-start.1 = (bf16[64,2048]{1,0:T(8,128)(2,1)S(1)}, bf16[64,2048]{1,0:T(8,128)(2,1)}, u32[]{:S(2)}) copy-start(bf16[64,2048]{1,0:T(8,128)(2,1)} %param.19) | copy-start | bytes 786436
  17.5 19.5 %copy-start.3 = (f32[1024]{0:T(1024)S(1)}, f32[1024]{0:T(1024)}, u32[]{:S(2)}) copy-start(f32[1024]{0:T(1024)} %param.17) | copy-start | bytes 12292
  17.5 19.5 %copy-start.4 = (f32[1024]{0:T(1024)S(1)}, f32[1024]{0:T(1024)}, u32[]{:S(2)}) copy-start(f32[1024]{0:T(1024)} %param.16) | copy-start | bytes 12292
  18.6 17.2 %all-to-all-start = ((bf16[16,2,2048]{2,1,0:T(2,128)(2,1)}), bf16[16,2,2048]{2,1,0:T(2,128)(2,1)S(1)}, u32[]{:S(2)}, u32[]{:S(2)}) async-start(bf16[16,2,2048]{2,1,0:T(2,128)(2,1)} %reshape.99), calls=%async_computation | async-start | bytes 262144 | tf_op jit(solution)/shard_map/all_to_all | solution.py:45
  27.2 81.6 %all-gather.2.cloned.1.call-start = ((), (), s32[]{:S(2)}) async-start(), calls=%async_computation.4 | async-start | bytes 8912896 | tf_op jit(solution)/shard_map/all_gather | solution.py:87
  36.3 4.1 %copy-start.2 = (f32[2048]{0:T(1024)S(1)}, f32[2048]{0:T(1024)}, u32[]{:S(2)}) copy-start(f32[2048]{0:T(1024)} %param.22) | copy-start | bytes 24580
  58.8 138.0 %reduce-scatter.2.cloned.1.call-start = ((), (), s32[]{:S(2)}) async-start(), calls=%async_computation.5 | async-start | bytes 8912896 | tf_op jit(solution)/shard_map/reduce_scatter | solution.py:91
  108.8 7.2 %copy-start.6 = (bf16[2048,2048]{1,0:T(8,128)(2,1)S(1)}, bf16[2048,2048]{1,0:T(8,128)(2,1)}, u32[]{:S(2)}) copy-start(bf16[2048,2048]{1,0:T(8,128)(2,1)} %all-gather.2.cloned.1.call-done) | copy-start | bytes 25165828
  108.8 7.2 %copy-start.7 = (bf16[1,2048,448]{1,2,0:T(8,128)(2,1)S(1)}, bf16[1,2048,448]{1,2,0:T(8,128)(2,1)}, u32[]{:S(2)}) copy-start(bf16[1,2048,448]{1,2,0:T(8,128)(2,1)} %param.24) | copy-start | bytes 5505028
  127.2 76.8 %copy-start.5 = (f32[64,2]{0,1:T(2,128)S(1)}, f32[64,2]{0,1:T(2,128)}, u32[]{:S(2)}) copy-start(f32[64,2]{0,1:T(2,128)} %param.21) | copy-start | bytes 1540
  196.8 15.9 %all-to-all-start.2 = ((bf16[16,8,2048]{2,1,0:T(8,128)(2,1)}), bf16[16,8,2048]{2,1,0:T(8,128)(2,1)S(1)}, u32[]{:S(2)}, u32[]{:S(2)}) async-start(bf16[16,8,2048]{2,1,0:T(8,128)(2,1)} %bitcast.100), calls=%async_computation.3 | async-start | bytes 1048576 | tf_op jit(solution)/shard_map/all_to_all | solution.py:98
Sparse Core Ops, SparseCore 0:
  59.0 49.8 all-gather.1
  127.4 69.3 reduce-scatter.1
where the time goes:
time: 226 us; the launch traced here: 225 us
  waiting for transfers between devices  136 us (60%)
  matrix products  22 us (10%)
  starting transfers between devices  19.3 us (9%)
  blocking collectives  18.1 us (8%)
  between operations  13.7 us (6%)
  local copies, waits for them, and re-layouts  8.64 us (4%)
  other arithmetic  7.29 us (3%)
    reduce_scatter x1, waiting for transfers between devices, per_device(): lax.psum_scatter(jnp.dot(hidden, down_w, preferred_element_type=f32).asty...  69.5 us
    all_gather x1, waiting for transfers between devices, per_device(): piece = lax.all_gather(flat_recv, 'tp', axis=0, tiled=True)  49.8 us
    all_to_all x1, blocking collectives, per_device(): lax.all_to_all(send_rows, 'sp', split_axis=0, concat_axis=0, tiled=True)  18.1 us
    all_to_all x1, starting transfers between devices, per_device(): lax.all_to_all(conv_out, 'tp', split_axis=1, concat_axis=0, tiled=True)  8.57 us
    all_to_all x1, waiting for transfers between devices, per_device(): lax.all_to_all(result, 'sp', split_axis=0, concat_axis=0, tiled=True)  8.52 us
    all_to_all x1, waiting for transfers between devices, per_device(): lax.all_to_all(conv_out, 'tp', split_axis=1, concat_axis=0, tiled=True)  8.41 us
    dot_general x1, matrix products, per_device(): gate_val = jnp.dot(piece, gate_w, preferred_element_type=f32)  7.17 us
    all_to_all x1, starting transfers between devices, per_device(): lax.all_to_all(result, 'sp', split_axis=0, concat_axis=0, tiled=True)  7.1 us
  transfers between devices with their start and end apart: 5, of which 4 were waited for; matrix products, arithmetic and copies ran while one was open for 2% of the time, Pallas kernels for 0%

commit v1 on v0

v1 whole, which is shorter than its diff:
```python
import functools
import jax
import jax.numpy as jnp
from jax import lax
from jax.experimental import pallas as pl
from jax.experimental.pallas import tpu as pltpu
from jax.sharding import PartitionSpec as P

epsilon = 1e-06
f32 = jnp.float32
bf16 = jnp.bfloat16
VMEM_LIMIT = 32 << 20


def shifted(value, axis, steps):
    count = lax.axis_size(axis)
    initial, last = (max(0, -steps), min(count, count - steps))
    return lax.ppermute(value, axis, [(source, source + steps) for source in range(initial, last)])


def z_shift(value, steps):
    count = lax.axis_size("tp")
    return lax.ppermute(value, "tp", [(i, (i + 2 * steps) % count) for i in range(count)])


def other_core(value):
    count = lax.axis_size("tp")
    return lax.ppermute(value, "tp", [(i, i ^ 1) for i in range(count)])


def contract_last(a, b):
    return lax.dot_general(a, b, (((1,), (1,)), ((), ())), preferred_element_type=f32)


def expert_kernel(sizes, with_token, *refs):
    count = len(sizes)
    pieces = refs[:count]
    gate_a, gate_b, up_a, up_b, down_a, down_b = refs[count : count + 6]
    at = count + 6 + with_token
    outs = refs[at : at + count]
    rows, total = refs[at + count :]
    step = pl.program_id(0)
    starts = [sum(sizes[:i]) for i in range(count)]

    @pl.when(step == 0)
    def _():
        for start, size, piece in zip(starts, sizes, pieces):
            rows[start : start + size, :] = piece[...]

    x = rows[...]
    gate_val = contract_last(x, jnp.concatenate([gate_a[...], gate_b[...]], axis=0))
    up_val = contract_last(x, jnp.concatenate([up_a[...], up_b[...]], axis=0))
    hidden = (jax.nn.silu(gate_val) * up_val).astype(bf16)
    down = jnp.concatenate([down_a[...], down_b[...]], axis=0)
    partial = jnp.dot(hidden, down, preferred_element_type=f32)

    @pl.when(step == 0)
    def _():
        total[...] = partial

    @pl.when(step > 0)
    def _():
        total[...] += partial

    @pl.when(step == pl.num_programs(0) - 1)
    def _():
        for start, size, out in zip(starts, sizes, outs):
            out[...] = total[start : start + size, :].astype(bf16)


def expert(pieces, weights, token=None, block=112):
    sizes = tuple(p.shape[0] for p in pieces)
    width = pieces[0].shape[1]
    hidden = weights[0].shape[0]
    whole = lambda size: pl.BlockSpec((size, width), lambda j: (0, 0))
    tokens = () if token is None else (token,)
    flops = 2 * 3 * sum(sizes) * width * 2 * hidden
    return pl.pallas_call(
        functools.partial(expert_kernel, sizes, len(tokens)),
        grid=(hidden // block,),
        in_specs=[whole(size) for size in sizes]
        + [pl.BlockSpec((block, width), lambda j: (j, 0))] * 6
        + [pl.BlockSpec(memory_space=pl.ANY)] * len(tokens),
        out_specs=[whole(size) for size in sizes],
        out_shape=[jax.ShapeDtypeStruct((size, width), bf16) for size in sizes],
        scratch_shapes=[
            pltpu.VMEM((sum(sizes), width), bf16),
            pltpu.VMEM((sum(sizes), width), f32),
        ],
        compiler_params=pltpu.CompilerParams(vmem_limit_bytes=VMEM_LIMIT),
        cost_estimate=pl.CostEstimate(
            flops=flops, bytes_accessed=6 * hidden * width * 2, transcendentals=0
        ),
    )(*pieces, *weights, *tokens)


def add_kernel(a, b, out):
    out[...] = (a[...].astype(f32) + b[...].astype(f32)).astype(bf16)


def add(a, b):
    return pl.pallas_call(
        add_kernel,
        out_shape=jax.ShapeDtypeStruct(a.shape, bf16),
        compiler_params=pltpu.CompilerParams(vmem_limit_bytes=8 << 20),
        cost_estimate=pl.CostEstimate(
            flops=a.size * 500, bytes_accessed=a.size * 6, transcendentals=0
        ),
    )(a, b)


def close_kernel(right_a, left_a, own_a, right_b, left_b, own_b, out):
    half = right_a.shape[0]
    out[:half, :] = (
        right_a[...].astype(f32) + left_a[...].astype(f32) + own_a[...].astype(f32)
    ).astype(bf16)
    out[half:, :] = (
        right_b[...].astype(f32) + left_b[...].astype(f32) + own_b[...].astype(f32)
    ).astype(bf16)


def close(*parts):
    half, width = parts[0].shape
    return pl.pallas_call(
        close_kernel,
        out_shape=jax.ShapeDtypeStruct((2 * half, width), bf16),
        compiler_params=pltpu.CompilerParams(vmem_limit_bytes=8 << 20),
    )(*parts)


def per_device(
    conv_value,
    conv_gate,
    conv_taps,
    norm_gain,
    norm_bias,
    out_weight,
    stream,
    routes,
    route_weights,
    expert_gain,
    expert_gate,
    expert_up,
    expert_down,
):
    local_ch = conv_value.shape[0]
    run_len = conv_value.shape[1]
    kernel_len = conv_taps.shape[1]
    gate_t = expert_gate[0].T
    up_t = expert_up[0].T
    down_w = expert_down[0]
    weights = (
        gate_t,
        other_core(gate_t),
        up_t,
        other_core(up_t),
        down_w,
        other_core(down_w),
    )

    gated_input = (conv_value.astype(f32) * jax.nn.sigmoid(conv_gate.astype(f32))).astype(bf16)
    left_rim = shifted(gated_input[:, run_len - (kernel_len - 1) :], "sp", 1)
    padded = jnp.concatenate([left_rim, gated_input], axis=1).astype(f32)
    conv_sum = jnp.zeros((local_ch, run_len), f32)
    for offset in range(kernel_len):
        conv_sum = (
            conv_sum + conv_taps[:, offset : offset + 1] * padded[:, offset : offset + run_len]
        )
    conv_out = conv_sum.astype(bf16)
    whole_conv = lax.all_to_all(conv_out, "tp", split_axis=1, concat_axis=0, tiled=True).astype(f32)
    center = jnp.mean(whole_conv, axis=0, keepdims=True)
    spread = jnp.mean((whole_conv - center) ** 2, axis=0, keepdims=True)
    scaled = (whole_conv - center) * lax.rsqrt(spread + epsilon) * norm_gain[:, None] + norm_bias[
        :, None
    ]
    token_major = jax.nn.silu(scaled).astype(bf16)
    projected = lax.dot_general(
        token_major, out_weight, (((0,), (0,)), ((), ())), preferred_element_type=f32
    )
    residual = (stream.astype(f32) + projected).astype(bf16)
    res_float = residual.astype(f32)
    normed = (
        res_float
        * lax.rsqrt(jnp.mean(res_float * res_float, axis=1, keepdims=True) + epsilon)
        * expert_gain
    ).astype(bf16)
    tok_rows = stream.shape[0]
    width = stream.shape[1]
    top_count = routes.shape[1]
    experts = lax.axis_size("sp")
    capacity = top_count * tok_rows // experts
    flat_ids = routes.reshape(-1)
    onehot = (flat_ids[:, None] == jnp.arange(experts, dtype=jnp.int32)[None, :]).astype(jnp.int32)
    before = jnp.cumsum(onehot, axis=0) - onehot
    rank = jnp.sum(before * onehot, axis=1)
    slots = (flat_ids * capacity + rank).reshape(tok_rows, top_count)
    slot_ids = jnp.arange(experts * capacity, dtype=jnp.int32)
    chooser = jnp.any(slots[None, :, :] == slot_ids[:, None, None], axis=2).astype(bf16)
    send_rows = (
        jnp.dot(chooser, normed, preferred_element_type=f32)
        .astype(bf16)
        .reshape(experts, capacity, width)
    )
    received = lax.all_to_all(send_rows, "sp", split_axis=0, concat_axis=0, tiled=True)
    received, weights = lax.optimization_barrier((received, weights))
    own = received.reshape(-1, width)

    far = lax.axis_size("tp") // 4
    half = own.shape[0] // 2
    from_left = {0: (own[:half], own[half:])}
    from_right = {0: from_left[0]}
    for k in range(1, far + 1):
        left_a, left_b = from_left[k - 1]
        right_a, right_b = from_right[k - 1]
        from_left[k] = (z_shift(left_a, 1), z_shift(left_b, 1) if k < far else None)
        from_right[k] = (z_shift(right_a, -1) if k < far else None, z_shift(right_b, -1))

    first = expert((*from_left[0], *from_left[1], *from_right[1]), weights)
    part_own = first[0:2]
    part_left, part_right = {1: first[2:4]}, {1: first[4:6]}
    token = first[0]
    for k in range(2, far):
        parts = expert((*from_left[k], *from_right[k]), weights, token)
        part_left[k], part_right[k] = parts[0:2], parts[2:4]
        token = parts[0]
    antipode = expert((from_left[far][0], from_right[far][1]), weights, token)

    right_a, left_b = z_shift(antipode[0], 1), z_shift(antipode[1], -1)
    right_b, left_a = None, None
    for k in range(far - 1, 0, -1):
        out_rb = part_right[k][1] if right_b is None else add(right_b, part_right[k][1])
        out_la = part_left[k][0] if left_a is None else add(left_a, part_left[k][0])
        right_b, left_a = z_shift(out_rb, 1), z_shift(out_la, -1)
        right_a = z_shift(add(right_a, part_right[k][0]), 1)
        left_b = z_shift(add(left_b, part_left[k][1]), -1)
    result = close(right_a, left_a, part_own[0], right_b, left_b, part_own[1])
    result = result.reshape(received.shape)
    returned = lax.all_to_all(result, "sp", split_axis=0, concat_axis=0, tiled=True)
    weight_hi = route_weights.astype(bf16).astype(f32)
    weight_lo = route_weights - weight_hi

    def spread_weights(weight):
        hit = slots[:, :, None] == slot_ids[None, None, :]
        return jnp.sum(jnp.where(hit, weight[:, :, None], 0.0), axis=1).astype(bf16)

    rows = returned.reshape(experts * capacity, width)
    expert_sum = jnp.dot(
        spread_weights(weight_hi), rows, preferred_element_type=f32
    ) + jnp.dot(spread_weights(weight_lo), rows, preferred_element_type=f32)
    return (res_float + expert_sum).astype(bf16)


def solution(mesh):
    return jax.shard_map(
        per_device,
        mesh=mesh,
        in_specs=(
            P("tp", "sp"),
            P("tp", "sp"),
            P("tp", None),
            P(),
            P(),
            P(),
            P(("sp", "tp"), None),
            P(("sp", "tp"), None),
            P(("sp", "tp"), None),
            P(),
            P("sp", None, "tp"),
            P("sp", None, "tp"),
            P("sp", "tp", None),
        ),
        out_specs=P(("sp", "tp"), None),
        check_vma=False,
    )
```

time: 226 us -> 169 us (0.75)
  waiting for transfers between devices: 136 us -> 46.3 us
  starting transfers between devices: 19.3 us -> 59.8 us
  Pallas kernels: 0 us -> 28.9 us
  matrix products: 22 us -> 4.93 us
  between operations: 13.7 us -> 0.46 us
  local copies, waits for them, and re-layouts: 8.64 us -> 5.05 us
  other arithmetic: 7.29 us -> 4.94 us
    reduce_scatter x1 -> x0, waiting for transfers between devices: 69.5 us -> none  [per_device(): lax.psum_scatter(jnp.dot(hidden, down_w, preferred_element_type=f32).asty...]
    all_gather x1 -> x0, waiting for transfers between devices: 49.8 us -> none  [per_device(): piece = lax.all_gather(flat_recv, 'tp', axis=0, tiled=True)]
    ppermute x0 -> x31, starting transfers between devices: none -> 43 us  [the longest x28 42.3 us: z_shift(): lax.ppermute(value, 'tp', [(i, (i + 2 * steps) % count) for i in range(co...]
    ppermute x0 -> x31, waiting for transfers between devices: none -> 29.1 us  [the longest x28 29.1 us: z_shift(): lax.ppermute(value, 'tp', [(i, (i + 2 * steps) % count) for i in range(co...]
    pallas_call x0 -> x15, Pallas kernels: none -> 28.9 us  [the longest x4 27.3 us: expert(): pl.pallas_call(functools.partial(expert_kernel, sizes, len(tokens)), grid...]
    dot_general x4 -> x3, matrix products: 18.7 us -> 1.51 us  [the longest x1 0.93 us: per_device(): jnp.dot(spread_weights(weight_hi), rows, preferred_element_type=f32)]
    all_to_all x1, starting transfers between devices: 7.1 us -> 4.82 us  [per_device(): lax.all_to_all(result, 'sp', split_axis=0, concat_axis=0, tiled=True)]
    convert_element_type x3 -> x2, other arithmetic: 4.6 us -> 3.7 us  [the longest x1 2.66 us: per_device(): conv_out = conv_sum.astype(bf16)]
  transfers between devices with their start and end apart: 5 -> 34, of which waited for: 4 -> 12; matrix products, arithmetic and copies ran while one was open for 2% -> 7% of each run, Pallas kernels for 0% -> 13%
where the time goes in v1:
time: 169 us; the launch traced here: 168 us
  starting transfers between devices  59.8 us (35%)
  waiting for transfers between devices  46.3 us (27%)
  Pallas kernels  28.9 us (17%)
  blocking collectives  18.1 us (11%)
  local copies, waits for them, and re-layouts  5.05 us (3%)
  other arithmetic  4.94 us (3%)
  matrix products  4.93 us (3%)
    ppermute x28, starting transfers between devices, z_shift(): lax.ppermute(value, 'tp', [(i, (i + 2 * steps) % count) for i in range(co...  42.3 us
    ppermute x28, waiting for transfers between devices, z_shift(): lax.ppermute(value, 'tp', [(i, (i + 2 * steps) % count) for i in range(co...  29.1 us
    pallas_call x4, Pallas kernels, expert(): pl.pallas_call(functools.partial(expert_kernel, sizes, len(tokens)), grid...  27.3 us
    all_to_all x1, blocking collectives, per_device(): lax.all_to_all(send_rows, 'sp', split_axis=0, concat_axis=0, tiled=True)  18.1 us
    all_to_all x1, waiting for transfers between devices, per_device(): lax.all_to_all(result, 'sp', split_axis=0, concat_axis=0, tiled=True)  8.72 us
    all_to_all x1, starting transfers between devices, per_device(): lax.all_to_all(conv_out, 'tp', split_axis=1, concat_axis=0, tiled=True)  8.58 us
    all_to_all x1, waiting for transfers between devices, per_device(): lax.all_to_all(conv_out, 'tp', split_axis=1, concat_axis=0, tiled=True)  8.5 us
    all_to_all x1, starting transfers between devices, per_device(): lax.all_to_all(result, 'sp', split_axis=0, concat_axis=0, tiled=True)  4.82 us
  transfers between devices with their start and end apart: 34, of which 12 were waited for; matrix products, arithmetic and copies ran while one was open for 7% of the time, Pallas kernels for 13%

profile of v1, /device:TPU:2, one launch (start us, length us, event | category | flops | bytes accessed | tf_op | source)
XLA Modules:
  0.0 168.5 jit_solution(12041669707887822151)
XLA Ops:
  0.0 1.0 multiply_convert_fusion.3
  1.1 3.4 %collective-permute-start = (bf16[64,30]{1,0:T(8,128)(2,1)S(1)}, bf16[64,30]{1,0:T(8,128)(2,1)S(1)}, u32[]{:S(2)}, u32[]{:S(2)}) collective-permute-start(bf16[64,30]{1,0:T(8,128)(2,1)S(1)} %slice.268), channel_id=1, source_target_pairs={{0,16},{16,32},{32,48},{48,64},{64,80},{80,96},{96,112},{112,128},... | collective-permute-start | bytes 11528 | tf_op jit(solution)/shard_map/ppermute | solution.py:18
  4.6 0.5 collective-permute-start.2
  5.2 1.0 slice_bitcast_fusion.32
  6.3 1.0 slice_bitcast_fusion.31
  7.2 0.8 copy.41
  9.0 2.7 %fusion.11 = bf16[64,1024]{1,0:T(8,128)(2,1)S(1)} fusion(f32[64,1054]{1,0:T(8,128)S(1)} %maximum_convert_fusion, f32[64]{0:T(128)S(1)} %get-tuple-element.84, f32[64]{0:T(128)S(1)} %get-tuple-element.85, f32[64]{0:T(128)S(1)} %get-tuple-element.56, f32[64]{0:T(128)S(1)} %get-tuple-element.57, f32[64]{0:T(128)S(1)} %get-tuple-element.58, ...), kind=kLoop, calls=%fused_computation.20 | loop fusion | flops 4063232 | bytes 8265472 | tf_op jit(solution)/shard_map/convert_element_type | solution.py:169
  11.8 0.9 reshape.65
  12.7 8.6 %all-to-all-start = ((bf16[16,2,2048]{2,1,0:T(2,128)(2,1)}), bf16[16,2,2048]{2,1,0:T(2,128)(2,1)S(1)}, u32[]{:S(2)}, u32[]{:S(2)}) async-start(bf16[16,2,2048]{2,1,0:T(2,128)(2,1)} %reshape.65), calls=%async_computation | async-start | bytes 262144 | tf_op jit(solution)/shard_map/all_to_all | solution.py:170
  21.4 8.5 %all-to-all-done = bf16[16,2,2048]{2,1,0:T(2,128)(2,1)S(1)} async-done(((bf16[16,2,2048]{2,1,0:T(2,128)(2,1)}), bf16[16,2,2048]{2,1,0:T(2,128)(2,1)S(1)}, u32[]{:S(2)}, u32[]{:S(2)}) %all-to-all-start) | async-done | bytes 131104 | tf_op jit(solution)/shard_map/all_to_all | solution.py:170
  30.4 0.3 copy.40
  30.9 0.3 fusion.6
  31.2 3.4 %multiply_reduce_fusion = (f32[64]{0:T(128)S(1)}, f32[64,2048]{1,0:T(8,128)S(1)}) fusion(bf16[1024,2048]{1,0:T(8,128)(2,1)} %param.18, f32[1024,64]{0,1:T(8,128)S(1)} %reshape.64, f32[1024]{0:T(1024)S(1)} %copy-done.5, f32[1024]{0:T(1024)S(1)} %copy-done.6, f32[64]{0:T(128)S(1)} %add_rsqrt_fusion.1, f32[64]{0:T(128)S(1)} %broadcast_multiply_fusion, ...), kind=kOutput, calls=%fused_computation.17 | convolution fusion | flops 269811648 | bytes 5251840 | tf_op jit(solution)/shard_map/dot_general | solution.py:177
  34.6 0.4 fusion.1
  35.0 18.1 %all_to_all.23 = bf16[16,8,2048]{2,1,0:T(8,128)(2,1)S(1)} all-to-all(bf16[16,8,2048]{2,1,0:T(8,128)(2,1)S(1)} %fusion.1), channel_id=1, replica_groups=mesh['sp'=16,'tp'=16] {'sp'}, dimensions={0} | all-to-all | bytes 1048576 | tf_op jit(solution)/shard_map/all_to_all | solution.py:204
  53.2 0.6 collective-permute-start.12
  53.8 2.7 %collective-permute-start.15 = (bf16[64,2048]{1,0:T(8,128)(2,1)S(1)}, bf16[64,2048]{1,0:T(8,128)(2,1)S(1)}, u32[]{:S(2)}, u32[]{:S(2)}) collective-permute-start(bf16[64,2048]{1,0:T(8,128)(2,1)S(1)} %get-tuple-element.54.refs_0_), channel_id=1, source_target_pairs={{0,14},{1,15},{2,0},{3,1},{4,2},{5,3},{6,4},{7,5},{8,6},{9,7},{10,... | collective-permute-start | bytes 786440 | tf_op jit(solution)/shard_map/ppermute | solution.py:23
  56.5 3.2 %collective-permute-start.8 = (bf16[64,2048]{1,0:T(8,128)(2,1)S(1)}, bf16[64,2048]{1,0:T(8,128)(2,1)S(1)}, u32[]{:S(2)}, u32[]{:S(2)}) collective-permute-start(bf16[64,2048]{1,0:T(8,128)(2,1)S(1)} %get-tuple-element.53.refs_1_), channel_id=1, source_target_pairs={{0,14},{1,15},{2,0},{3,1},{4,2},{5,3},{6,4},{7,5},{8,6},{9,7},{10,... | collective-permute-start | bytes 786440 | tf_op jit(solution)/shard_map/ppermute | solution.py:23
  59.7 3.9 %collective-permute-done.12.refs_3_ = bf16[64,2048]{1,0:T(8,128)(2,1)S(1)} collective-permute-done((bf16[64,2048]{1,0:T(8,128)(2,1)S(1)}, bf16[64,2048]{1,0:T(8,128)(2,1)S(1)}, u32[]{:S(2)}, u32[]{:S(2)}) %collective-permute-start.12) | collective-permute-done | bytes 262176 | tf_op jit(solution)/shard_map/ppermute | solution.py:23
  63.6 3.2 %collective-permute-start.16 = (bf16[64,2048]{1,0:T(8,128)(2,1)S(1)}, bf16[64,2048]{1,0:T(8,128)(2,1)S(1)}, u32[]{:S(2)}, u32[]{:S(2)}) collective-permute-start(bf16[64,2048]{1,0:T(8,128)(2,1)S(1)} %collective-permute-done.15.refs_4_), channel_id=1, source_target_pairs={{0,14},{1,15},{2,0},{3,1},{4,2},{5,3},{6,4},{7,5},{8,6},{9,7},{10,... | collective-permute-start | bytes 786440 | tf_op jit(solution)/shard_map/ppermute | solution.py:23
  66.9 2.4 %collective-permute-done.4.refs_2_ = bf16[64,2048]{1,0:T(8,128)(2,1)S(1)} collective-permute-done((bf16[64,2048]{1,0:T(8,128)(2,1)S(1)}, bf16[64,2048]{1,0:T(8,128)(2,1)S(1)}, u32[]{:S(2)}, u32[]{:S(2)}) %collective-permute-start.4) | collective-permute-done | bytes 262176 | tf_op jit(solution)/shard_map/ppermute | solution.py:23
  69.3 3.2 %collective-permute-start.9 = (bf16[64,2048]{1,0:T(8,128)(2,1)S(1)}, bf16[64,2048]{1,0:T(8,128)(2,1)S(1)}, u32[]{:S(2)}, u32[]{:S(2)}) collective-permute-start(bf16[64,2048]{1,0:T(8,128)(2,1)S(1)} %collective-permute-done.8.refs_5_), channel_id=1, source_target_pairs={{0,14},{1,15},{2,0},{3,1},{4,2},{5,3},{6,4},{7,5},{8,6},{9,7},{10,... | collective-permute-start | bytes 786440 | tf_op jit(solution)/shard_map/ppermute | solution.py:23
  72.5 8.5 %shard_map.127 = (bf16[64,2048]{1,0:T(8,128)(2,1)S(1)}, bf16[64,2048]{1,0:T(8,128)(2,1)S(1)}, bf16[64,2048]{1,0:T(8,128)(2,1)S(1)}, bf16[64,2048]{1,0:T(8,128)(2...) custom-call(bf16[64,2048]{1,0:T(8,128)(2,1)S(1)} %get-tuple-element.54.refs_0_, ...), custom_call_target="tpu_custom_call" | custom-call | flops 4227858432 | bytes 11010048 | tf_op jit(solution)/shard_map/pallas_call | solution.py:78
  81.0 0.7 collective-permute-start.10
  81.7 1.4 collective-permute-start.14
  83.1 1.8 %collective-permute-start.17 = (bf16[64,2048]{1,0:T(8,128)(2,1)S(1)}, bf16[64,2048]{1,0:T(8,128)(2,1)S(1)}, u32[]{:S(2)}, u32[]{:S(2)}) collective-permute-start(bf16[64,2048]{1,0:T(8,128)(2,1)S(1)} %collective-permute-done.16.refs_2_), channel_id=1, source_target_pairs={{0,14},{1,15},{2,0},{3,1},{4,2},{5,3},{6,4},{7,5},{8,6},{9,7},{10,... | collective-permute-start | bytes 786440 | tf_op jit(solution)/shard_map/ppermute | solution.py:23
  85.2 6.5 %shard_map.128 = (bf16[64,2048]{1,0:T(8,128)(2,1)S(1)}, bf16[64,2048]{1,0:T(8,128)(2,1)S(1)}, bf16[64,2048]{1,0:T(8,128)(2,1)S(1)}, bf16[64,2048]{1,0:T(8,128)(2,1)S(1)}) custom-call(bf16[64,2048]{1,0:T(8,128)(2,1)S(1)} %collective-permute-done.5.refs_0_, bf16[64,2048]{1,0:T(8,128)(2,1)S(1)} %collective-permute-done.13.refs_1_, ...), custom_call_target="tpu_custom_call" | custom-call | flops 2818572288 | bytes 11010048 | tf_op jit(solution)/shard_map/pallas_call | solution.py:78
  91.7 3.1 %collective-permute-start.11 = (bf16[64,2048]{1,0:T(8,128)(2,1)S(1)}, bf16[64,2048]{1,0:T(8,128)(2,1)S(1)}, u32[]{:S(2)}, u32[]{:S(2)}) collective-permute-start(bf16[64,2048]{1,0:T(8,128)(2,1)S(1)} %collective-permute-done.10.refs_3_), channel_id=1, source_target_pairs={{0,14},{1,15},{2,0},{3,1},{4,2},{5,3},{6,4},{7,5},{8,6},{9,7},{10,... | collective-permute-start | bytes 786440 | tf_op jit(solution)/shard_map/ppermute | solution.py:23
  94.8 6.5 %shard_map.129 = (bf16[64,2048]{1,0:T(8,128)(2,1)S(1)}, bf16[64,2048]{1,0:T(8,128)(2,1)S(1)}, bf16[64,2048]{1,0:T(8,128)(2,1)S(1)}, bf16[64,2048]{1,0:T(8,128)(2,1)S(1)}) custom-call(bf16[64,2048]{1,0:T(8,128)(2,1)S(1)} %collective-permute-done.6.refs_0_, bf16[64,2048]{1,0:T(8,128)(2,1)S(1)} %collective-permute-done.14.refs_1_, ...), custom_call_target="tpu_custom_call" | custom-call | flops 2818572288 | bytes 11010048 | tf_op jit(solution)/shard_map/pallas_call | solution.py:78
  101.4 1.0 collective-permute-done.7.refs_0_
  102.4 5.7 %shard_map.130 = (bf16[64,2048]{1,0:T(8,128)(2,1)S(1)}, bf16[64,2048]{1,0:T(8,128)(2,1)S(1)}) custom-call(bf16[64,2048]{1,0:T(8,128)(2,1)S(1)} %collective-permute-done.7.refs_0_, bf16[64,2048]{1,0:T(8,128)(2,1)S(1)} %collective-permute-done.11.refs_1_, bf16[448,2048]{1,0:T(8,128)(2,1)S(1)} %bitcast.99, ...), custom_call_target="tpu_custom_call" | custom-call | flops 1409286144 | bytes 11010048 | tf_op jit(solution)/shard_map/pallas_call | solution.py:78
  108.1 2.5 %collective-permute-start.28 = (bf16[64,2048]{1,0:T(8,128)(2,1)S(1)}, bf16[64,2048]{1,0:T(8,128)(2,1)S(1)}, u32[]{:S(2)}, u32[]{:S(2)}) collective-permute-start(bf16[64,2048]{1,0:T(8,128)(2,1)S(1)} %get-tuple-element.46), channel_id=1, source_target_pairs={{0,14},{1,15},{2,0},{3,1},{4,2},{5,3},{6,4},{7,5},{8,6},{9,7},{10,... | collective-permute-start | bytes 786440 | tf_op jit(solution)/shard_map/ppermute | solution.py:23
  110.7 3.3 %collective-permute-start.22 = (bf16[64,2048]{1,0:T(8,128)(2,1)S(1)}, bf16[64,2048]{1,0:T(8,128)(2,1)S(1)}, u32[]{:S(2)}, u32[]{:S(2)}) collective-permute-start(bf16[64,2048]{1,0:T(8,128)(2,1)S(1)} %get-tuple-element.37.refs_8_), channel_id=1, source_target_pairs={{0,14},{1,15},{2,0},{3,1},{4,2},{5,3},{6,4},{7,5},{8,6},{9,7},{10,... | collective-permute-start | bytes 786440 | tf_op jit(solution)/shard_map/ppermute | solution.py:23
  113.9 3.5 %collective-permute-done.28.a = bf16[64,2048]{1,0:T(8,128)(2,1)S(1)} collective-permute-done((bf16[64,2048]{1,0:T(8,128)(2,1)S(1)}, bf16[64,2048]{1,0:T(8,128)(2,1)S(1)}, u32[]{:S(2)}, u32[]{:S(2)}) %collective-permute-start.28) | collective-permute-done | bytes 262176 | tf_op jit(solution)/shard_map/ppermute | solution.py:23
  117.5 3.7 %collective-permute-start.29 = (bf16[64,2048]{1,0:T(8,128)(2,1)S(1)}, bf16[64,2048]{1,0:T(8,128)(2,1)S(1)}, u32[]{:S(2)}, u32[]{:S(2)}) collective-permute-start(bf16[64,2048]{1,0:T(8,128)(2,1)S(1)} %shard_map.138), channel_id=1, source_target_pairs={{0,14},{1,15},{2,0},{3,1},{4,2},{5,3},{6,4},{7,5},{8,6},{9,7},{10,... | collective-permute-start | bytes 786440 | tf_op jit(solution)/shard_map/ppermute | solution.py:23
  121.3 5.0 %collective-permute-done.25.a = bf16[64,2048]{1,0:T(8,128)(2,1)S(1)} collective-permute-done((bf16[64,2048]{1,0:T(8,128)(2,1)S(1)}, bf16[64,2048]{1,0:T(8,128)(2,1)S(1)}, u32[]{:S(2)}, u32[]{:S(2)}) %collective-permute-start.25) | collective-permute-done | bytes 262176 | tf_op jit(solution)/shard_map/ppermute | solution.py:23
  126.6 3.3 %collective-permute-start.23 = (bf16[64,2048]{1,0:T(8,128)(2,1)S(1)}, bf16[64,2048]{1,0:T(8,128)(2,1)S(1)}, u32[]{:S(2)}, u32[]{:S(2)}) collective-permute-start(bf16[64,2048]{1,0:T(8,128)(2,1)S(1)} %shard_map.134), channel_id=1, source_target_pairs={{0,14},{1,15},{2,0},{3,1},{4,2},{5,3},{6,4},{7,5},{8,6},{9,7},{10,... | collective-permute-start | bytes 786440 | tf_op jit(solution)/shard_map/ppermute | solution.py:23
  129.9 1.8 %collective-permute-start.30 = (bf16[64,2048]{1,0:T(8,128)(2,1)S(1)}, bf16[64,2048]{1,0:T(8,128)(2,1)S(1)}, u32[]{:S(2)}, u32[]{:S(2)}) collective-permute-start(bf16[64,2048]{1,0:T(8,128)(2,1)S(1)} %shard_map.139), channel_id=1, source_target_pairs={{0,14},{1,15},{2,0},{3,1},{4,2},{5,3},{6,4},{7,5},{8,6},{9,7},{10,... | collective-permute-start | bytes 786440 | tf_op jit(solution)/shard_map/ppermute | solution.py:23
  132.2 5.4 %collective-permute-done.26.a = bf16[64,2048]{1,0:T(8,128)(2,1)S(1)} collective-permute-done((bf16[64,2048]{1,0:T(8,128)(2,1)S(1)}, bf16[64,2048]{1,0:T(8,128)(2,1)S(1)}, u32[]{:S(2)}, u32[]{:S(2)}) %collective-permute-start.26) | collective-permute-done | bytes 262176 | tf_op jit(solution)/shard_map/ppermute | solution.py:23
  137.8 3.3 %collective-permute-start.24 = (bf16[64,2048]{1,0:T(8,128)(2,1)S(1)}, bf16[64,2048]{1,0:T(8,128)(2,1)S(1)}, u32[]{:S(2)}, u32[]{:S(2)}) collective-permute-start(bf16[64,2048]{1,0:T(8,128)(2,1)S(1)} %shard_map.135), channel_id=1, source_target_pairs={{0,14},{1,15},{2,0},{3,1},{4,2},{5,3},{6,4},{7,5},{8,6},{9,7},{10,... | collective-permute-start | bytes 786440 | tf_op jit(solution)/shard_map/ppermute | solution.py:23
  141.2 3.8 %collective-permute-start.31 = (bf16[64,2048]{1,0:T(8,128)(2,1)S(1)}, bf16[64,2048]{1,0:T(8,128)(2,1)S(1)}, u32[]{:S(2)}, u32[]{:S(2)}) collective-permute-start(bf16[64,2048]{1,0:T(8,128)(2,1)S(1)} %shard_map.140), channel_id=1, source_target_pairs={{0,14},{1,15},{2,0},{3,1},{4,2},{5,3},{6,4},{7,5},{8,6},{9,7},{10,... | collective-permute-start | bytes 786440 | tf_op jit(solution)/shard_map/ppermute | solution.py:23
  145.1 2.0 %collective-permute-done.27.right_b = bf16[64,2048]{1,0:T(8,128)(2,1)S(1)} collective-permute-done((bf16[64,2048]{1,0:T(8,128)(2,1)S(1)}, bf16[64,2048]{1,0:T(8,128)(2,1)S(1)}, u32[]{:S(2)}, u32[]{:S(2)}) %collective-permute-start.27) | collective-permute-done | bytes 262176 | tf_op jit(solution)/shard_map/ppermute | solution.py:23
  147.1 1.7 %collective-permute-done.31.left_b = bf16[64,2048]{1,0:T(8,128)(2,1)S(1)} collective-permute-done((bf16[64,2048]{1,0:T(8,128)(2,1)S(1)}, bf16[64,2048]{1,0:T(8,128)(2,1)S(1)}, u32[]{:S(2)}, u32[]{:S(2)}) %collective-permute-start.31) | collective-permute-done | bytes 262176 | tf_op jit(solution)/shard_map/ppermute | solution.py:23
  148.8 3.8 %collective-permute-done.21.right_a = bf16[64,2048]{1,0:T(8,128)(2,1)S(1)} collective-permute-done((bf16[64,2048]{1,0:T(8,128)(2,1)S(1)}, bf16[64,2048]{1,0:T(8,128)(2,1)S(1)}, u32[]{:S(2)}, u32[]{:S(2)}) %collective-permute-start.21) | collective-permute-done | bytes 262176 | tf_op jit(solution)/shard_map/ppermute | solution.py:23
  152.7 1.0 shard_map.141
  153.7 4.8 %all-to-all-start.2 = ((bf16[16,8,2048]{2,1,0:T(8,128)(2,1)}), bf16[16,8,2048]{2,1,0:T(8,128)(2,1)S(1)}, u32[]{:S(2)}, u32[]{:S(2)}) async-start(bf16[16,8,2048]{2,1,0:T(8,128)(2,1)} %bitcast.43), calls=%async_computation.2 | async-start | bytes 1048576 | tf_op jit(solution)/shard_map/all_to_all | solution.py:238
  158.6 8.7 %all-to-all-done.2 = bf16[16,8,2048]{2,1,0:T(8,128)(2,1)S(1)} async-done(((bf16[16,8,2048]{2,1,0:T(8,128)(2,1)}), bf16[16,8,2048]{2,1,0:T(8,128)(2,1)S(1)}, u32[]{:S(2)}, u32[]{:S(2)}) %all-to-all-start.2) | async-done | bytes 524320 | tf_op jit(solution)/shard_map/all_to_all | solution.py:238
  167.6 0.9 fusion.4
  (87 shorter events, 4.1 us)
Async XLA Ops:
  1.1 7.7 %collective-permute-start = (bf16[64,30]{1,0:T(8,128)(2,1)S(1)}, bf16[64,30]{1,0:T(8,128)(2,1)S(1)}, u32[]{:S(2)}, u32[]{:S(2)}) collective-permute-start(bf16[64,30]{1,0:T(8,128)(2,1)S(1)} %slice.268), channel_id=1, source_target_pairs={{0,16},{16,32},{32,48},{48,64},{64,80},{80,96},{96,112},{112,128},... | collective-permute-start | bytes 11528 | tf_op jit(solution)/shard_map/ppermute | solution.py:18
  4.5 48.6 %collective-permute-start.1 = (bf16[448,2048]{1,0:T(8,128)(2,1)}, bf16[448,2048]{1,0:T(8,128)(2,1)S(1)}, u32[]{:S(2)}, u32[]{:S(2)}) collective-permute-start(bf16[448,2048]{1,0:T(8,128)(2,1)} %bitcast.95), channel_id=1, source_target_pairs={{0,1},{1,0},{2,3},{3,2},{4,5},{5,4},{6,7},{7,6},{8,9},{9,8},{10,11... | collective-permute-start | bytes 5505032 | tf_op jit(solution)/shard_map/ppermute | solution.py:28
  4.6 48.5 %collective-permute-start.2 = (bf16[448,2048]{1,0:T(8,128)(2,1)}, bf16[448,2048]{1,0:T(8,128)(2,1)}, u32[]{:S(2)}, u32[]{:S(2)}) collective-permute-start(bf16[448,2048]{1,0:T(8,128)(2,1)} %bitcast.100), channel_id=1, source_target_pairs={{0,1},{1,0},{2,3},{3,2},{4,5},{5,4},{6,7},{7,6},{8,9},{9,8},{10,11... | collective-permute-start | bytes 5505032 | tf_op jit(solution)/shard_map/ppermute | solution.py:28
  5.1 48.0 %collective-permute-start.3 = (bf16[448,2048]{1,0:T(8,128)(2,1)}, bf16[448,2048]{1,0:T(8,128)(2,1)}, u32[]{:S(2)}, u32[]{:S(2)}) collective-permute-start(bf16[448,2048]{1,0:T(8,128)(2,1)} %bitcast.105), channel_id=1, source_target_pairs={{0,1},{1,0},{2,3},{3,2},{4,5},{5,4},{6,7},{7,6},{8,9},{9,8},{10,11... | collective-permute-start | bytes 5505032 | tf_op jit(solution)/shard_map/ppermute | solution.py:28
  8.9 12.4 %copy-start.7 = (s32[64,2]{0,1:T(2,128)S(1)}, s32[64,2]{0,1:T(2,128)}, u32[]{:S(2)}) copy-start(s32[64,2]{0,1:T(2,128)} %param.20) | copy-start | bytes 1540
  12.7 17.2 %all-to-all-start = ((bf16[16,2,2048]{2,1,0:T(2,128)(2,1)}), bf16[16,2,2048]{2,1,0:T(2,128)(2,1)S(1)}, u32[]{:S(2)}, u32[]{:S(2)}) async-start(bf16[16,2,2048]{2,1,0:T(2,128)(2,1)} %reshape.65), calls=%async_computation | async-start | bytes 262144 | tf_op jit(solution)/shard_map/all_to_all | solution.py:170
  21.3 9.8 %copy-start.3 = (bf16[64,2048]{1,0:T(8,128)(2,1)S(1)}, bf16[64,2048]{1,0:T(8,128)(2,1)}, u32[]{:S(2)}) copy-start(bf16[64,2048]{1,0:T(8,128)(2,1)} %param.19) | copy-start | bytes 786436
  21.3 9.8 %copy-start.5 = (f32[1024]{0:T(1024)S(1)}, f32[1024]{0:T(1024)}, u32[]{:S(2)}) copy-start(f32[1024]{0:T(1024)} %param.17) | copy-start | bytes 12292
  21.3 9.8 %copy-start.6 = (f32[1024]{0:T(1024)S(1)}, f32[1024]{0:T(1024)}, u32[]{:S(2)}) copy-start(f32[1024]{0:T(1024)} %param.16) | copy-start | bytes 12292
  31.1 3.5 %copy-start.4 = (f32[2048]{0:T(1024)S(1)}, f32[2048]{0:T(1024)}, u32[]{:S(2)}) copy-start(f32[2048]{0:T(1024)} %param.22) | copy-start | bytes 24580
  31.2 41.3 %copy-start.1 = (bf16[1,2048,448]{1,2,0:T(8,128)(2,1)S(1)}, bf16[1,2048,448]{1,2,0:T(8,128)(2,1)}, u32[]{:S(2)}) copy-start(bf16[1,2048,448]{1,2,0:T(8,128)(2,1)} %param.24) | copy-start | bytes 5505028
  31.2 41.3 %copy-start.2 = (bf16[1,448,2048]{2,1,0:T(8,128)(2,1)S(1)}, bf16[1,448,2048]{2,1,0:T(8,128)(2,1)}, u32[]{:S(2)}) copy-start(bf16[1,448,2048]{2,1,0:T(8,128)(2,1)} %param.25) | copy-start | bytes 5505028
  34.6 37.9 %copy-start = (bf16[1,2048,448]{1,2,0:T(8,128)(2,1)S(1)}, bf16[1,2048,448]{1,2,0:T(8,128)(2,1)}, u32[]{:S(2)}) copy-start(bf16[1,2048,448]{1,2,0:T(8,128)(2,1)} %param.23) | copy-start | bytes 5505028
  53.2 10.5 %collective-permute-start.12 = (bf16[64,2048]{1,0:T(8,128)(2,1)S(1)}, bf16[64,2048]{1,0:T(8,128)(2,1)S(1)}, u32[]{:S(2)}, u32[]{:S(2)}) collective-permute-start(bf16[64,2048]{1,0:T(8,128)(2,1)S(1)} %get-tuple-element.53.refs_1_), channel_id=1, source_target_pairs={{0,2},{1,3},{2,4},{3,5},{4,6},{5,7},{6,8},{7,9},{8,10},{9,11},{10,... | collective-permute-start | bytes 786440 | tf_op jit(solution)/shard_map/ppermute | solution.py:23
  53.8 9.8 %collective-permute-start.15 = (bf16[64,2048]{1,0:T(8,128)(2,1)S(1)}, bf16[64,2048]{1,0:T(8,128)(2,1)S(1)}, u32[]{:S(2)}, u32[]{:S(2)}) collective-permute-start(bf16[64,2048]{1,0:T(8,128)(2,1)S(1)} %get-tuple-element.54.refs_0_), channel_id=1, source_target_pairs={{0,14},{1,15},{2,0},{3,1},{4,2},{5,3},{6,4},{7,5},{8,6},{9,7},{10,... | collective-permute-start | bytes 786440 | tf_op jit(solution)/shard_map/ppermute | solution.py:23
  56.5 12.8 %collective-permute-start.4 = (bf16[64,2048]{1,0:T(8,128)(2,1)S(1)}, bf16[64,2048]{1,0:T(8,128)(2,1)S(1)}, u32[]{:S(2)}, u32[]{:S(2)}) collective-permute-start(bf16[64,2048]{1,0:T(8,128)(2,1)S(1)} %get-tuple-element.54.refs_0_), channel_id=1, source_target_pairs={{0,2},{1,3},{2,4},{3,5},{4,6},{5,7},{6,8},{7,9},{8,10},{9,11},{10,... | collective-permute-start | bytes 786440 | tf_op jit(solution)/shard_map/ppermute | solution.py:23
  56.5 12.8 %collective-permute-start.8 = (bf16[64,2048]{1,0:T(8,128)(2,1)S(1)}, bf16[64,2048]{1,0:T(8,128)(2,1)S(1)}, u32[]{:S(2)}, u32[]{:S(2)}) collective-permute-start(bf16[64,2048]{1,0:T(8,128)(2,1)S(1)} %get-tuple-element.53.refs_1_), channel_id=1, source_target_pairs={{0,14},{1,15},{2,0},{3,1},{4,2},{5,3},{6,4},{7,5},{8,6},{9,7},{10,... | collective-permute-start | bytes 786440 | tf_op jit(solution)/shard_map/ppermute | solution.py:23
  63.6 18.1 %collective-permute-start.13 = (bf16[64,2048]{1,0:T(8,128)(2,1)S(1)}, bf16[64,2048]{1,0:T(8,128)(2,1)S(1)}, u32[]{:S(2)}, u32[]{:S(2)}) collective-permute-start(bf16[64,2048]{1,0:T(8,128)(2,1)S(1)} %collective-permute-done.12.refs_3_), channel_id=1, source_target_pairs={{0,2},{1,3},{2,4},{3,5},{4,6},{5,7},{6,8},{7,9},{8,10},{9,11},{10,... | collective-permute-start | bytes 786440 | tf_op jit(solution)/shard_map/ppermute | solution.py:23
  63.6 19.5 %collective-permute-start.16 = (bf16[64,2048]{1,0:T(8,128)(2,1)S(1)}, bf16[64,2048]{1,0:T(8,128)(2,1)S(1)}, u32[]{:S(2)}, u32[]{:S(2)}) collective-permute-start(bf16[64,2048]{1,0:T(8,128)(2,1)S(1)} %collective-permute-done.15.refs_4_), channel_id=1, source_target_pairs={{0,14},{1,15},{2,0},{3,1},{4,2},{5,3},{6,4},{7,5},{8,6},{9,7},{10,... | collective-permute-start | bytes 786440 | tf_op jit(solution)/shard_map/ppermute | solution.py:23
  69.3 15.7 %collective-permute-start.5 = (bf16[64,2048]{1,0:T(8,128)(2,1)S(1)}, bf16[64,2048]{1,0:T(8,128)(2,1)S(1)}, u32[]{:S(2)}, u32[]{:S(2)}) collective-permute-start(bf16[64,2048]{1,0:T(8,128)(2,1)S(1)} %collective-permute-done.4.refs_2_), channel_id=1, source_target_pairs={{0,2},{1,3},{2,4},{3,5},{4,6},{5,7},{6,8},{7,9},{8,10},{9,11},{10,... | collective-permute-start | bytes 786440 | tf_op jit(solution)/shard_map/ppermute | solution.py:23
  69.3 11.8 %collective-permute-start.9 = (bf16[64,2048]{1,0:T(8,128)(2,1)S(1)}, bf16[64,2048]{1,0:T(8,128)(2,1)S(1)}, u32[]{:S(2)}, u32[]{:S(2)}) collective-permute-start(bf16[64,2048]{1,0:T(8,128)(2,1)S(1)} %collective-permute-done.8.refs_5_), channel_id=1, source_target_pairs={{0,14},{1,15},{2,0},{3,1},{4,2},{5,3},{6,4},{7,5},{8,6},{9,7},{10,... | collective-permute-start | bytes 786440 | tf_op jit(solution)/shard_map/ppermute | solution.py:23
  81.0 10.7 %collective-permute-start.10 = (bf16[64,2048]{1,0:T(8,128)(2,1)S(1)}, bf16[64,2048]{1,0:T(8,128)(2,1)S(1)}, u32[]{:S(2)}, u32[]{:S(2)}) collective-permute-start(bf16[64,2048]{1,0:T(8,128)(2,1)S(1)} %collective-permute-done.9.refs_3_), channel_id=1, source_target_pairs={{0,14},{1,15},{2,0},{3,1},{4,2},{5,3},{6,4},{7,5},{8,6},{9,7},{10,... | collective-permute-start | bytes 786440 | tf_op jit(solution)/shard_map/ppermute | solution.py:23
  81.7 13.1 %collective-permute-start.14 = (bf16[64,2048]{1,0:T(8,128)(2,1)S(1)}, bf16[64,2048]{1,0:T(8,128)(2,1)S(1)}, u32[]{:S(2)}, u32[]{:S(2)}) collective-permute-start(bf16[64,2048]{1,0:T(8,128)(2,1)S(1)} %collective-permute-done.13.refs_1_), channel_id=1, source_target_pairs={{0,2},{1,3},{2,4},{3,5},{4,6},{5,7},{6,8},{7,9},{8,10},{9,11},{10,... | collective-permute-start | bytes 786440 | tf_op jit(solution)/shard_map/ppermute | solution.py:23
  83.1 11.7 %collective-permute-start.17 = (bf16[64,2048]{1,0:T(8,128)(2,1)S(1)}, bf16[64,2048]{1,0:T(8,128)(2,1)S(1)}, u32[]{:S(2)}, u32[]{:S(2)}) collective-permute-start(bf16[64,2048]{1,0:T(8,128)(2,1)S(1)} %collective-permute-done.16.refs_2_), channel_id=1, source_target_pairs={{0,14},{1,15},{2,0},{3,1},{4,2},{5,3},{6,4},{7,5},{8,6},{9,7},{10,... | collective-permute-start | bytes 786440 | tf_op jit(solution)/shard_map/ppermute | solution.py:23
  84.9 9.8 %collective-permute-start.6 = (bf16[64,2048]{1,0:T(8,128)(2,1)S(1)}, bf16[64,2048]{1,0:T(8,128)(2,1)S(1)}, u32[]{:S(2)}, u32[]{:S(2)}) collective-permute-start(bf16[64,2048]{1,0:T(8,128)(2,1)S(1)} %collective-permute-done.5.refs_0_), channel_id=1, source_target_pairs={{0,2},{1,3},{2,4},{3,5},{4,6},{5,7},{6,8},{7,9},{8,10},{9,11},{10,... | collective-permute-start | bytes 786440 | tf_op jit(solution)/shard_map/ppermute | solution.py:23
  91.7 9.7 %collective-permute-start.11 = (bf16[64,2048]{1,0:T(8,128)(2,1)S(1)}, bf16[64,2048]{1,0:T(8,128)(2,1)S(1)}, u32[]{:S(2)}, u32[]{:S(2)}) collective-permute-start(bf16[64,2048]{1,0:T(8,128)(2,1)S(1)} %collective-permute-done.10.refs_3_), channel_id=1, source_target_pairs={{0,14},{1,15},{2,0},{3,1},{4,2},{5,3},{6,4},{7,5},{8,6},{9,7},{10,... | collective-permute-start | bytes 786440 | tf_op jit(solution)/shard_map/ppermute | solution.py:23
  94.8 7.6 %collective-permute-start.7 = (bf16[64,2048]{1,0:T(8,128)(2,1)S(1)}, bf16[64,2048]{1,0:T(8,128)(2,1)S(1)}, u32[]{:S(2)}, u32[]{:S(2)}) collective-permute-start(bf16[64,2048]{1,0:T(8,128)(2,1)S(1)} %collective-permute-done.6.refs_0_), channel_id=1, source_target_pairs={{0,2},{1,3},{2,4},{3,5},{4,6},{5,7},{6,8},{7,9},{8,10},{9,11},{10,... | collective-permute-start | bytes 786440 | tf_op jit(solution)/shard_map/ppermute | solution.py:23
  108.1 9.3 %collective-permute-start.28 = (bf16[64,2048]{1,0:T(8,128)(2,1)S(1)}, bf16[64,2048]{1,0:T(8,128)(2,1)S(1)}, u32[]{:S(2)}, u32[]{:S(2)}) collective-permute-start(bf16[64,2048]{1,0:T(8,128)(2,1)S(1)} %get-tuple-element.46), channel_id=1, source_target_pairs={{0,14},{1,15},{2,0},{3,1},{4,2},{5,3},{6,4},{7,5},{8,6},{9,7},{10,... | collective-permute-start | bytes 786440 | tf_op jit(solution)/shard_map/ppermute | solution.py:23
  110.6 10.5 %collective-permute-start.18 = (bf16[64,2048]{1,0:T(8,128)(2,1)S(1)}, bf16[64,2048]{1,0:T(8,128)(2,1)S(1)}, u32[]{:S(2)}, u32[]{:S(2)}) collective-permute-start(bf16[64,2048]{1,0:T(8,128)(2,1)S(1)} %get-tuple-element.38), channel_id=1, source_target_pairs={{0,2},{1,3},{2,4},{3,5},{4,6},{5,7},{6,8},{7,9},{8,10},{9,11},{10,... | collective-permute-start | bytes 786440 | tf_op jit(solution)/shard_map/ppermute | solution.py:23
  110.7 15.7 %collective-permute-start.25 = (bf16[64,2048]{1,0:T(8,128)(2,1)S(1)}, bf16[64,2048]{1,0:T(8,128)(2,1)S(1)}, u32[]{:S(2)}, u32[]{:S(2)}) collective-permute-start(bf16[64,2048]{1,0:T(8,128)(2,1)S(1)} %get-tuple-element.43), channel_id=1, source_target_pairs={{0,2},{1,3},{2,4},{3,5},{4,6},{5,7},{6,8},{7,9},{8,10},{9,11},{10,... | collective-permute-start | bytes 786440 | tf_op jit(solution)/shard_map/ppermute | solution.py:23
  110.7 15.8 %collective-permute-start.22 = (bf16[64,2048]{1,0:T(8,128)(2,1)S(1)}, bf16[64,2048]{1,0:T(8,128)(2,1)S(1)}, u32[]{:S(2)}, u32[]{:S(2)}) collective-permute-start(bf16[64,2048]{1,0:T(8,128)(2,1)S(1)} %get-tuple-element.37.refs_8_), channel_id=1, source_target_pairs={{0,14},{1,15},{2,0},{3,1},{4,2},{5,3},{6,4},{7,5},{8,6},{9,7},{10,... | collective-permute-start | bytes 786440 | tf_op jit(solution)/shard_map/ppermute | solution.py:23
  117.5 12.3 %collective-permute-start.29 = (bf16[64,2048]{1,0:T(8,128)(2,1)S(1)}, bf16[64,2048]{1,0:T(8,128)(2,1)S(1)}, u32[]{:S(2)}, u32[]{:S(2)}) collective-permute-start(bf16[64,2048]{1,0:T(8,128)(2,1)S(1)} %shard_map.138), channel_id=1, source_target_pairs={{0,14},{1,15},{2,0},{3,1},{4,2},{5,3},{6,4},{7,5},{8,6},{9,7},{10,... | collective-permute-start | bytes 786440 | tf_op jit(solution)/shard_map/ppermute | solution.py:23
  121.2 10.7 %collective-permute-start.19 = (bf16[64,2048]{1,0:T(8,128)(2,1)S(1)}, bf16[64,2048]{1,0:T(8,128)(2,1)S(1)}, u32[]{:S(2)}, u32[]{:S(2)}) collective-permute-start(bf16[64,2048]{1,0:T(8,128)(2,1)S(1)} %shard_map.131), channel_id=1, source_target_pairs={{0,2},{1,3},{2,4},{3,5},{4,6},{5,7},{6,8},{7,9},{8,10},{9,11},{10,... | collective-permute-start | bytes 786440 | tf_op jit(solution)/shard_map/ppermute | solution.py:23
  126.4 11.2 %collective-permute-start.26 = (bf16[64,2048]{1,0:T(8,128)(2,1)S(1)}, bf16[64,2048]{1,0:T(8,128)(2,1)S(1)}, u32[]{:S(2)}, u32[]{:S(2)}) collective-permute-start(bf16[64,2048]{1,0:T(8,128)(2,1)S(1)} %shard_map.136), channel_id=1, source_target_pairs={{0,2},{1,3},{2,4},{3,5},{4,6},{5,7},{6,8},{7,9},{8,10},{9,11},{10,... | collective-permute-start | bytes 786440 | tf_op jit(solution)/shard_map/ppermute | solution.py:23
  126.6 11.2 %collective-permute-start.23 = (bf16[64,2048]{1,0:T(8,128)(2,1)S(1)}, bf16[64,2048]{1,0:T(8,128)(2,1)S(1)}, u32[]{:S(2)}, u32[]{:S(2)}) collective-permute-start(bf16[64,2048]{1,0:T(8,128)(2,1)S(1)} %shard_map.134), channel_id=1, source_target_pairs={{0,14},{1,15},{2,0},{3,1},{4,2},{5,3},{6,4},{7,5},{8,6},{9,7},{10,... | collective-permute-start | bytes 786440 | tf_op jit(solution)/shard_map/ppermute | solution.py:23
  129.9 11.2 %collective-permute-start.30 = (bf16[64,2048]{1,0:T(8,128)(2,1)S(1)}, bf16[64,2048]{1,0:T(8,128)(2,1)S(1)}, u32[]{:S(2)}, u32[]{:S(2)}) collective-permute-start(bf16[64,2048]{1,0:T(8,128)(2,1)S(1)} %shard_map.139), channel_id=1, source_target_pairs={{0,14},{1,15},{2,0},{3,1},{4,2},{5,3},{6,4},{7,5},{8,6},{9,7},{10,... | collective-permute-start | bytes 786440 | tf_op jit(solution)/shard_map/ppermute | solution.py:23
  132.0 12.9 %collective-permute-start.20 = (bf16[64,2048]{1,0:T(8,128)(2,1)S(1)}, bf16[64,2048]{1,0:T(8,128)(2,1)S(1)}, u32[]{:S(2)}, u32[]{:S(2)}) collective-permute-start(bf16[64,2048]{1,0:T(8,128)(2,1)S(1)} %shard_map.132), channel_id=1, source_target_pairs={{0,2},{1,3},{2,4},{3,5},{4,6},{5,7},{6,8},{7,9},{8,10},{9,11},{10,... | collective-permute-start | bytes 786440 | tf_op jit(solution)/shard_map/ppermute | solution.py:23
  137.6 9.5 %collective-permute-start.27 = (bf16[64,2048]{1,0:T(8,128)(2,1)S(1)}, bf16[64,2048]{1,0:T(8,128)(2,1)S(1)}, u32[]{:S(2)}, u32[]{:S(2)}) collective-permute-start(bf16[64,2048]{1,0:T(8,128)(2,1)S(1)} %shard_map.137), channel_id=1, source_target_pairs={{0,2},{1,3},{2,4},{3,5},{4,6},{5,7},{6,8},{7,9},{8,10},{9,11},{10,... | collective-permute-start | bytes 786440 | tf_op jit(solution)/shard_map/ppermute | solution.py:23
  137.8 9.3 %collective-permute-start.24 = (bf16[64,2048]{1,0:T(8,128)(2,1)S(1)}, bf16[64,2048]{1,0:T(8,128)(2,1)S(1)}, u32[]{:S(2)}, u32[]{:S(2)}) collective-permute-start(bf16[64,2048]{1,0:T(8,128)(2,1)S(1)} %shard_map.135), channel_id=1, source_target_pairs={{0,14},{1,15},{2,0},{3,1},{4,2},{5,3},{6,4},{7,5},{8,6},{9,7},{10,... | collective-permute-start | bytes 786440 | tf_op jit(solution)/shard_map/ppermute | solution.py:23
  141.2 7.7 %collective-permute-start.31 = (bf16[64,2048]{1,0:T(8,128)(2,1)S(1)}, bf16[64,2048]{1,0:T(8,128)(2,1)S(1)}, u32[]{:S(2)}, u32[]{:S(2)}) collective-permute-start(bf16[64,2048]{1,0:T(8,128)(2,1)S(1)} %shard_map.140), channel_id=1, source_target_pairs={{0,14},{1,15},{2,0},{3,1},{4,2},{5,3},{6,4},{7,5},{8,6},{9,7},{10,... | collective-permute-start | bytes 786440 | tf_op jit(solution)/shard_map/ppermute | solution.py:23
  144.9 13.6 %copy-start.8 = (f32[64,2]{0,1:T(2,128)S(1)}, f32[64,2]{0,1:T(2,128)}, u32[]{:S(2)}) copy-start(f32[64,2]{0,1:T(2,128)} %param.21) | copy-start | bytes 1540
  145.0 7.7 %collective-permute-start.21 = (bf16[64,2048]{1,0:T(8,128)(2,1)S(1)}, bf16[64,2048]{1,0:T(8,128)(2,1)S(1)}, u32[]{:S(2)}, u32[]{:S(2)}) collective-permute-start(bf16[64,2048]{1,0:T(8,128)(2,1)S(1)} %shard_map.133), channel_id=1, source_target_pairs={{0,2},{1,3},{2,4},{3,5},{4,6},{5,7},{6,8},{7,9},{8,10},{9,11},{10,... | collective-permute-start | bytes 786440 | tf_op jit(solution)/shard_map/ppermute | solution.py:23
  153.7 13.7 %all-to-all-start.2 = ((bf16[16,8,2048]{2,1,0:T(8,128)(2,1)}), bf16[16,8,2048]{2,1,0:T(8,128)(2,1)S(1)}, u32[]{:S(2)}, u32[]{:S(2)}) async-start(bf16[16,8,2048]{2,1,0:T(8,128)(2,1)} %bitcast.43), calls=%async_computation.2 | async-start | bytes 1048576 | tf_op jit(solution)/shard_map/all_to_all | solution.py:238

commit v2 on v1

v2 whole, which is shorter than its diff:
```python
import functools
import jax
import jax.numpy as jnp
from jax import lax
from jax.experimental import pallas as pl
from jax.experimental.pallas import tpu as pltpu
from jax.sharding import PartitionSpec as P

epsilon = 1e-06
f32 = jnp.float32
bf16 = jnp.bfloat16
VMEM_LIMIT = 12 << 20
TILE = 128
EXPERTS = 16


def shifted(value, axis, steps):
    count = lax.axis_size(axis)
    initial, last = (max(0, -steps), min(count, count - steps))
    return lax.ppermute(value, axis, [(source, source + steps) for source in range(initial, last)])


def z_shift(value, steps):
    count = lax.axis_size("tp")
    return lax.ppermute(value, "tp", [(i, (i + 2 * steps) % count) for i in range(count)])


def other_core(value):
    count = lax.axis_size("tp")
    return lax.ppermute(value, "tp", [(i, i ^ 1) for i in range(count)])


def contract_last(a, b):
    return lax.dot_general(a, b, (((1,), (1,)), ((), ())), preferred_element_type=f32)


def expert_kernel(sizes, block, with_token, *refs):
    count = len(sizes)
    pieces = refs[:count]
    gate_a, gate_b, up_a, up_b, down_a, down_b = refs[count : count + 6]
    at = count + 6 + with_token
    outs = refs[at : at + count]
    rows, total = refs[at + count :]
    starts = [sum(sizes[:i]) for i in range(count)]
    for start, size, piece in zip(starts, sizes, pieces):
        rows[start : start + size, :] = piece[...]
    x = rows[...]

    def partial(step):
        at = pl.ds(pl.multiple_of(step * block, block), block)
        both = lambda a, b: jnp.concatenate([a[at, :], b[at, :]], axis=0)
        gate_val = contract_last(x, both(gate_a, gate_b))
        up_val = contract_last(x, both(up_a, up_b))
        hidden = (jax.nn.silu(gate_val) * up_val).astype(bf16)
        return jnp.dot(hidden, both(down_a, down_b), preferred_element_type=f32)

    total[...] = jnp.zeros_like(total)

    @pl.loop(0, gate_a.shape[0] // block)
    def _(step):
        total[...] += partial(step)

    for start, size, out in zip(starts, sizes, outs):
        out[...] = total[start : start + size, :].astype(bf16)


def in_vmem(count):
    return [pl.BlockSpec(memory_space=pltpu.VMEM)] * count


def expert(pieces, weights, token=None):
    sizes = tuple(p.shape[0] for p in pieces)
    width = pieces[0].shape[1]
    hidden = weights[0].shape[0]
    tokens = () if token is None else (token,)
    flops = 2 * 3 * sum(sizes) * width * 2 * hidden
    return pl.pallas_call(
        functools.partial(expert_kernel, sizes, hidden // 2, len(tokens)),
        in_specs=in_vmem(len(sizes) + 6) + [pl.BlockSpec(memory_space=pl.ANY)] * len(tokens),
        out_specs=in_vmem(len(sizes)),
        out_shape=[jax.ShapeDtypeStruct((size, width), bf16) for size in sizes],
        scratch_shapes=[
            pltpu.VMEM((sum(sizes), width), bf16),
            pltpu.VMEM((sum(sizes), width), f32),
        ],
        compiler_params=pltpu.CompilerParams(vmem_limit_bytes=VMEM_LIMIT),
        cost_estimate=pl.CostEstimate(flops=flops, bytes_accessed=1 << 20, transcendentals=0),
    )(*pieces, *weights, *tokens)


def gated(value, gate):
    value, gate = value.astype(f32), gate.astype(f32)
    return (value * jax.nn.sigmoid(gate)).astype(bf16)


def position_major(lanes):
    pair = TILE // 4
    last = lanes.shape[1] - TILE
    here = lanes[:, :last]
    ahead = jnp.concatenate([lanes[:, pair:last], lanes[:, last : last + pair]], axis=1)
    return jnp.concatenate([here, ahead], axis=0).T


def tap_sum(laid, start, rows, taps):
    count = taps.shape[0]
    total = jnp.zeros((rows, laid.shape[1]), f32)
    for j in range(count):
        total = total + taps[j : j + 1, :] * laid[start + j : start + j + rows, :]
    return total.astype(bf16)


def twice(taps):
    return jnp.concatenate([taps[...], taps[...]], axis=1)


def conv_main_kernel(far_value, far_gate, far_taps, out, laid, value, gate, taps, arrived):
    pairs = ((far_value, value), (far_gate, gate), (far_taps, taps))
    fetches = [pltpu.make_async_copy(*pair, arrived.at[i]) for i, pair in enumerate(pairs)]
    for fetch in fetches:
        fetch.start()
    for fetch in fetches:
        fetch.wait()
    blocks, rows, _ = out.shape
    both = twice(taps)
    line = gated(value[...], gate[...]).astype(f32)
    line = jnp.concatenate([line, jnp.zeros((line.shape[0], TILE), f32)], axis=1)
    laid[...] = position_major(line)
    lead = both.shape[0] - 1

    @pl.loop(1, blocks)
    def _(block):
        window = laid[pl.ds(pl.multiple_of(2 * rows * (block - 1) + rows, rows), 2 * rows), :]
        out[block, :, :] = tap_sum(window, rows - lead, rows, both)


def conv_first_kernel(rim, value, gate, taps, _, out, laid):
    rows = out.shape[1]
    both = twice(taps)
    line = gated(value[...], gate[...]).astype(f32)
    line = jnp.concatenate([rim[...].astype(f32), line, jnp.zeros_like(line)], axis=1)
    laid[...] = position_major(line)
    lead = both.shape[0] - 1
    out[0, :, :] = tap_sum(laid, rim.shape[1] - lead, rows, both)


def convolve(conv_value, conv_gate, taps, rim, blocks):
    channels, length = conv_value.shape
    rows = length // blocks // 2
    shape = jax.ShapeDtypeStruct((blocks, rows, 2 * channels), bf16)
    main = pl.pallas_call(
        conv_main_kernel,
        in_specs=[pl.BlockSpec(memory_space=pltpu.HBM)] * 3,
        out_specs=in_vmem(1)[0],
        out_shape=shape,
        scratch_shapes=[
            pltpu.VMEM((length, 2 * channels), f32),
            pltpu.VMEM(conv_value.shape, bf16),
            pltpu.VMEM(conv_gate.shape, bf16),
            pltpu.VMEM(taps.shape, f32),
            pltpu.SemaphoreType.DMA((3,)),
        ],
        compiler_params=pltpu.CompilerParams(vmem_limit_bytes=4 << 20),
        cost_estimate=pl.CostEstimate(flops=5 << 28, bytes_accessed=1 << 20, transcendentals=0),
    )(conv_value, conv_gate, taps)
    return pl.pallas_call(
        conv_first_kernel,
        grid=(1,),
        in_specs=[
            pl.BlockSpec(rim.shape, lambda i: (0, 0)),
            pl.BlockSpec((channels, TILE), lambda i: (0, 0)),
            pl.BlockSpec((channels, TILE), lambda i: (0, 0)),
            pl.BlockSpec(taps.shape, lambda i: (0, 0)),
            pl.BlockSpec(memory_space=pl.ANY),
        ],
        out_specs=pl.BlockSpec((1, rows, 2 * channels), lambda i: (0, 0, 0)),
        out_shape=shape,
        scratch_shapes=[pltpu.VMEM((rim.shape[1] + TILE, 2 * channels), f32)],
        input_output_aliases={4: 0},
        compiler_params=pltpu.CompilerParams(vmem_limit_bytes=4 << 20),
        cost_estimate=pl.CostEstimate(flops=1 << 27, bytes_accessed=1 << 16, transcendentals=0),
    )(rim, conv_value, conv_gate, taps, main)


def token_kernel(
    conv,
    gain,
    bias,
    out_weight,
    stream,
    expert_gain,
    routes,
    route_weights,
    send,
    residual,
    mixer_hi,
    mixer_lo,
):
    top, tokens = routes.shape
    slot_count = send.shape[0]
    capacity = slot_count // EXPERTS
    names = lax.broadcasted_iota(jnp.int32, (EXPERTS, tokens), 0)
    hits = [(names == routes[k : k + 1, :]).astype(f32) for k in range(top)]
    earlier = lax.broadcasted_iota(jnp.int32, (tokens, tokens), 0) < lax.broadcasted_iota(
        jnp.int32, (tokens, tokens), 1
    )
    before = jnp.dot(
        sum(hits).astype(bf16), earlier.astype(bf16), preferred_element_type=f32
    )
    places = lax.broadcasted_iota(jnp.int32, (slot_count, tokens), 0)
    chooser = jnp.zeros((slot_count, tokens), f32)
    weighted = jnp.zeros((slot_count, tokens), f32)
    for k in range(top):
        rank = jnp.sum(before * hits[k], axis=0, keepdims=True).astype(jnp.int32)
        taken = places == routes[k : k + 1, :] * capacity + rank
        chooser = chooser + jnp.where(taken, 1.0, 0.0)
        weighted = weighted + jnp.where(taken, route_weights[k : k + 1, :], 0.0)
        before = before + hits[k]
    upper = weighted.astype(bf16)
    mixer_hi[...] = upper
    mixer_lo[...] = (weighted - upper.astype(f32)).astype(bf16)

    parts, _, lanes = conv.shape
    half = lanes // 2
    x = jnp.concatenate(
        [
            jnp.concatenate([conv[p, :, :half] for p in range(parts)], axis=1),
            jnp.concatenate([conv[p, :, half:] for p in range(parts)], axis=1),
        ],
        axis=0,
    ).astype(f32)
    center = jnp.mean(x, axis=1, keepdims=True)
    x = x - center
    spread = jnp.mean(x * x, axis=1, keepdims=True)
    scaled = x * lax.rsqrt(spread + epsilon) * gain[...] + bias[...]
    active = jax.nn.silu(scaled).astype(bf16)
    projected = jnp.dot(active, out_weight[...], preferred_element_type=f32)
    kept = (stream[...].astype(f32) + projected).astype(bf16)
    residual[...] = kept
    kept = kept.astype(f32)
    scale = lax.rsqrt(jnp.mean(kept * kept, axis=1, keepdims=True) + epsilon)
    normed = (kept * scale * expert_gain[...]).astype(bf16)
    send[...] = jnp.dot(chooser.astype(bf16), normed, preferred_element_type=f32).astype(bf16)


def token_block(conv, gain, bias, out_weight, stream, expert_gain, routes, route_weights):
    top, tokens = routes.shape
    return pl.pallas_call(
        token_kernel,
        in_specs=in_vmem(8),
        out_specs=in_vmem(4),
        out_shape=[
            jax.ShapeDtypeStruct((top * tokens, stream.shape[1]), bf16),
            jax.ShapeDtypeStruct(stream.shape, bf16),
            jax.ShapeDtypeStruct((top * tokens, tokens), bf16),
            jax.ShapeDtypeStruct((top * tokens, tokens), bf16),
        ],
        compiler_params=pltpu.CompilerParams(vmem_limit_bytes=12 << 20),
        cost_estimate=pl.CostEstimate(flops=3 << 29, bytes_accessed=5 << 20, transcendentals=0),
    )(
        conv,
        gain[None, :],
        bias[None, :],
        out_weight,
        stream,
        expert_gain[None, :],
        routes,
        route_weights,
    )


def add_kernel(a, b, out):
    out[...] = (a[...].astype(f32) + b[...].astype(f32)).astype(bf16)


def add(a, b):
    return pl.pallas_call(
        add_kernel,
        out_shape=jax.ShapeDtypeStruct(a.shape, bf16),
        compiler_params=pltpu.CompilerParams(vmem_limit_bytes=4 << 20),
        cost_estimate=pl.CostEstimate(
            flops=a.size * 500, bytes_accessed=a.size * 6, transcendentals=0
        ),
    )(a, b)


def split_kernel(both, first, second):
    half = first.shape[0]
    first[...] = both[:half, :]
    second[...] = both[half:, :]


def split(both):
    half = jax.ShapeDtypeStruct((both.shape[0] // 2, both.shape[1]), both.dtype)
    return pl.pallas_call(
        split_kernel,
        in_specs=in_vmem(1),
        out_specs=in_vmem(2),
        out_shape=[half, half],
        compiler_params=pltpu.CompilerParams(vmem_limit_bytes=4 << 20),
    )(both)


def close_kernel(right_a, left_a, own_a, right_b, left_b, own_b, out):
    half = right_a.shape[0]
    out[:half, :] = (
        right_a[...].astype(f32) + left_a[...].astype(f32) + own_a[...].astype(f32)
    ).astype(bf16)
    out[half:, :] = (
        right_b[...].astype(f32) + left_b[...].astype(f32) + own_b[...].astype(f32)
    ).astype(bf16)


def close(*parts):
    half, width = parts[0].shape
    return pl.pallas_call(
        close_kernel,
        out_shape=jax.ShapeDtypeStruct((2 * half, width), bf16),
        compiler_params=pltpu.CompilerParams(vmem_limit_bytes=4 << 20),
    )(*parts)


def per_device(
    conv_value,
    conv_gate,
    conv_taps,
    norm_gain,
    norm_bias,
    out_weight,
    stream,
    routes,
    route_weights,
    expert_gain,
    expert_gate,
    expert_up,
    expert_down,
):
    run_len = conv_value.shape[1]
    rim = gated(conv_value[:, run_len - TILE :], conv_gate[:, run_len - TILE :])
    rim = shifted(rim, "sp", 1)
    blocks = lax.axis_size("tp")
    conv_out = convolve(conv_value, conv_gate, conv_taps.T, rim, blocks)
    tok_rows = stream.shape[0]
    width = stream.shape[1]
    top_count = routes.shape[1]
    experts = lax.axis_size("sp")
    capacity = top_count * tok_rows // experts
    whole_conv = lax.all_to_all(conv_out, "tp", split_axis=0, concat_axis=0, tiled=True)
    send_rows, residual, mixer_hi, mixer_lo = token_block(
        whole_conv,
        norm_gain,
        norm_bias,
        out_weight,
        stream,
        expert_gain,
        routes.T,
        route_weights.T,
    )
    mine = (expert_gate[0].T, expert_up[0].T, expert_down[0])
    send_rows, gone = lax.optimization_barrier((send_rows, mine))
    weights = [w for pair in zip(mine, map(other_core, gone)) for w in pair]
    send_rows = send_rows.reshape(experts, capacity, width)
    received = lax.all_to_all(send_rows, "sp", split_axis=0, concat_axis=0, tiled=True)
    received, weights = lax.optimization_barrier((received, weights))
    own = received.reshape(-1, width)

    far = lax.axis_size("tp") // 4
    from_left = {0: tuple(split(own))}
    from_right = {0: from_left[0]}
    for k in range(1, far + 1):
        left_a, left_b = from_left[k - 1]
        right_a, right_b = from_right[k - 1]
        from_left[k] = (z_shift(left_a, 1), z_shift(left_b, 1) if k < far else None)
        from_right[k] = (z_shift(right_a, -1) if k < far else None, z_shift(right_b, -1))

    first = expert((*from_left[0], *from_left[1], *from_right[1]), weights)
    part_own = first[0:2]
    part_left, part_right = {1: first[2:4]}, {1: first[4:6]}
    token = first[0]
    for k in range(2, far):
        parts = expert((*from_left[k], *from_right[k]), weights, token)
        part_left[k], part_right[k] = parts[0:2], parts[2:4]
        token = parts[0]
    right_b = z_shift(part_right[far - 1][1], 1)
    left_a = z_shift(part_left[far - 1][0], -1)
    antipode = expert((from_left[far][0], from_right[far][1]), weights, token)

    right_a, left_b = z_shift(antipode[0], 1), z_shift(antipode[1], -1)
    for k in range(far - 1, 0, -1):
        if k < far - 1:
            right_b = z_shift(add(right_b, part_right[k][1]), 1)
            left_a = z_shift(add(left_a, part_left[k][0]), -1)
        right_a = z_shift(add(right_a, part_right[k][0]), 1)
        left_b = z_shift(add(left_b, part_left[k][1]), -1)
    result = close(right_a, left_a, part_own[0], right_b, left_b, part_own[1])
    result = result.reshape(received.shape)
    returned = lax.all_to_all(result, "sp", split_axis=0, concat_axis=0, tiled=True)
    rows = returned.reshape(experts * capacity, width)

    def mix(weight):
        return lax.dot_general(weight, rows, (((0,), (0,)), ((), ())), preferred_element_type=f32)

    expert_sum = mix(mixer_hi) + mix(mixer_lo)
    return (residual.astype(f32) + expert_sum).astype(bf16)


def solution(mesh):
    return jax.shard_map(
        per_device,
        mesh=mesh,
        in_specs=(
            P("tp", "sp"),
            P("tp", "sp"),
            P("tp", None),
            P(),
            P(),
            P(),
            P(("sp", "tp"), None),
            P(("sp", "tp"), None),
            P(("sp", "tp"), None),
            P(),
            P("sp", None, "tp"),
            P("sp", None, "tp"),
            P("sp", "tp", None),
        ),
        out_specs=P(("sp", "tp"), None),
        check_vma=False,
    )
```

time: 169 us -> 156 us (0.923)
  blocking collectives: 18.1 us -> 48.6 us
  starting transfers between devices: 59.8 us -> 45.9 us
  waiting for transfers between devices: 46.3 us -> 34.1 us
  Pallas kernels: 28.9 us -> 22.1 us
  other arithmetic: 4.94 us -> 0.8 us
  matrix products: 4.93 us -> 1.21 us
  local copies, waits for them, and re-layouts: 5.05 us -> 2.57 us
    all_to_all x0 -> x2, blocking collectives: none -> 31.3 us  [the longest x1 17 us: per_device(): lax.all_to_all(conv_out, 'tp', split_axis=0, concat_axis=0, tiled=True)]
    all_to_all x2 -> x0, waiting for transfers between devices: 17.2 us -> none  [the longest x1 8.72 us: per_device(): lax.all_to_all(result, 'sp', split_axis=0, concat_axis=0, tiled=True)]
    all_to_all x2 -> x0, starting transfers between devices: 13.4 us -> none  [the longest x1 8.58 us: per_device(): lax.all_to_all(conv_out, 'tp', split_axis=1, concat_axis=0, tiled=True)]
    pallas_call x4 -> x8, Pallas kernels: 27.3 us -> 21.3 us  [the longest x4 17.3 us: expert(): pl.pallas_call(functools.partial(expert_kernel, sizes, hidden // 2, len(t...]
    ppermute x28, waiting for transfers between devices: 29.1 us -> 34.1 us  [z_shift(): lax.ppermute(value, 'tp', [(i, (i + 2 * steps) % count) for i in range(co...]
    dot_general x4 -> x2, matrix products: 4.93 us -> 1.21 us  [mix(): lax.dot_general(weight, rows, (((0,), (0,)), ((), ())), preferred_element...]
    convert_element_type x5 -> x1, other arithmetic: 3.96 us -> 0.8 us  [gated(): return (value * jax.nn.sigmoid(gate)).astype(bf16)]
    mul x2 -> x0, local copies, waits for them, and re-layouts: 2 us -> none  [per_device(): conv_taps[:, offset:offset + 1] * padded[:, offset:offset + run_len]]
  transfers between devices with their start and end apart: 34 -> 32, of which waited for: 12 -> 11; matrix products, arithmetic and copies ran while one was open for 7% -> 0% of each run, Pallas kernels for 13% -> 11%
where the time goes in v2:
time: 156 us
  blocking collectives  48.6 us (31%)
  starting transfers between devices  45.9 us (29%)
  waiting for transfers between devices  34.1 us (22%)
  Pallas kernels  22.1 us (14%)
  local copies, waits for them, and re-layouts  2.57 us (2%)
    ppermute x28, starting transfers between devices, z_shift(): lax.ppermute(value, 'tp', [(i, (i + 2 * steps) % count) for i in range(co...  40.8 us
    ppermute x28, waiting for transfers between devices, z_shift(): lax.ppermute(value, 'tp', [(i, (i + 2 * steps) % count) for i in range(co...  34.1 us
    pallas_call x4, Pallas kernels, expert(): pl.pallas_call(functools.partial(expert_kernel, sizes, hidden // 2, len(t...  17.3 us
    all_to_all x1, blocking collectives, per_device(): lax.all_to_all(send_rows, 'sp', split_axis=0, concat_axis=0, tiled=True)  17.3 us
    all_to_all x1, blocking collectives, per_device(): lax.all_to_all(conv_out, 'tp', split_axis=0, concat_axis=0, tiled=True)  17 us
    all_to_all x1, blocking collectives, per_device(): lax.all_to_all(result, 'sp', split_axis=0, concat_axis=0, tiled=True)  14.3 us
    ppermute x1, starting transfers between devices, shifted(): lax.ppermute(value, axis, [(source, source + steps) for source in range(i...  3.4 us
  transfers between devices with their start and end apart: 32, of which 11 were waited for; matrix products, arithmetic and copies ran while one was open for 0% of the time, Pallas kernels for 11%

profile of v2, /device:TPU:2, one launch (start us, length us, event | category | flops | bytes accessed | tf_op | source)
XLA Modules:
  0.0 155.6 jit_solution(14767008596118235262)
XLA Ops:
  0.0 0.8 multiply_convert_fusion
  0.8 3.4 %collective-permute-start = (bf16[64,128]{1,0:T(8,128)(2,1)S(1)}, bf16[64,128]{1,0:T(8,128)(2,1)S(1)}, u32[]{:S(2)}, u32[]{:S(2)}) collective-permute-start(bf16[64,128]{1,0:T(8,128)(2,1)S(1)} %multiply_convert_fusion), channel_id=1, source_target_pairs={{0,16},{16,32},{32,48},{48,64},{64,80},{80,96},{96,112},{112,128},... | collective-permute-start | bytes 49160 | tf_op jit(solution)/shard_map/ppermute | solution.py:20
  4.2 0.9 copy-done.3
  5.1 0.9 copy-done.4
  6.0 0.7 copy-done.5
  6.8 2.2 %shard_map.127._ = bf16[16,32,128]{2,1,0:T(8,128)(2,1)S(1)} custom-call(bf16[64,1024]{1,0:T(8,128)(2,1)S(1)} %copy-done.4, bf16[64,1024]{1,0:T(8,128)(2,1)S(1)} %copy-done.3, f32[31,64]{1,0:T(8,128)S(1)} %bitcast.43), custom_call_target="tpu_custom_call" | custom-call | flops 1342177280 | bytes 1048576 | tf_op jit(solution)/shard_map/pallas_call | solution.py:150
  9.3 17.0 %all_to_all.15.conv = bf16[16,32,128]{2,1,0:T(8,128)(2,1)S(1)} all-to-all(bf16[16,32,128]{2,1,0:T(8,128)(2,1)S(1)} %shard_map.128), channel_id=1, replica_groups=mesh['sp'=16,'tp'=16] {'tp'}, dimensions={0} | all-to-all | bytes 262144 | tf_op jit(solution)/shard_map/all_to_all | solution.py:347
  26.4 1.5 shard_map.129
  27.9 0.7 collective-permute-start.1
  29.0 0.6 collective-permute-start.3
  29.6 17.3 %all_to_all.16 = bf16[16,8,2048]{2,1,0:T(8,128)(2,1)S(1)} all-to-all(bf16[16,8,2048]{2,1,0:T(8,128)(2,1)S(1)} %bitcast.42), channel_id=1, replica_groups=mesh['sp'=16,'tp'=16] {'sp'}, dimensions={0} | all-to-all | bytes 1048576 | tf_op jit(solution)/shard_map/all_to_all | solution.py:362
  47.0 0.6 collective-permute-start.12
  47.6 2.7 %collective-permute-start.15 = (bf16[64,2048]{1,0:T(8,128)(2,1)S(1)}, bf16[64,2048]{1,0:T(8,128)(2,1)S(1)}, u32[]{:S(2)}, u32[]{:S(2)}) collective-permute-start(bf16[64,2048]{1,0:T(8,128)(2,1)S(1)} %get-tuple-element.46.refs_0_), channel_id=1, source_target_pairs={{0,14},{1,15},{2,0},{3,1},{4,2},{5,3},{6,4},{7,5},{8,6},{9,7},{10,... | collective-permute-start | bytes 786440 | tf_op jit(solution)/shard_map/ppermute | solution.py:25
  50.3 3.2 %collective-permute-start.8 = (bf16[64,2048]{1,0:T(8,128)(2,1)S(1)}, bf16[64,2048]{1,0:T(8,128)(2,1)S(1)}, u32[]{:S(2)}, u32[]{:S(2)}) collective-permute-start(bf16[64,2048]{1,0:T(8,128)(2,1)S(1)} %get-tuple-element.47.refs_1_), channel_id=1, source_target_pairs={{0,14},{1,15},{2,0},{3,1},{4,2},{5,3},{6,4},{7,5},{8,6},{9,7},{10,... | collective-permute-start | bytes 786440 | tf_op jit(solution)/shard_map/ppermute | solution.py:25
  53.5 3.9 %collective-permute-done.12.refs_3_ = bf16[64,2048]{1,0:T(8,128)(2,1)S(1)} collective-permute-done((bf16[64,2048]{1,0:T(8,128)(2,1)S(1)}, bf16[64,2048]{1,0:T(8,128)(2,1)S(1)}, u32[]{:S(2)}, u32[]{:S(2)}) %collective-permute-start.12) | collective-permute-done | bytes 262176 | tf_op jit(solution)/shard_map/ppermute | solution.py:25
  57.4 3.2 %collective-permute-start.16 = (bf16[64,2048]{1,0:T(8,128)(2,1)S(1)}, bf16[64,2048]{1,0:T(8,128)(2,1)S(1)}, u32[]{:S(2)}, u32[]{:S(2)}) collective-permute-start(bf16[64,2048]{1,0:T(8,128)(2,1)S(1)} %collective-permute-done.15.refs_4_), channel_id=1, source_target_pairs={{0,14},{1,15},{2,0},{3,1},{4,2},{5,3},{6,4},{7,5},{8,6},{9,7},{10,... | collective-permute-start | bytes 786440 | tf_op jit(solution)/shard_map/ppermute | solution.py:25
  60.7 2.4 %collective-permute-done.4.refs_2_ = bf16[64,2048]{1,0:T(8,128)(2,1)S(1)} collective-permute-done((bf16[64,2048]{1,0:T(8,128)(2,1)S(1)}, bf16[64,2048]{1,0:T(8,128)(2,1)S(1)}, u32[]{:S(2)}, u32[]{:S(2)}) %collective-permute-start.4) | collective-permute-done | bytes 262176 | tf_op jit(solution)/shard_map/ppermute | solution.py:25
  63.0 3.2 %collective-permute-start.9 = (bf16[64,2048]{1,0:T(8,128)(2,1)S(1)}, bf16[64,2048]{1,0:T(8,128)(2,1)S(1)}, u32[]{:S(2)}, u32[]{:S(2)}) collective-permute-start(bf16[64,2048]{1,0:T(8,128)(2,1)S(1)} %collective-permute-done.8.refs_5_), channel_id=1, source_target_pairs={{0,14},{1,15},{2,0},{3,1},{4,2},{5,3},{6,4},{7,5},{8,6},{9,7},{10,... | collective-permute-start | bytes 786440 | tf_op jit(solution)/shard_map/ppermute | solution.py:25
  66.3 5.8 %shard_map.131 = (bf16[64,2048]{1,0:T(8,128)(2,1)S(1)}, bf16[64,2048]{1,0:T(8,128)(2,1)S(1)}, bf16[64,2048]{1,0:T(8,128)(2,1)S(1)}, bf16[64,2048]{1,0:T(8,128)(2...) custom-call(bf16[64,2048]{1,0:T(8,128)(2,1)S(1)} %get-tuple-element.46.refs_0_, ...), custom_call_target="tpu_custom_call" | custom-call | flops 4227858432 | bytes 1048576 | tf_op jit(solution)/shard_map/pallas_call | solution.py:77
  72.1 2.8 %collective-permute-start.10 = (bf16[64,2048]{1,0:T(8,128)(2,1)S(1)}, bf16[64,2048]{1,0:T(8,128)(2,1)S(1)}, u32[]{:S(2)}, u32[]{:S(2)}) collective-permute-start(bf16[64,2048]{1,0:T(8,128)(2,1)S(1)} %collective-permute-done.9.refs_3_), channel_id=1, source_target_pairs={{0,14},{1,15},{2,0},{3,1},{4,2},{5,3},{6,4},{7,5},{8,6},{9,7},{10,... | collective-permute-start | bytes 786440 | tf_op jit(solution)/shard_map/ppermute | solution.py:25
  75.0 3.2 %collective-permute-start.17 = (bf16[64,2048]{1,0:T(8,128)(2,1)S(1)}, bf16[64,2048]{1,0:T(8,128)(2,1)S(1)}, u32[]{:S(2)}, u32[]{:S(2)}) collective-permute-start(bf16[64,2048]{1,0:T(8,128)(2,1)S(1)} %collective-permute-done.16.refs_2_), channel_id=1, source_target_pairs={{0,14},{1,15},{2,0},{3,1},{4,2},{5,3},{6,4},{7,5},{8,6},{9,7},{10,... | collective-permute-start | bytes 786440 | tf_op jit(solution)/shard_map/ppermute | solution.py:25
  78.2 4.1 %shard_map.132 = (bf16[64,2048]{1,0:T(8,128)(2,1)S(1)}, bf16[64,2048]{1,0:T(8,128)(2,1)S(1)}, bf16[64,2048]{1,0:T(8,128)(2,1)S(1)}, bf16[64,2048]{1,0:T(8,128)(2,1)S(1)}) custom-call(bf16[64,2048]{1,0:T(8,128)(2,1)S(1)} %collective-permute-done.5.refs_0_, bf16[64,2048]{1,0:T(8,128)(2,1)S(1)} %collective-permute-done.13.refs_1_, ...), custom_call_target="tpu_custom_call" | custom-call | flops 2818572288 | bytes 1048576 | tf_op jit(solution)/shard_map/pallas_call | solution.py:77
  82.3 2.3 %collective-permute-start.11 = (bf16[64,2048]{1,0:T(8,128)(2,1)S(1)}, bf16[64,2048]{1,0:T(8,128)(2,1)S(1)}, u32[]{:S(2)}, u32[]{:S(2)}) collective-permute-start(bf16[64,2048]{1,0:T(8,128)(2,1)S(1)} %collective-permute-done.10.refs_3_), channel_id=1, source_target_pairs={{0,14},{1,15},{2,0},{3,1},{4,2},{5,3},{6,4},{7,5},{8,6},{9,7},{10,... | collective-permute-start | bytes 786440 | tf_op jit(solution)/shard_map/ppermute | solution.py:25
  84.7 5.3 %collective-permute-done.14.refs_1_ = bf16[64,2048]{1,0:T(8,128)(2,1)S(1)} collective-permute-done((bf16[64,2048]{1,0:T(8,128)(2,1)S(1)}, bf16[64,2048]{1,0:T(8,128)(2,1)S(1)}, u32[]{:S(2)}, u32[]{:S(2)}) %collective-permute-start.14) | collective-permute-done | bytes 262176 | tf_op jit(solution)/shard_map/ppermute | solution.py:25
  89.9 4.1 %shard_map.133 = (bf16[64,2048]{1,0:T(8,128)(2,1)S(1)}, bf16[64,2048]{1,0:T(8,128)(2,1)S(1)}, bf16[64,2048]{1,0:T(8,128)(2,1)S(1)}, bf16[64,2048]{1,0:T(8,128)(2,1)S(1)}) custom-call(bf16[64,2048]{1,0:T(8,128)(2,1)S(1)} %collective-permute-done.6.refs_0_, bf16[64,2048]{1,0:T(8,128)(2,1)S(1)} %collective-permute-done.14.refs_1_, ...), custom_call_target="tpu_custom_call" | custom-call | flops 2818572288 | bytes 1048576 | tf_op jit(solution)/shard_map/pallas_call | solution.py:77
  94.1 3.3 %shard_map.134 = (bf16[64,2048]{1,0:T(8,128)(2,1)S(1)}, bf16[64,2048]{1,0:T(8,128)(2,1)S(1)}) custom-call(bf16[64,2048]{1,0:T(8,128)(2,1)S(1)} %collective-permute-done.7.refs_0_, bf16[64,2048]{1,0:T(8,128)(2,1)S(1)} %collective-permute-done.11.refs_1_, bf16[448,2048]{1,0:T(8,128)(2,1)S(1)} %bitcast.29, ...), custom_call_target="tpu_custom_call" | custom-call | flops 1409286144 | bytes 1048576 | tf_op jit(solution)/shard_map/pallas_call | solution.py:77
  97.4 0.6 collective-permute-start.28
  98.0 1.7 %collective-permute-start.18 = (bf16[64,2048]{1,0:T(8,128)(2,1)S(1)}, bf16[64,2048]{1,0:T(8,128)(2,1)S(1)}, u32[]{:S(2)}, u32[]{:S(2)}) collective-permute-start(bf16[64,2048]{1,0:T(8,128)(2,1)S(1)} %get-tuple-element.57), channel_id=1, source_target_pairs={{0,2},{1,3},{2,4},{3,5},{4,6},{5,7},{6,8},{7,9},{8,10},{9,11},{10,... | collective-permute-start | bytes 786440 | tf_op jit(solution)/shard_map/ppermute | solution.py:25
  99.8 3.2 %collective-permute-start.22 = (bf16[64,2048]{1,0:T(8,128)(2,1)S(1)}, bf16[64,2048]{1,0:T(8,128)(2,1)S(1)}, u32[]{:S(2)}, u32[]{:S(2)}) collective-permute-start(bf16[64,2048]{1,0:T(8,128)(2,1)S(1)} %get-tuple-element.56.refs_8_), channel_id=1, source_target_pairs={{0,14},{1,15},{2,0},{3,1},{4,2},{5,3},{6,4},{7,5},{8,6},{9,7},{10,... | collective-permute-start | bytes 786440 | tf_op jit(solution)/shard_map/ppermute | solution.py:25
  103.0 3.9 %collective-permute-done.28.a = bf16[64,2048]{1,0:T(8,128)(2,1)S(1)} collective-permute-done((bf16[64,2048]{1,0:T(8,128)(2,1)S(1)}, bf16[64,2048]{1,0:T(8,128)(2,1)S(1)}, u32[]{:S(2)}, u32[]{:S(2)}) %collective-permute-start.28) | collective-permute-done | bytes 262176 | tf_op jit(solution)/shard_map/ppermute | solution.py:25
  107.0 1.6 %collective-permute-start.29 = (bf16[64,2048]{1,0:T(8,128)(2,1)S(1)}, bf16[64,2048]{1,0:T(8,128)(2,1)S(1)}, u32[]{:S(2)}, u32[]{:S(2)}) collective-permute-start(bf16[64,2048]{1,0:T(8,128)(2,1)S(1)} %shard_map.142), channel_id=1, source_target_pairs={{0,14},{1,15},{2,0},{3,1},{4,2},{5,3},{6,4},{7,5},{8,6},{9,7},{10,... | collective-permute-start | bytes 786440 | tf_op jit(solution)/shard_map/ppermute | solution.py:25
  108.6 0.6 collective-permute-start.19
  109.2 4.1 %collective-permute-done.25.a = bf16[64,2048]{1,0:T(8,128)(2,1)S(1)} collective-permute-done((bf16[64,2048]{1,0:T(8,128)(2,1)S(1)}, bf16[64,2048]{1,0:T(8,128)(2,1)S(1)}, u32[]{:S(2)}, u32[]{:S(2)}) %collective-permute-start.25) | collective-permute-done | bytes 262176 | tf_op jit(solution)/shard_map/ppermute | solution.py:25
  113.4 1.3 collective-permute-start.26
  114.7 2.1 %collective-permute-start.23 = (bf16[64,2048]{1,0:T(8,128)(2,1)S(1)}, bf16[64,2048]{1,0:T(8,128)(2,1)S(1)}, u32[]{:S(2)}, u32[]{:S(2)}) collective-permute-start(bf16[64,2048]{1,0:T(8,128)(2,1)S(1)} %shard_map.138), channel_id=1, source_target_pairs={{0,14},{1,15},{2,0},{3,1},{4,2},{5,3},{6,4},{7,5},{8,6},{9,7},{10,... | collective-permute-start | bytes 786440 | tf_op jit(solution)/shard_map/ppermute | solution.py:25
  116.9 1.3 collective-permute-done.29.a
  118.2 1.6 %collective-permute-start.30 = (bf16[64,2048]{1,0:T(8,128)(2,1)S(1)}, bf16[64,2048]{1,0:T(8,128)(2,1)S(1)}, u32[]{:S(2)}, u32[]{:S(2)}) collective-permute-start(bf16[64,2048]{1,0:T(8,128)(2,1)S(1)} %shard_map.143), channel_id=1, source_target_pairs={{0,14},{1,15},{2,0},{3,1},{4,2},{5,3},{6,4},{7,5},{8,6},{9,7},{10,... | collective-permute-start | bytes 786440 | tf_op jit(solution)/shard_map/ppermute | solution.py:25
  119.8 0.6 collective-permute-start.20
  120.4 3.4 %collective-permute-done.26.a = bf16[64,2048]{1,0:T(8,128)(2,1)S(1)} collective-permute-done((bf16[64,2048]{1,0:T(8,128)(2,1)S(1)}, bf16[64,2048]{1,0:T(8,128)(2,1)S(1)}, u32[]{:S(2)}, u32[]{:S(2)}) %collective-permute-start.26) | collective-permute-done | bytes 262176 | tf_op jit(solution)/shard_map/ppermute | solution.py:25
  123.9 1.9 %collective-permute-start.27 = (bf16[64,2048]{1,0:T(8,128)(2,1)S(1)}, bf16[64,2048]{1,0:T(8,128)(2,1)S(1)}, u32[]{:S(2)}, u32[]{:S(2)}) collective-permute-start(bf16[64,2048]{1,0:T(8,128)(2,1)S(1)} %shard_map.141), channel_id=1, source_target_pairs={{0,2},{1,3},{2,4},{3,5},{4,6},{5,7},{6,8},{7,9},{8,10},{9,11},{10,... | collective-permute-start | bytes 786440 | tf_op jit(solution)/shard_map/ppermute | solution.py:25
  125.9 1.5 collective-permute-start.24
  127.4 2.2 %collective-permute-done.30.a = bf16[64,2048]{1,0:T(8,128)(2,1)S(1)} collective-permute-done((bf16[64,2048]{1,0:T(8,128)(2,1)S(1)}, bf16[64,2048]{1,0:T(8,128)(2,1)S(1)}, u32[]{:S(2)}, u32[]{:S(2)}) %collective-permute-start.30) | collective-permute-done | bytes 262176 | tf_op jit(solution)/shard_map/ppermute | solution.py:25
  129.7 2.5 %collective-permute-start.31 = (bf16[64,2048]{1,0:T(8,128)(2,1)S(1)}, bf16[64,2048]{1,0:T(8,128)(2,1)S(1)}, u32[]{:S(2)}, u32[]{:S(2)}) collective-permute-start(bf16[64,2048]{1,0:T(8,128)(2,1)S(1)} %shard_map.144), channel_id=1, source_target_pairs={{0,14},{1,15},{2,0},{3,1},{4,2},{5,3},{6,4},{7,5},{8,6},{9,7},{10,... | collective-permute-start | bytes 786440 | tf_op jit(solution)/shard_map/ppermute | solution.py:25
  132.4 1.6 %collective-permute-done.27.right_b = bf16[64,2048]{1,0:T(8,128)(2,1)S(1)} collective-permute-done((bf16[64,2048]{1,0:T(8,128)(2,1)S(1)}, bf16[64,2048]{1,0:T(8,128)(2,1)S(1)}, u32[]{:S(2)}, u32[]{:S(2)}) %collective-permute-start.27) | collective-permute-done | bytes 262176 | tf_op jit(solution)/shard_map/ppermute | solution.py:25
  134.0 2.1 %collective-permute-done.31.left_b = bf16[64,2048]{1,0:T(8,128)(2,1)S(1)} collective-permute-done((bf16[64,2048]{1,0:T(8,128)(2,1)S(1)}, bf16[64,2048]{1,0:T(8,128)(2,1)S(1)}, u32[]{:S(2)}, u32[]{:S(2)}) %collective-permute-start.31) | collective-permute-done | bytes 262176 | tf_op jit(solution)/shard_map/ppermute | solution.py:25
  136.1 3.8 %collective-permute-done.21.right_a = bf16[64,2048]{1,0:T(8,128)(2,1)S(1)} collective-permute-done((bf16[64,2048]{1,0:T(8,128)(2,1)S(1)}, bf16[64,2048]{1,0:T(8,128)(2,1)S(1)}, u32[]{:S(2)}, u32[]{:S(2)}) %collective-permute-start.21) | collective-permute-done | bytes 262176 | tf_op jit(solution)/shard_map/ppermute | solution.py:25
  140.1 14.3 %all_to_all.17 = bf16[16,8,2048]{2,1,0:T(8,128)(2,1)S(1)} all-to-all(bf16[16,8,2048]{2,1,0:T(8,128)(2,1)S(1)} %bitcast.41), channel_id=1, replica_groups=mesh['sp'=16,'tp'=16] {'sp'}, dimensions={0} | all-to-all | bytes 1048576 | tf_op jit(solution)/shard_map/all_to_all | solution.py:396
  154.7 1.0 add_convert_fusion
  (67 shorter events, 2.1 us)
Async XLA Ops:
  0.8 8.2 %collective-permute-start = (bf16[64,128]{1,0:T(8,128)(2,1)S(1)}, bf16[64,128]{1,0:T(8,128)(2,1)S(1)}, u32[]{:S(2)}, u32[]{:S(2)}) collective-permute-start(bf16[64,128]{1,0:T(8,128)(2,1)S(1)} %multiply_convert_fusion), channel_id=1, source_target_pairs={{0,16},{16,32},{32,48},{48,64},{64,80},{80,96},{96,112},{112,128},... | collective-permute-start | bytes 49160 | tf_op jit(solution)/shard_map/ppermute | solution.py:20
  4.2 0.9 copy-start.3
  5.1 0.9 copy-start.4
  6.0 0.7 copy-start.5
  6.7 19.5 %copy-start.6 = (bf16[1024,2048]{1,0:T(8,128)(2,1)S(1)}, bf16[1024,2048]{1,0:T(8,128)(2,1)}, u32[]{:S(2)}) copy-start(bf16[1024,2048]{1,0:T(8,128)(2,1)} %out_weight.1) | copy-start | bytes 12582916
  6.7 19.5 %copy-start.7 = (bf16[64,2048]{1,0:T(8,128)(2,1)S(1)}, bf16[64,2048]{1,0:T(8,128)(2,1)}, u32[]{:S(2)}) copy-start(bf16[64,2048]{1,0:T(8,128)(2,1)} %stream.1) | copy-start | bytes 786436
  6.7 19.5 %copy-start.8 = (f32[2048]{0:T(1024)S(1)}, f32[2048]{0:T(1024)}, u32[]{:S(2)}) copy-start(f32[2048]{0:T(1024)} %param.22) | copy-start | bytes 24580
  6.7 19.5 %copy-start.9 = (f32[1024]{0:T(1024)S(1)}, f32[1024]{0:T(1024)}, u32[]{:S(2)}) copy-start(f32[1024]{0:T(1024)} %param.16) | copy-start | bytes 12292
  6.8 19.5 %copy-start.10 = (f32[1024]{0:T(1024)S(1)}, f32[1024]{0:T(1024)}, u32[]{:S(2)}) copy-start(f32[1024]{0:T(1024)} %param.17) | copy-start | bytes 12292
  6.8 19.5 %copy-start.11 = (s32[64,2]{0,1:T(2,128)S(1)}, s32[64,2]{0,1:T(2,128)}, u32[]{:S(2)}) copy-start(s32[64,2]{0,1:T(2,128)} %param.20) | copy-start | bytes 1540
  6.8 19.5 %copy-start.12 = (f32[64,2]{0,1:T(2,128)S(1)}, f32[64,2]{0,1:T(2,128)}, u32[]{:S(2)}) copy-start(f32[64,2]{0,1:T(2,128)} %param.21) | copy-start | bytes 1540
  26.3 1.5 copy-start
  26.3 2.3 %copy-start.1 = (bf16[1,2048,448]{1,2,0:T(8,128)(2,1)S(1)}, bf16[1,2048,448]{1,2,0:T(8,128)(2,1)}, u32[]{:S(2)}) copy-start(bf16[1,2048,448]{1,2,0:T(8,128)(2,1)} %param.24) | copy-start | bytes 5505028
  26.4 2.7 %copy-start.2 = (bf16[1,448,2048]{2,1,0:T(8,128)(2,1)S(1)}, bf16[1,448,2048]{2,1,0:T(8,128)(2,1)}, u32[]{:S(2)}) copy-start(bf16[1,448,2048]{2,1,0:T(8,128)(2,1)} %param.25) | copy-start | bytes 5505028
  27.9 19.0 %collective-permute-start.1 = (bf16[448,2048]{1,0:T(8,128)(2,1)S(1)}, bf16[448,2048]{1,0:T(8,128)(2,1)S(1)}, u32[]{:S(2)}, u32[]{:S(2)}) collective-permute-start(bf16[448,2048]{1,0:T(8,128)(2,1)S(1)} %bitcast.25), channel_id=1, source_target_pairs={{0,1},{1,0},{2,3},{3,2},{4,5},{5,4},{6,7},{7,6},{8,9},{9,8},{10,11... | collective-permute-start | bytes 5505032 | tf_op jit(solution)/shard_map/ppermute | solution.py:30
  28.6 18.3 %collective-permute-start.2 = (bf16[448,2048]{1,0:T(8,128)(2,1)S(1)}, bf16[448,2048]{1,0:T(8,128)(2,1)S(1)}, u32[]{:S(2)}, u32[]{:S(2)}) collective-permute-start(bf16[448,2048]{1,0:T(8,128)(2,1)S(1)} %bitcast.30), channel_id=1, source_target_pairs={{0,1},{1,0},{2,3},{3,2},{4,5},{5,4},{6,7},{7,6},{8,9},{9,8},{10,11... | collective-permute-start | bytes 5505032 | tf_op jit(solution)/shard_map/ppermute | solution.py:30
  29.0 17.9 %collective-permute-start.3 = (bf16[448,2048]{1,0:T(8,128)(2,1)S(1)}, bf16[448,2048]{1,0:T(8,128)(2,1)S(1)}, u32[]{:S(2)}, u32[]{:S(2)}) collective-permute-start(bf16[448,2048]{1,0:T(8,128)(2,1)S(1)} %bitcast.35), channel_id=1, source_target_pairs={{0,1},{1,0},{2,3},{3,2},{4,5},{5,4},{6,7},{7,6},{8,9},{9,8},{10,11... | collective-permute-start | bytes 5505032 | tf_op jit(solution)/shard_map/ppermute | solution.py:30
  47.0 10.5 %collective-permute-start.12 = (bf16[64,2048]{1,0:T(8,128)(2,1)S(1)}, bf16[64,2048]{1,0:T(8,128)(2,1)S(1)}, u32[]{:S(2)}, u32[]{:S(2)}) collective-permute-start(bf16[64,2048]{1,0:T(8,128)(2,1)S(1)} %get-tuple-element.47.refs_1_), channel_id=1, source_target_pairs={{0,2},{1,3},{2,4},{3,5},{4,6},{5,7},{6,8},{7,9},{8,10},{9,11},{10,... | collective-permute-start | bytes 786440 | tf_op jit(solution)/shard_map/ppermute | solution.py:25
  47.6 9.8 %collective-permute-start.15 = (bf16[64,2048]{1,0:T(8,128)(2,1)S(1)}, bf16[64,2048]{1,0:T(8,128)(2,1)S(1)}, u32[]{:S(2)}, u32[]{:S(2)}) collective-permute-start(bf16[64,2048]{1,0:T(8,128)(2,1)S(1)} %get-tuple-element.46.refs_0_), channel_id=1, source_target_pairs={{0,14},{1,15},{2,0},{3,1},{4,2},{5,3},{6,4},{7,5},{8,6},{9,7},{10,... | collective-permute-start | bytes 786440 | tf_op jit(solution)/shard_map/ppermute | solution.py:25
  50.3 12.8 %collective-permute-start.4 = (bf16[64,2048]{1,0:T(8,128)(2,1)S(1)}, bf16[64,2048]{1,0:T(8,128)(2,1)S(1)}, u32[]{:S(2)}, u32[]{:S(2)}) collective-permute-start(bf16[64,2048]{1,0:T(8,128)(2,1)S(1)} %get-tuple-element.46.refs_0_), channel_id=1, source_target_pairs={{0,2},{1,3},{2,4},{3,5},{4,6},{5,7},{6,8},{7,9},{8,10},{9,11},{10,... | collective-permute-start | bytes 786440 | tf_op jit(solution)/shard_map/ppermute | solution.py:25
  50.3 12.8 %collective-permute-start.8 = (bf16[64,2048]{1,0:T(8,128)(2,1)S(1)}, bf16[64,2048]{1,0:T(8,128)(2,1)S(1)}, u32[]{:S(2)}, u32[]{:S(2)}) collective-permute-start(bf16[64,2048]{1,0:T(8,128)(2,1)S(1)} %get-tuple-element.47.refs_1_), channel_id=1, source_target_pairs={{0,14},{1,15},{2,0},{3,1},{4,2},{5,3},{6,4},{7,5},{8,6},{9,7},{10,... | collective-permute-start | bytes 786440 | tf_op jit(solution)/shard_map/ppermute | solution.py:25
  57.4 17.5 %collective-permute-start.13 = (bf16[64,2048]{1,0:T(8,128)(2,1)S(1)}, bf16[64,2048]{1,0:T(8,128)(2,1)S(1)}, u32[]{:S(2)}, u32[]{:S(2)}) collective-permute-start(bf16[64,2048]{1,0:T(8,128)(2,1)S(1)} %collective-permute-done.12.refs_3_), channel_id=1, source_target_pairs={{0,2},{1,3},{2,4},{3,5},{4,6},{5,7},{6,8},{7,9},{8,10},{9,11},{10,... | collective-permute-start | bytes 786440 | tf_op jit(solution)/shard_map/ppermute | solution.py:25
  57.4 17.6 %collective-permute-start.16 = (bf16[64,2048]{1,0:T(8,128)(2,1)S(1)}, bf16[64,2048]{1,0:T(8,128)(2,1)S(1)}, u32[]{:S(2)}, u32[]{:S(2)}) collective-permute-start(bf16[64,2048]{1,0:T(8,128)(2,1)S(1)} %collective-permute-done.15.refs_4_), channel_id=1, source_target_pairs={{0,14},{1,15},{2,0},{3,1},{4,2},{5,3},{6,4},{7,5},{8,6},{9,7},{10,... | collective-permute-start | bytes 786440 | tf_op jit(solution)/shard_map/ppermute | solution.py:25
  63.0 11.8 %collective-permute-start.5 = (bf16[64,2048]{1,0:T(8,128)(2,1)S(1)}, bf16[64,2048]{1,0:T(8,128)(2,1)S(1)}, u32[]{:S(2)}, u32[]{:S(2)}) collective-permute-start(bf16[64,2048]{1,0:T(8,128)(2,1)S(1)} %collective-permute-done.4.refs_2_), channel_id=1, source_target_pairs={{0,2},{1,3},{2,4},{3,5},{4,6},{5,7},{6,8},{7,9},{8,10},{9,11},{10,... | collective-permute-start | bytes 786440 | tf_op jit(solution)/shard_map/ppermute | solution.py:25
  63.0 9.0 %collective-permute-start.9 = (bf16[64,2048]{1,0:T(8,128)(2,1)S(1)}, bf16[64,2048]{1,0:T(8,128)(2,1)S(1)}, u32[]{:S(2)}, u32[]{:S(2)}) collective-permute-start(bf16[64,2048]{1,0:T(8,128)(2,1)S(1)} %collective-permute-done.8.refs_5_), channel_id=1, source_target_pairs={{0,14},{1,15},{2,0},{3,1},{4,2},{5,3},{6,4},{7,5},{8,6},{9,7},{10,... | collective-permute-start | bytes 786440 | tf_op jit(solution)/shard_map/ppermute | solution.py:25
  72.1 10.2 %collective-permute-start.10 = (bf16[64,2048]{1,0:T(8,128)(2,1)S(1)}, bf16[64,2048]{1,0:T(8,128)(2,1)S(1)}, u32[]{:S(2)}, u32[]{:S(2)}) collective-permute-start(bf16[64,2048]{1,0:T(8,128)(2,1)S(1)} %collective-permute-done.9.refs_3_), channel_id=1, source_target_pairs={{0,14},{1,15},{2,0},{3,1},{4,2},{5,3},{6,4},{7,5},{8,6},{9,7},{10,... | collective-permute-start | bytes 786440 | tf_op jit(solution)/shard_map/ppermute | solution.py:25
  74.9 9.8 %collective-permute-start.6 = (bf16[64,2048]{1,0:T(8,128)(2,1)S(1)}, bf16[64,2048]{1,0:T(8,128)(2,1)S(1)}, u32[]{:S(2)}, u32[]{:S(2)}) collective-permute-start(bf16[64,2048]{1,0:T(8,128)(2,1)S(1)} %collective-permute-done.5.refs_0_), channel_id=1, source_target_pairs={{0,2},{1,3},{2,4},{3,5},{4,6},{5,7},{6,8},{7,9},{8,10},{9,11},{10,... | collective-permute-start | bytes 786440 | tf_op jit(solution)/shard_map/ppermute | solution.py:25
  74.9 15.0 %collective-permute-start.14 = (bf16[64,2048]{1,0:T(8,128)(2,1)S(1)}, bf16[64,2048]{1,0:T(8,128)(2,1)S(1)}, u32[]{:S(2)}, u32[]{:S(2)}) collective-permute-start(bf16[64,2048]{1,0:T(8,128)(2,1)S(1)} %collective-permute-done.13.refs_1_), channel_id=1, source_target_pairs={{0,2},{1,3},{2,4},{3,5},{4,6},{5,7},{6,8},{7,9},{8,10},{9,11},{10,... | collective-permute-start | bytes 786440 | tf_op jit(solution)/shard_map/ppermute | solution.py:25
  75.0 14.9 %collective-permute-start.17 = (bf16[64,2048]{1,0:T(8,128)(2,1)S(1)}, bf16[64,2048]{1,0:T(8,128)(2,1)S(1)}, u32[]{:S(2)}, u32[]{:S(2)}) collective-permute-start(bf16[64,2048]{1,0:T(8,128)(2,1)S(1)} %collective-permute-done.16.refs_2_), channel_id=1, source_target_pairs={{0,14},{1,15},{2,0},{3,1},{4,2},{5,3},{6,4},{7,5},{8,6},{9,7},{10,... | collective-permute-start | bytes 786440 | tf_op jit(solution)/shard_map/ppermute | solution.py:25
  82.3 11.7 %collective-permute-start.11 = (bf16[64,2048]{1,0:T(8,128)(2,1)S(1)}, bf16[64,2048]{1,0:T(8,128)(2,1)S(1)}, u32[]{:S(2)}, u32[]{:S(2)}) collective-permute-start(bf16[64,2048]{1,0:T(8,128)(2,1)S(1)} %collective-permute-done.10.refs_3_), channel_id=1, source_target_pairs={{0,14},{1,15},{2,0},{3,1},{4,2},{5,3},{6,4},{7,5},{8,6},{9,7},{10,... | collective-permute-start | bytes 786440 | tf_op jit(solution)/shard_map/ppermute | solution.py:25
  84.7 9.4 %collective-permute-start.7 = (bf16[64,2048]{1,0:T(8,128)(2,1)S(1)}, bf16[64,2048]{1,0:T(8,128)(2,1)S(1)}, u32[]{:S(2)}, u32[]{:S(2)}) collective-permute-start(bf16[64,2048]{1,0:T(8,128)(2,1)S(1)} %collective-permute-done.6.refs_0_), channel_id=1, source_target_pairs={{0,2},{1,3},{2,4},{3,5},{4,6},{5,7},{6,8},{7,9},{8,10},{9,11},{10,... | collective-permute-start | bytes 786440 | tf_op jit(solution)/shard_map/ppermute | solution.py:25
  97.4 9.5 %collective-permute-start.28 = (bf16[64,2048]{1,0:T(8,128)(2,1)S(1)}, bf16[64,2048]{1,0:T(8,128)(2,1)S(1)}, u32[]{:S(2)}, u32[]{:S(2)}) collective-permute-start(bf16[64,2048]{1,0:T(8,128)(2,1)S(1)} %get-tuple-element.65), channel_id=1, source_target_pairs={{0,14},{1,15},{2,0},{3,1},{4,2},{5,3},{6,4},{7,5},{8,6},{9,7},{10,... | collective-permute-start | bytes 786440 | tf_op jit(solution)/shard_map/ppermute | solution.py:25
  98.0 10.5 %collective-permute-start.18 = (bf16[64,2048]{1,0:T(8,128)(2,1)S(1)}, bf16[64,2048]{1,0:T(8,128)(2,1)S(1)}, u32[]{:S(2)}, u32[]{:S(2)}) collective-permute-start(bf16[64,2048]{1,0:T(8,128)(2,1)S(1)} %get-tuple-element.57), channel_id=1, source_target_pairs={{0,2},{1,3},{2,4},{3,5},{4,6},{5,7},{6,8},{7,9},{8,10},{9,11},{10,... | collective-permute-start | bytes 786440 | tf_op jit(solution)/shard_map/ppermute | solution.py:25
  99.7 13.6 %collective-permute-start.25 = (bf16[64,2048]{1,0:T(8,128)(2,1)S(1)}, bf16[64,2048]{1,0:T(8,128)(2,1)S(1)}, u32[]{:S(2)}, u32[]{:S(2)}) collective-permute-start(bf16[64,2048]{1,0:T(8,128)(2,1)S(1)} %get-tuple-element.62), channel_id=1, source_target_pairs={{0,2},{1,3},{2,4},{3,5},{4,6},{5,7},{6,8},{7,9},{8,10},{9,11},{10,... | collective-permute-start | bytes 786440 | tf_op jit(solution)/shard_map/ppermute | solution.py:25
  99.8 14.9 %collective-permute-start.22 = (bf16[64,2048]{1,0:T(8,128)(2,1)S(1)}, bf16[64,2048]{1,0:T(8,128)(2,1)S(1)}, u32[]{:S(2)}, u32[]{:S(2)}) collective-permute-start(bf16[64,2048]{1,0:T(8,128)(2,1)S(1)} %get-tuple-element.56.refs_8_), channel_id=1, source_target_pairs={{0,14},{1,15},{2,0},{3,1},{4,2},{5,3},{6,4},{7,5},{8,6},{9,7},{10,... | collective-permute-start | bytes 786440 | tf_op jit(solution)/shard_map/ppermute | solution.py:25
  107.0 11.2 %collective-permute-start.29 = (bf16[64,2048]{1,0:T(8,128)(2,1)S(1)}, bf16[64,2048]{1,0:T(8,128)(2,1)S(1)}, u32[]{:S(2)}, u32[]{:S(2)}) collective-permute-start(bf16[64,2048]{1,0:T(8,128)(2,1)S(1)} %shard_map.142), channel_id=1, source_target_pairs={{0,14},{1,15},{2,0},{3,1},{4,2},{5,3},{6,4},{7,5},{8,6},{9,7},{10,... | collective-permute-start | bytes 786440 | tf_op jit(solution)/shard_map/ppermute | solution.py:25
  108.6 11.2 %collective-permute-start.19 = (bf16[64,2048]{1,0:T(8,128)(2,1)S(1)}, bf16[64,2048]{1,0:T(8,128)(2,1)S(1)}, u32[]{:S(2)}, u32[]{:S(2)}) collective-permute-start(bf16[64,2048]{1,0:T(8,128)(2,1)S(1)} %shard_map.135), channel_id=1, source_target_pairs={{0,2},{1,3},{2,4},{3,5},{4,6},{5,7},{6,8},{7,9},{8,10},{9,11},{10,... | collective-permute-start | bytes 786440 | tf_op jit(solution)/shard_map/ppermute | solution.py:25
  113.4 10.5 %collective-permute-start.26 = (bf16[64,2048]{1,0:T(8,128)(2,1)S(1)}, bf16[64,2048]{1,0:T(8,128)(2,1)S(1)}, u32[]{:S(2)}, u32[]{:S(2)}) collective-permute-start(bf16[64,2048]{1,0:T(8,128)(2,1)S(1)} %shard_map.140), channel_id=1, source_target_pairs={{0,2},{1,3},{2,4},{3,5},{4,6},{5,7},{6,8},{7,9},{8,10},{9,11},{10,... | collective-permute-start | bytes 786440 | tf_op jit(solution)/shard_map/ppermute | solution.py:25
  114.7 11.1 %collective-permute-start.23 = (bf16[64,2048]{1,0:T(8,128)(2,1)S(1)}, bf16[64,2048]{1,0:T(8,128)(2,1)S(1)}, u32[]{:S(2)}, u32[]{:S(2)}) collective-permute-start(bf16[64,2048]{1,0:T(8,128)(2,1)S(1)} %shard_map.138), channel_id=1, source_target_pairs={{0,14},{1,15},{2,0},{3,1},{4,2},{5,3},{6,4},{7,5},{8,6},{9,7},{10,... | collective-permute-start | bytes 786440 | tf_op jit(solution)/shard_map/ppermute | solution.py:25
  118.2 11.4 %collective-permute-start.30 = (bf16[64,2048]{1,0:T(8,128)(2,1)S(1)}, bf16[64,2048]{1,0:T(8,128)(2,1)S(1)}, u32[]{:S(2)}, u32[]{:S(2)}) collective-permute-start(bf16[64,2048]{1,0:T(8,128)(2,1)S(1)} %shard_map.143), channel_id=1, source_target_pairs={{0,14},{1,15},{2,0},{3,1},{4,2},{5,3},{6,4},{7,5},{8,6},{9,7},{10,... | collective-permute-start | bytes 786440 | tf_op jit(solution)/shard_map/ppermute | solution.py:25
  119.8 12.4 %collective-permute-start.20 = (bf16[64,2048]{1,0:T(8,128)(2,1)S(1)}, bf16[64,2048]{1,0:T(8,128)(2,1)S(1)}, u32[]{:S(2)}, u32[]{:S(2)}) collective-permute-start(bf16[64,2048]{1,0:T(8,128)(2,1)S(1)} %shard_map.136), channel_id=1, source_target_pairs={{0,2},{1,3},{2,4},{3,5},{4,6},{5,7},{6,8},{7,9},{8,10},{9,11},{10,... | collective-permute-start | bytes 786440 | tf_op jit(solution)/shard_map/ppermute | solution.py:25
  123.9 10.1 %collective-permute-start.27 = (bf16[64,2048]{1,0:T(8,128)(2,1)S(1)}, bf16[64,2048]{1,0:T(8,128)(2,1)S(1)}, u32[]{:S(2)}, u32[]{:S(2)}) collective-permute-start(bf16[64,2048]{1,0:T(8,128)(2,1)S(1)} %shard_map.141), channel_id=1, source_target_pairs={{0,2},{1,3},{2,4},{3,5},{4,6},{5,7},{6,8},{7,9},{8,10},{9,11},{10,... | collective-permute-start | bytes 786440 | tf_op jit(solution)/shard_map/ppermute | solution.py:25
  125.9 8.1 %collective-permute-start.24 = (bf16[64,2048]{1,0:T(8,128)(2,1)S(1)}, bf16[64,2048]{1,0:T(8,128)(2,1)S(1)}, u32[]{:S(2)}, u32[]{:S(2)}) collective-permute-start(bf16[64,2048]{1,0:T(8,128)(2,1)S(1)} %shard_map.139), channel_id=1, source_target_pairs={{0,14},{1,15},{2,0},{3,1},{4,2},{5,3},{6,4},{7,5},{8,6},{9,7},{10,... | collective-permute-start | bytes 786440 | tf_op jit(solution)/shard_map/ppermute | solution.py:25
  129.7 6.5 %collective-permute-start.31 = (bf16[64,2048]{1,0:T(8,128)(2,1)S(1)}, bf16[64,2048]{1,0:T(8,128)(2,1)S(1)}, u32[]{:S(2)}, u32[]{:S(2)}) collective-permute-start(bf16[64,2048]{1,0:T(8,128)(2,1)S(1)} %shard_map.144), channel_id=1, source_target_pairs={{0,14},{1,15},{2,0},{3,1},{4,2},{5,3},{6,4},{7,5},{8,6},{9,7},{10,... | collective-permute-start | bytes 786440 | tf_op jit(solution)/shard_map/ppermute | solution.py:25
  132.3 7.7 %collective-permute-start.21 = (bf16[64,2048]{1,0:T(8,128)(2,1)S(1)}, bf16[64,2048]{1,0:T(8,128)(2,1)S(1)}, u32[]{:S(2)}, u32[]{:S(2)}) collective-permute-start(bf16[64,2048]{1,0:T(8,128)(2,1)S(1)} %shard_map.137), channel_id=1, source_target_pairs={{0,2},{1,3},{2,4},{3,5},{4,6},{5,7},{6,8},{7,9},{8,10},{9,11},{10,... | collective-permute-start | bytes 786440 | tf_op jit(solution)/shard_map/ppermute | solution.py:25

commit v3 on v2

--- a/solution.py
+++ b/solution.py
@@ -369,13 +369,16 @@
     for k in range(1, far + 1):
         left_a, left_b = from_left[k - 1]
         right_a, right_b = from_right[k - 1]
-        from_left[k] = (z_shift(left_a, 1), z_shift(left_b, 1) if k < far else None)
-        from_right[k] = (z_shift(right_a, -1) if k < far else None, z_shift(right_b, -1))
-
-    first = expert((*from_left[0], *from_left[1], *from_right[1]), weights)
-    part_own = first[0:2]
-    part_left, part_right = {1: first[2:4]}, {1: first[4:6]}
-    token = first[0]
+        left_a = z_shift(left_a, 1)
+        right_b = z_shift(right_b, -1)
+        left_b = z_shift(left_b, 1) if k < far else None
+        right_a = z_shift(right_a, -1) if k < far else None
+        from_left[k] = (left_a, left_b)
+        from_right[k] = (right_a, right_b)
+
+    part_own = expert(from_left[0], weights)
+    part_left, part_right = {}, {}
+    token = part_own[0]
     for k in range(2, far):
         parts = expert((*from_left[k], *from_right[k]), weights, token)
         part_left[k], part_right[k] = parts[0:2], parts[2:4]
@@ -384,7 +387,10 @@
     left_a = z_shift(part_left[far - 1][0], -1)
     antipode = expert((from_left[far][0], from_right[far][1]), weights, token)
 
-    right_a, left_b = z_shift(antipode[0], 1), z_shift(antipode[1], -1)
+    right_a = z_shift(antipode[0], 1)
+    left_b = z_shift(antipode[1], -1)
+    parts = expert((*from_left[1], *from_right[1]), weights, antipode[0])
+    part_left[1], part_right[1] = parts[0:2], parts[2:4]
     for k in range(far - 1, 0, -1):
         if k < far - 1:
             right_b = z_shift(add(right_b, part_right[k][1]), 1)

time: 156 us -> 151 us (0.968)
  starting transfers between devices: 45.9 us -> 41.8 us
  waiting for transfers between devices: 34.1 us -> 32 us
  Pallas kernels: 22.1 us -> 23.8 us
    ppermute x28, starting transfers between devices: 40.8 us -> 36.7 us  [z_shift(): lax.ppermute(value, 'tp', [(i, (i + 2 * steps) % count) for i in range(co...]
    ppermute x28, waiting for transfers between devices: 34.1 us -> 32 us  [z_shift(): lax.ppermute(value, 'tp', [(i, (i + 2 * steps) % count) for i in range(co...]
    pallas_call x4 -> x5, Pallas kernels: 17.3 us -> 19 us  [expert(): pl.pallas_call(functools.partial(expert_kernel, sizes, hidden // 2, len(t...]
  transfers between devices with their start and end apart: 32 -> 32, of which waited for: 11 -> 13; matrix products, arithmetic and copies ran while one was open for 0% -> 0% of each run, Pallas kernels for 11% -> 12%
where the time goes in v3:
time: 151 us
  blocking collectives  48.4 us (32%)
  starting transfers between devices  41.8 us (28%)
  waiting for transfers between devices  32 us (21%)
  Pallas kernels  23.8 us (16%)
  local copies, waits for them, and re-layouts  2.57 us (2%)
    ppermute x28, starting transfers between devices, z_shift(): lax.ppermute(value, 'tp', [(i, (i + 2 * steps) % count) for i in range(co...  36.7 us
    ppermute x28, waiting for transfers between devices, z_shift(): lax.ppermute(value, 'tp', [(i, (i + 2 * steps) % count) for i in range(co...  32 us
    pallas_call x5, Pallas kernels, expert(): pl.pallas_call(functools.partial(expert_kernel, sizes, hidden // 2, len(t...  19 us
    all_to_all x1, blocking collectives, per_device(): lax.all_to_all(send_rows, 'sp', split_axis=0, concat_axis=0, tiled=True)  17.3 us
    all_to_all x1, blocking collectives, per_device(): lax.all_to_all(conv_out, 'tp', split_axis=0, concat_axis=0, tiled=True)  17 us
    all_to_all x1, blocking collectives, per_device(): lax.all_to_all(result, 'sp', split_axis=0, concat_axis=0, tiled=True)  14.1 us
    ppermute x1, starting transfers between devices, shifted(): lax.ppermute(value, axis, [(source, source + steps) for source in range(i...  3.4 us
  transfers between devices with their start and end apart: 32, of which 13 were waited for; matrix products, arithmetic and copies ran while one was open for 0% of the time, Pallas kernels for 12%

profile of v3, /device:TPU:2, one launch (start us, length us, event | category | flops | bytes accessed | tf_op | source)
XLA Modules:
  0.0 150.9 jit_solution(18355091094903011942)
XLA Ops:
  0.0 0.8 multiply_convert_fusion
  0.8 3.4 %collective-permute-start = (bf16[64,128]{1,0:T(8,128)(2,1)S(1)}, bf16[64,128]{1,0:T(8,128)(2,1)S(1)}, u32[]{:S(2)}, u32[]{:S(2)}) collective-permute-start(bf16[64,128]{1,0:T(8,128)(2,1)S(1)} %multiply_convert_fusion), channel_id=1, source_target_pairs={{0,16},{16,32},{32,48},{48,64},{64,80},{80,96},{96,112},{112,128},... | collective-permute-start | bytes 49160 | tf_op jit(solution)/shard_map/ppermute | solution.py:20
  4.2 0.9 copy-done.3
  5.1 0.9 copy-done.4
  6.0 0.7 copy-done.5
  6.8 2.2 %shard_map.127._ = bf16[16,32,128]{2,1,0:T(8,128)(2,1)S(1)} custom-call(bf16[64,1024]{1,0:T(8,128)(2,1)S(1)} %copy-done.4, bf16[64,1024]{1,0:T(8,128)(2,1)S(1)} %copy-done.3, f32[31,64]{1,0:T(8,128)S(1)} %bitcast.46), custom_call_target="tpu_custom_call" | custom-call | flops 1342177280 | bytes 1048576 | tf_op jit(solution)/shard_map/pallas_call | solution.py:150
  9.3 17.0 %all_to_all.15.conv = bf16[16,32,128]{2,1,0:T(8,128)(2,1)S(1)} all-to-all(bf16[16,32,128]{2,1,0:T(8,128)(2,1)S(1)} %shard_map.128), channel_id=1, replica_groups=mesh['sp'=16,'tp'=16] {'tp'}, dimensions={0} | all-to-all | bytes 262144 | tf_op jit(solution)/shard_map/all_to_all | solution.py:347
  26.4 1.5 shard_map.129
  27.9 0.7 collective-permute-start.1
  29.0 0.6 collective-permute-start.3
  29.6 17.3 %all_to_all.16 = bf16[16,8,2048]{2,1,0:T(8,128)(2,1)S(1)} all-to-all(bf16[16,8,2048]{2,1,0:T(8,128)(2,1)S(1)} %bitcast.45), channel_id=1, replica_groups=mesh['sp'=16,'tp'=16] {'sp'}, dimensions={0} | all-to-all | bytes 1048576 | tf_op jit(solution)/shard_map/all_to_all | solution.py:362
  47.4 1.7 %collective-permute-start.4 = (bf16[64,2048]{1,0:T(8,128)(2,1)S(1)}, bf16[64,2048]{1,0:T(8,128)(2,1)S(1)}, u32[]{:S(2)}, u32[]{:S(2)}) collective-permute-start(bf16[64,2048]{1,0:T(8,128)(2,1)S(1)} %get-tuple-element.46.refs_0_), channel_id=1, source_target_pairs={{0,2},{1,3},{2,4},{3,5},{4,6},{5,7},{6,8},{7,9},{8,10},{9,11},{10,... | collective-permute-start | bytes 786440 | tf_op jit(solution)/shard_map/ppermute | solution.py:25
  49.6 2.7 %collective-permute-start.15 = (bf16[64,2048]{1,0:T(8,128)(2,1)S(1)}, bf16[64,2048]{1,0:T(8,128)(2,1)S(1)}, u32[]{:S(2)}, u32[]{:S(2)}) collective-permute-start(bf16[64,2048]{1,0:T(8,128)(2,1)S(1)} %get-tuple-element.46.refs_0_), channel_id=1, source_target_pairs={{0,14},{1,15},{2,0},{3,1},{4,2},{5,3},{6,4},{7,5},{8,6},{9,7},{10,... | collective-permute-start | bytes 786440 | tf_op jit(solution)/shard_map/ppermute | solution.py:25
  52.3 3.9 %collective-permute-done.8.refs_3_ = bf16[64,2048]{1,0:T(8,128)(2,1)S(1)} collective-permute-done((bf16[64,2048]{1,0:T(8,128)(2,1)S(1)}, bf16[64,2048]{1,0:T(8,128)(2,1)S(1)}, u32[]{:S(2)}, u32[]{:S(2)}) %collective-permute-start.8) | collective-permute-done | bytes 262176 | tf_op jit(solution)/shard_map/ppermute | solution.py:25
  56.2 0.7 collective-permute-start.9
  56.9 0.8 collective-permute-done.4.refs_0_
  58.2 5.1 %collective-permute-done.12.refs_1_ = bf16[64,2048]{1,0:T(8,128)(2,1)S(1)} collective-permute-done((bf16[64,2048]{1,0:T(8,128)(2,1)S(1)}, bf16[64,2048]{1,0:T(8,128)(2,1)S(1)}, u32[]{:S(2)}, u32[]{:S(2)}) %collective-permute-start.12) | collective-permute-done | bytes 262176 | tf_op jit(solution)/shard_map/ppermute | solution.py:25
  63.9 2.8 %collective-permute-start.16 = (bf16[64,2048]{1,0:T(8,128)(2,1)S(1)}, bf16[64,2048]{1,0:T(8,128)(2,1)S(1)}, u32[]{:S(2)}, u32[]{:S(2)}) collective-permute-start(bf16[64,2048]{1,0:T(8,128)(2,1)S(1)} %collective-permute-done.15.refs_2_), channel_id=1, source_target_pairs={{0,14},{1,15},{2,0},{3,1},{4,2},{5,3},{6,4},{7,5},{8,6},{9,7},{10,... | collective-permute-start | bytes 786440 | tf_op jit(solution)/shard_map/ppermute | solution.py:25
  66.6 3.3 %shard_map.131 = (bf16[64,2048]{1,0:T(8,128)(2,1)S(1)}, bf16[64,2048]{1,0:T(8,128)(2,1)S(1)}) custom-call(bf16[64,2048]{1,0:T(8,128)(2,1)S(1)} %get-tuple-element.46.refs_0_, bf16[64,2048]{1,0:T(8,128)(2,1)S(1)} %get-tuple-element.47.refs_1_, bf16[448,2048]{1,0:T(8,128)(2,1)S(1)} %bitcast.26, bf16[448,2048]{1,0:T(8,128)(2,1)S(1)} %collective-permute-done.1.refs_3_.refs_5_, ...), custom_call_target="tpu_custom_call" | custom-call | flops 1409286144 | bytes 1048576 | tf_op jit(solution)/shard_map/pallas_call | solution.py:77
  70.1 2.0 %collective-permute-start.6 = (bf16[64,2048]{1,0:T(8,128)(2,1)S(1)}, bf16[64,2048]{1,0:T(8,128)(2,1)S(1)}, u32[]{:S(2)}, u32[]{:S(2)}) collective-permute-start(bf16[64,2048]{1,0:T(8,128)(2,1)S(1)} %collective-permute-done.5.refs_0_), channel_id=1, source_target_pairs={{0,2},{1,3},{2,4},{3,5},{4,6},{5,7},{6,8},{7,9},{8,10},{9,11},{10,... | collective-permute-start | bytes 786440 | tf_op jit(solution)/shard_map/ppermute | solution.py:25
  72.1 2.5 %collective-permute-done.13.refs_1_ = bf16[64,2048]{1,0:T(8,128)(2,1)S(1)} collective-permute-done((bf16[64,2048]{1,0:T(8,128)(2,1)S(1)}, bf16[64,2048]{1,0:T(8,128)(2,1)S(1)}, u32[]{:S(2)}, u32[]{:S(2)}) %collective-permute-start.13) | collective-permute-done | bytes 262176 | tf_op jit(solution)/shard_map/ppermute | solution.py:25
  75.1 2.8 %collective-permute-start.17 = (bf16[64,2048]{1,0:T(8,128)(2,1)S(1)}, bf16[64,2048]{1,0:T(8,128)(2,1)S(1)}, u32[]{:S(2)}, u32[]{:S(2)}) collective-permute-start(bf16[64,2048]{1,0:T(8,128)(2,1)S(1)} %collective-permute-done.16.refs_2_), channel_id=1, source_target_pairs={{0,14},{1,15},{2,0},{3,1},{4,2},{5,3},{6,4},{7,5},{8,6},{9,7},{10,... | collective-permute-start | bytes 786440 | tf_op jit(solution)/shard_map/ppermute | solution.py:25
  77.9 4.1 %shard_map.132 = (bf16[64,2048]{1,0:T(8,128)(2,1)S(1)}, bf16[64,2048]{1,0:T(8,128)(2,1)S(1)}, bf16[64,2048]{1,0:T(8,128)(2,1)S(1)}, bf16[64,2048]{1,0:T(8,128)(2,1)S(1)}) custom-call(bf16[64,2048]{1,0:T(8,128)(2,1)S(1)} %collective-permute-done.5.refs_0_, bf16[64,2048]{1,0:T(8,128)(2,1)S(1)} %collective-permute-done.13.refs_1_, ...), custom_call_target="tpu_custom_call" | custom-call | flops 2818572288 | bytes 1048576 | tf_op jit(solution)/shard_map/pallas_call | solution.py:77
  82.1 2.0 %collective-permute-start.7 = (bf16[64,2048]{1,0:T(8,128)(2,1)S(1)}, bf16[64,2048]{1,0:T(8,128)(2,1)S(1)}, u32[]{:S(2)}, u32[]{:S(2)}) collective-permute-start(bf16[64,2048]{1,0:T(8,128)(2,1)S(1)} %collective-permute-done.6.refs_0_), channel_id=1, source_target_pairs={{0,2},{1,3},{2,4},{3,5},{4,6},{5,7},{6,8},{7,9},{8,10},{9,11},{10,... | collective-permute-start | bytes 786440 | tf_op jit(solution)/shard_map/ppermute | solution.py:25
  84.1 2.0 %collective-permute-done.14.refs_1_ = bf16[64,2048]{1,0:T(8,128)(2,1)S(1)} collective-permute-done((bf16[64,2048]{1,0:T(8,128)(2,1)S(1)}, bf16[64,2048]{1,0:T(8,128)(2,1)S(1)}, u32[]{:S(2)}, u32[]{:S(2)}) %collective-permute-start.14) | collective-permute-done | bytes 262176 | tf_op jit(solution)/shard_map/ppermute | solution.py:25
  86.1 4.1 %shard_map.133 = (bf16[64,2048]{1,0:T(8,128)(2,1)S(1)}, bf16[64,2048]{1,0:T(8,128)(2,1)S(1)}, bf16[64,2048]{1,0:T(8,128)(2,1)S(1)}, bf16[64,2048]{1,0:T(8,128)(2,1)S(1)}) custom-call(bf16[64,2048]{1,0:T(8,128)(2,1)S(1)} %collective-permute-done.6.refs_0_, bf16[64,2048]{1,0:T(8,128)(2,1)S(1)} %collective-permute-done.14.refs_1_, ...), custom_call_target="tpu_custom_call" | custom-call | flops 2818572288 | bytes 1048576 | tf_op jit(solution)/shard_map/pallas_call | solution.py:77
  90.2 3.3 %shard_map.134 = (bf16[64,2048]{1,0:T(8,128)(2,1)S(1)}, bf16[64,2048]{1,0:T(8,128)(2,1)S(1)}) custom-call(bf16[64,2048]{1,0:T(8,128)(2,1)S(1)} %collective-permute-done.7.refs_0_, bf16[64,2048]{1,0:T(8,128)(2,1)S(1)} %collective-permute-done.11.refs_1_, bf16[448,2048]{1,0:T(8,128)(2,1)S(1)} %bitcast.29, ...), custom_call_target="tpu_custom_call" | custom-call | flops 1409286144 | bytes 1048576 | tf_op jit(solution)/shard_map/pallas_call | solution.py:77
  93.8 1.8 %collective-permute-start.18 = (bf16[64,2048]{1,0:T(8,128)(2,1)S(1)}, bf16[64,2048]{1,0:T(8,128)(2,1)S(1)}, u32[]{:S(2)}, u32[]{:S(2)}) collective-permute-start(bf16[64,2048]{1,0:T(8,128)(2,1)S(1)} %get-tuple-element.57.refs_10_), channel_id=1, source_target_pairs={{0,2},{1,3},{2,4},{3,5},{4,6},{5,7},{6,8},{7,9},{8,10},{9,11},{10,... | collective-permute-start | bytes 786440 | tf_op jit(solution)/shard_map/ppermute | solution.py:25
  96.1 2.8 %collective-permute-start.22 = (bf16[64,2048]{1,0:T(8,128)(2,1)S(1)}, bf16[64,2048]{1,0:T(8,128)(2,1)S(1)}, u32[]{:S(2)}, u32[]{:S(2)}) collective-permute-start(bf16[64,2048]{1,0:T(8,128)(2,1)S(1)} %get-tuple-element.56.refs_8_), channel_id=1, source_target_pairs={{0,14},{1,15},{2,0},{3,1},{4,2},{5,3},{6,4},{7,5},{8,6},{9,7},{10,... | collective-permute-start | bytes 786440 | tf_op jit(solution)/shard_map/ppermute | solution.py:25
  98.9 3.9 %collective-permute-done.28.a = bf16[64,2048]{1,0:T(8,128)(2,1)S(1)} collective-permute-done((bf16[64,2048]{1,0:T(8,128)(2,1)S(1)}, bf16[64,2048]{1,0:T(8,128)(2,1)S(1)}, u32[]{:S(2)}, u32[]{:S(2)}) %collective-permute-start.28) | collective-permute-done | bytes 262176 | tf_op jit(solution)/shard_map/ppermute | solution.py:25
  102.9 1.5 %collective-permute-start.29 = (bf16[64,2048]{1,0:T(8,128)(2,1)S(1)}, bf16[64,2048]{1,0:T(8,128)(2,1)S(1)}, u32[]{:S(2)}, u32[]{:S(2)}) collective-permute-start(bf16[64,2048]{1,0:T(8,128)(2,1)S(1)} %shard_map.143), channel_id=1, source_target_pairs={{0,14},{1,15},{2,0},{3,1},{4,2},{5,3},{6,4},{7,5},{8,6},{9,7},{10,... | collective-permute-start | bytes 786440 | tf_op jit(solution)/shard_map/ppermute | solution.py:25
  104.4 0.9 collective-permute-start.19
  105.3 4.2 %collective-permute-done.25.a = bf16[64,2048]{1,0:T(8,128)(2,1)S(1)} collective-permute-done((bf16[64,2048]{1,0:T(8,128)(2,1)S(1)}, bf16[64,2048]{1,0:T(8,128)(2,1)S(1)}, u32[]{:S(2)}, u32[]{:S(2)}) %collective-permute-start.25) | collective-permute-done | bytes 262176 | tf_op jit(solution)/shard_map/ppermute | solution.py:25
  109.6 0.6 collective-permute-start.26
  110.2 2.8 %collective-permute-start.23 = (bf16[64,2048]{1,0:T(8,128)(2,1)S(1)}, bf16[64,2048]{1,0:T(8,128)(2,1)S(1)}, u32[]{:S(2)}, u32[]{:S(2)}) collective-permute-start(bf16[64,2048]{1,0:T(8,128)(2,1)S(1)} %shard_map.139), channel_id=1, source_target_pairs={{0,14},{1,15},{2,0},{3,1},{4,2},{5,3},{6,4},{7,5},{8,6},{9,7},{10,... | collective-permute-start | bytes 786440 | tf_op jit(solution)/shard_map/ppermute | solution.py:25
  113.0 1.0 collective-permute-done.29.a
  114.1 1.5 %collective-permute-start.30 = (bf16[64,2048]{1,0:T(8,128)(2,1)S(1)}, bf16[64,2048]{1,0:T(8,128)(2,1)S(1)}, u32[]{:S(2)}, u32[]{:S(2)}) collective-permute-start(bf16[64,2048]{1,0:T(8,128)(2,1)S(1)} %shard_map.144), channel_id=1, source_target_pairs={{0,14},{1,15},{2,0},{3,1},{4,2},{5,3},{6,4},{7,5},{8,6},{9,7},{10,... | collective-permute-start | bytes 786440 | tf_op jit(solution)/shard_map/ppermute | solution.py:25
  115.7 0.7 collective-permute-start.20
  116.3 4.1 %shard_map.137 = (bf16[64,2048]{1,0:T(8,128)(2,1)S(1)}, bf16[64,2048]{1,0:T(8,128)(2,1)S(1)}, bf16[64,2048]{1,0:T(8,128)(2,1)S(1)}, bf16[64,2048]{1,0:T(8,128)(2,1)S(1)}) custom-call(bf16[64,2048]{1,0:T(8,128)(2,1)S(1)} %collective-permute-done.4.refs_0_, bf16[64,2048]{1,0:T(8,128)(2,1)S(1)} %collective-permute-done.12.refs_1_, ...), custom_call_target="tpu_custom_call" | custom-call | flops 2818572288 | bytes 1048576 | tf_op jit(solution)/shard_map/pallas_call | solution.py:77
  120.8 0.6 collective-permute-start.27
  121.5 2.8 %collective-permute-start.24 = (bf16[64,2048]{1,0:T(8,128)(2,1)S(1)}, bf16[64,2048]{1,0:T(8,128)(2,1)S(1)}, u32[]{:S(2)}, u32[]{:S(2)}) collective-permute-start(bf16[64,2048]{1,0:T(8,128)(2,1)S(1)} %shard_map.140), channel_id=1, source_target_pairs={{0,14},{1,15},{2,0},{3,1},{4,2},{5,3},{6,4},{7,5},{8,6},{9,7},{10,... | collective-permute-start | bytes 786440 | tf_op jit(solution)/shard_map/ppermute | solution.py:25
  124.3 0.7 collective-permute-done.30.a
  125.0 2.7 %collective-permute-start.31 = (bf16[64,2048]{1,0:T(8,128)(2,1)S(1)}, bf16[64,2048]{1,0:T(8,128)(2,1)S(1)}, u32[]{:S(2)}, u32[]{:S(2)}) collective-permute-start(bf16[64,2048]{1,0:T(8,128)(2,1)S(1)} %shard_map.145), channel_id=1, source_target_pairs={{0,14},{1,15},{2,0},{3,1},{4,2},{5,3},{6,4},{7,5},{8,6},{9,7},{10,... | collective-permute-start | bytes 786440 | tf_op jit(solution)/shard_map/ppermute | solution.py:25
  127.8 2.7 %collective-permute-done.27.right_b = bf16[64,2048]{1,0:T(8,128)(2,1)S(1)} collective-permute-done((bf16[64,2048]{1,0:T(8,128)(2,1)S(1)}, bf16[64,2048]{1,0:T(8,128)(2,1)S(1)}, u32[]{:S(2)}, u32[]{:S(2)}) %collective-permute-start.27) | collective-permute-done | bytes 262176 | tf_op jit(solution)/shard_map/ppermute | solution.py:25
  130.5 1.1 collective-permute-done.31.left_b
  131.6 3.8 %collective-permute-done.21.right_a = bf16[64,2048]{1,0:T(8,128)(2,1)S(1)} collective-permute-done((bf16[64,2048]{1,0:T(8,128)(2,1)S(1)}, bf16[64,2048]{1,0:T(8,128)(2,1)S(1)}, u32[]{:S(2)}, u32[]{:S(2)}) %collective-permute-start.21) | collective-permute-done | bytes 262176 | tf_op jit(solution)/shard_map/ppermute | solution.py:25
  135.6 14.1 %all_to_all.17 = bf16[16,8,2048]{2,1,0:T(8,128)(2,1)S(1)} all-to-all(bf16[16,8,2048]{2,1,0:T(8,128)(2,1)S(1)} %bitcast.44), channel_id=1, replica_groups=mesh['sp'=16,'tp'=16] {'sp'}, dimensions={0} | all-to-all | bytes 1048576 | tf_op jit(solution)/shard_map/all_to_all | solution.py:402
  150.0 1.0 add_convert_fusion
  (68 shorter events, 5.5 us)
Async XLA Ops:
  0.8 8.2 %collective-permute-start = (bf16[64,128]{1,0:T(8,128)(2,1)S(1)}, bf16[64,128]{1,0:T(8,128)(2,1)S(1)}, u32[]{:S(2)}, u32[]{:S(2)}) collective-permute-start(bf16[64,128]{1,0:T(8,128)(2,1)S(1)} %multiply_convert_fusion), channel_id=1, source_target_pairs={{0,16},{16,32},{32,48},{48,64},{64,80},{80,96},{96,112},{112,128},... | collective-permute-start | bytes 49160 | tf_op jit(solution)/shard_map/ppermute | solution.py:20
  4.2 0.9 copy-start.3
  5.1 0.9 copy-start.4
  6.0 0.7 copy-start.5
  6.7 19.5 %copy-start.6 = (bf16[1024,2048]{1,0:T(8,128)(2,1)S(1)}, bf16[1024,2048]{1,0:T(8,128)(2,1)}, u32[]{:S(2)}) copy-start(bf16[1024,2048]{1,0:T(8,128)(2,1)} %out_weight.1) | copy-start | bytes 12582916
  6.7 19.5 %copy-start.7 = (bf16[64,2048]{1,0:T(8,128)(2,1)S(1)}, bf16[64,2048]{1,0:T(8,128)(2,1)}, u32[]{:S(2)}) copy-start(bf16[64,2048]{1,0:T(8,128)(2,1)} %stream.1) | copy-start | bytes 786436
  6.7 19.5 %copy-start.8 = (f32[2048]{0:T(1024)S(1)}, f32[2048]{0:T(1024)}, u32[]{:S(2)}) copy-start(f32[2048]{0:T(1024)} %param.22) | copy-start | bytes 24580
  6.7 19.5 %copy-start.9 = (f32[1024]{0:T(1024)S(1)}, f32[1024]{0:T(1024)}, u32[]{:S(2)}) copy-start(f32[1024]{0:T(1024)} %param.16) | copy-start | bytes 12292
  6.8 19.5 %copy-start.10 = (f32[1024]{0:T(1024)S(1)}, f32[1024]{0:T(1024)}, u32[]{:S(2)}) copy-start(f32[1024]{0:T(1024)} %param.17) | copy-start | bytes 12292
  6.8 19.5 %copy-start.11 = (s32[64,2]{0,1:T(2,128)S(1)}, s32[64,2]{0,1:T(2,128)}, u32[]{:S(2)}) copy-start(s32[64,2]{0,1:T(2,128)} %param.20) | copy-start | bytes 1540
  6.8 19.5 %copy-start.12 = (f32[64,2]{0,1:T(2,128)S(1)}, f32[64,2]{0,1:T(2,128)}, u32[]{:S(2)}) copy-start(f32[64,2]{0,1:T(2,128)} %param.21) | copy-start | bytes 1540
  26.3 1.5 %copy-start = (bf16[1,2048,448]{1,2,0:T(8,128)(2,1)S(1)}, bf16[1,2048,448]{1,2,0:T(8,128)(2,1)}, u32[]{:S(2)}) copy-start(bf16[1,2048,448]{1,2,0:T(8,128)(2,1)} %param.23) | copy-start | bytes 5505028
  26.3 2.3 %copy-start.1 = (bf16[1,2048,448]{1,2,0:T(8,128)(2,1)S(1)}, bf16[1,2048,448]{1,2,0:T(8,128)(2,1)}, u32[]{:S(2)}) copy-start(bf16[1,2048,448]{1,2,0:T(8,128)(2,1)} %param.24) | copy-start | bytes 5505028
  26.4 2.7 %copy-start.2 = (bf16[1,448,2048]{2,1,0:T(8,128)(2,1)S(1)}, bf16[1,448,2048]{2,1,0:T(8,128)(2,1)}, u32[]{:S(2)}) copy-start(bf16[1,448,2048]{2,1,0:T(8,128)(2,1)} %param.25) | copy-start | bytes 5505028
  27.9 19.0 %collective-permute-start.1 = (bf16[448,2048]{1,0:T(8,128)(2,1)S(1)}, bf16[448,2048]{1,0:T(8,128)(2,1)S(1)}, u32[]{:S(2)}, u32[]{:S(2)}) collective-permute-start(bf16[448,2048]{1,0:T(8,128)(2,1)S(1)} %bitcast.25), channel_id=1, source_target_pairs={{0,1},{1,0},{2,3},{3,2},{4,5},{5,4},{6,7},{7,6},{8,9},{9,8},{10,11... | collective-permute-start | bytes 5505032 | tf_op jit(solution)/shard_map/ppermute | solution.py:30
  28.6 18.3 %collective-permute-start.2 = (bf16[448,2048]{1,0:T(8,128)(2,1)S(1)}, bf16[448,2048]{1,0:T(8,128)(2,1)S(1)}, u32[]{:S(2)}, u32[]{:S(2)}) collective-permute-start(bf16[448,2048]{1,0:T(8,128)(2,1)S(1)} %bitcast.31), channel_id=1, source_target_pairs={{0,1},{1,0},{2,3},{3,2},{4,5},{5,4},{6,7},{7,6},{8,9},{9,8},{10,11... | collective-permute-start | bytes 5505032 | tf_op jit(solution)/shard_map/ppermute | solution.py:30
  29.0 17.9 %collective-permute-start.3 = (bf16[448,2048]{1,0:T(8,128)(2,1)S(1)}, bf16[448,2048]{1,0:T(8,128)(2,1)S(1)}, u32[]{:S(2)}, u32[]{:S(2)}) collective-permute-start(bf16[448,2048]{1,0:T(8,128)(2,1)S(1)} %bitcast.37), channel_id=1, source_target_pairs={{0,1},{1,0},{2,3},{3,2},{4,5},{5,4},{6,7},{7,6},{8,9},{9,8},{10,11... | collective-permute-start | bytes 5505032 | tf_op jit(solution)/shard_map/ppermute | solution.py:30
  47.0 9.3 %collective-permute-start.8 = (bf16[64,2048]{1,0:T(8,128)(2,1)S(1)}, bf16[64,2048]{1,0:T(8,128)(2,1)S(1)}, u32[]{:S(2)}, u32[]{:S(2)}) collective-permute-start(bf16[64,2048]{1,0:T(8,128)(2,1)S(1)} %get-tuple-element.47.refs_1_), channel_id=1, source_target_pairs={{0,14},{1,15},{2,0},{3,1},{4,2},{5,3},{6,4},{7,5},{8,6},{9,7},{10,... | collective-permute-start | bytes 786440 | tf_op jit(solution)/shard_map/ppermute | solution.py:25
  47.4 10.4 %collective-permute-start.4 = (bf16[64,2048]{1,0:T(8,128)(2,1)S(1)}, bf16[64,2048]{1,0:T(8,128)(2,1)S(1)}, u32[]{:S(2)}, u32[]{:S(2)}) collective-permute-start(bf16[64,2048]{1,0:T(8,128)(2,1)S(1)} %get-tuple-element.46.refs_0_), channel_id=1, source_target_pairs={{0,2},{1,3},{2,4},{3,5},{4,6},{5,7},{6,8},{7,9},{8,10},{9,11},{10,... | collective-permute-start | bytes 786440 | tf_op jit(solution)/shard_map/ppermute | solution.py:25
  49.1 14.3 %collective-permute-start.12 = (bf16[64,2048]{1,0:T(8,128)(2,1)S(1)}, bf16[64,2048]{1,0:T(8,128)(2,1)S(1)}, u32[]{:S(2)}, u32[]{:S(2)}) collective-permute-start(bf16[64,2048]{1,0:T(8,128)(2,1)S(1)} %get-tuple-element.47.refs_1_), channel_id=1, source_target_pairs={{0,2},{1,3},{2,4},{3,5},{4,6},{5,7},{6,8},{7,9},{8,10},{9,11},{10,... | collective-permute-start | bytes 786440 | tf_op jit(solution)/shard_map/ppermute | solution.py:25
  49.6 14.2 %collective-permute-start.15 = (bf16[64,2048]{1,0:T(8,128)(2,1)S(1)}, bf16[64,2048]{1,0:T(8,128)(2,1)S(1)}, u32[]{:S(2)}, u32[]{:S(2)}) collective-permute-start(bf16[64,2048]{1,0:T(8,128)(2,1)S(1)} %get-tuple-element.46.refs_0_), channel_id=1, source_target_pairs={{0,14},{1,15},{2,0},{3,1},{4,2},{5,3},{6,4},{7,5},{8,6},{9,7},{10,... | collective-permute-start | bytes 786440 | tf_op jit(solution)/shard_map/ppermute | solution.py:25
  56.2 13.8 %collective-permute-start.9 = (bf16[64,2048]{1,0:T(8,128)(2,1)S(1)}, bf16[64,2048]{1,0:T(8,128)(2,1)S(1)}, u32[]{:S(2)}, u32[]{:S(2)}) collective-permute-start(bf16[64,2048]{1,0:T(8,128)(2,1)S(1)} %collective-permute-done.8.refs_3_), channel_id=1, source_target_pairs={{0,14},{1,15},{2,0},{3,1},{4,2},{5,3},{6,4},{7,5},{8,6},{9,7},{10,... | collective-permute-start | bytes 786440 | tf_op jit(solution)/shard_map/ppermute | solution.py:25
  57.8 12.3 %collective-permute-start.5 = (bf16[64,2048]{1,0:T(8,128)(2,1)S(1)}, bf16[64,2048]{1,0:T(8,128)(2,1)S(1)}, u32[]{:S(2)}, u32[]{:S(2)}) collective-permute-start(bf16[64,2048]{1,0:T(8,128)(2,1)S(1)} %collective-permute-done.4.refs_0_), channel_id=1, source_target_pairs={{0,2},{1,3},{2,4},{3,5},{4,6},{5,7},{6,8},{7,9},{8,10},{9,11},{10,... | collective-permute-start | bytes 786440 | tf_op jit(solution)/shard_map/ppermute | solution.py:25
  63.4 11.2 %collective-permute-start.13 = (bf16[64,2048]{1,0:T(8,128)(2,1)S(1)}, bf16[64,2048]{1,0:T(8,128)(2,1)S(1)}, u32[]{:S(2)}, u32[]{:S(2)}) collective-permute-start(bf16[64,2048]{1,0:T(8,128)(2,1)S(1)} %collective-permute-done.12.refs_1_), channel_id=1, source_target_pairs={{0,2},{1,3},{2,4},{3,5},{4,6},{5,7},{6,8},{7,9},{8,10},{9,11},{10,... | collective-permute-start | bytes 786440 | tf_op jit(solution)/shard_map/ppermute | solution.py:25
  63.9 11.2 %collective-permute-start.16 = (bf16[64,2048]{1,0:T(8,128)(2,1)S(1)}, bf16[64,2048]{1,0:T(8,128)(2,1)S(1)}, u32[]{:S(2)}, u32[]{:S(2)}) collective-permute-start(bf16[64,2048]{1,0:T(8,128)(2,1)S(1)} %collective-permute-done.15.refs_2_), channel_id=1, source_target_pairs={{0,14},{1,15},{2,0},{3,1},{4,2},{5,3},{6,4},{7,5},{8,6},{9,7},{10,... | collective-permute-start | bytes 786440 | tf_op jit(solution)/shard_map/ppermute | solution.py:25
  70.0 12.0 %collective-permute-start.10 = (bf16[64,2048]{1,0:T(8,128)(2,1)S(1)}, bf16[64,2048]{1,0:T(8,128)(2,1)S(1)}, u32[]{:S(2)}, u32[]{:S(2)}) collective-permute-start(bf16[64,2048]{1,0:T(8,128)(2,1)S(1)} %collective-permute-done.9.refs_3_), channel_id=1, source_target_pairs={{0,14},{1,15},{2,0},{3,1},{4,2},{5,3},{6,4},{7,5},{8,6},{9,7},{10,... | collective-permute-start | bytes 786440 | tf_op jit(solution)/shard_map/ppermute | solution.py:25
  70.1 12.0 %collective-permute-start.6 = (bf16[64,2048]{1,0:T(8,128)(2,1)S(1)}, bf16[64,2048]{1,0:T(8,128)(2,1)S(1)}, u32[]{:S(2)}, u32[]{:S(2)}) collective-permute-start(bf16[64,2048]{1,0:T(8,128)(2,1)S(1)} %collective-permute-done.5.refs_0_), channel_id=1, source_target_pairs={{0,2},{1,3},{2,4},{3,5},{4,6},{5,7},{6,8},{7,9},{8,10},{9,11},{10,... | collective-permute-start | bytes 786440 | tf_op jit(solution)/shard_map/ppermute | solution.py:25
  74.6 11.4 %collective-permute-start.14 = (bf16[64,2048]{1,0:T(8,128)(2,1)S(1)}, bf16[64,2048]{1,0:T(8,128)(2,1)S(1)}, u32[]{:S(2)}, u32[]{:S(2)}) collective-permute-start(bf16[64,2048]{1,0:T(8,128)(2,1)S(1)} %collective-permute-done.13.refs_1_), channel_id=1, source_target_pairs={{0,2},{1,3},{2,4},{3,5},{4,6},{5,7},{6,8},{7,9},{8,10},{9,11},{10,... | collective-permute-start | bytes 786440 | tf_op jit(solution)/shard_map/ppermute | solution.py:25
  75.1 11.0 %collective-permute-start.17 = (bf16[64,2048]{1,0:T(8,128)(2,1)S(1)}, bf16[64,2048]{1,0:T(8,128)(2,1)S(1)}, u32[]{:S(2)}, u32[]{:S(2)}) collective-permute-start(bf16[64,2048]{1,0:T(8,128)(2,1)S(1)} %collective-permute-done.16.refs_2_), channel_id=1, source_target_pairs={{0,14},{1,15},{2,0},{3,1},{4,2},{5,3},{6,4},{7,5},{8,6},{9,7},{10,... | collective-permute-start | bytes 786440 | tf_op jit(solution)/shard_map/ppermute | solution.py:25
  82.0 8.2 %collective-permute-start.11 = (bf16[64,2048]{1,0:T(8,128)(2,1)S(1)}, bf16[64,2048]{1,0:T(8,128)(2,1)S(1)}, u32[]{:S(2)}, u32[]{:S(2)}) collective-permute-start(bf16[64,2048]{1,0:T(8,128)(2,1)S(1)} %collective-permute-done.10.refs_3_), channel_id=1, source_target_pairs={{0,14},{1,15},{2,0},{3,1},{4,2},{5,3},{6,4},{7,5},{8,6},{9,7},{10,... | collective-permute-start | bytes 786440 | tf_op jit(solution)/shard_map/ppermute | solution.py:25
  82.1 8.1 %collective-permute-start.7 = (bf16[64,2048]{1,0:T(8,128)(2,1)S(1)}, bf16[64,2048]{1,0:T(8,128)(2,1)S(1)}, u32[]{:S(2)}, u32[]{:S(2)}) collective-permute-start(bf16[64,2048]{1,0:T(8,128)(2,1)S(1)} %collective-permute-done.6.refs_0_), channel_id=1, source_target_pairs={{0,2},{1,3},{2,4},{3,5},{4,6},{5,7},{6,8},{7,9},{8,10},{9,11},{10,... | collective-permute-start | bytes 786440 | tf_op jit(solution)/shard_map/ppermute | solution.py:25
  93.5 9.3 %collective-permute-start.28 = (bf16[64,2048]{1,0:T(8,128)(2,1)S(1)}, bf16[64,2048]{1,0:T(8,128)(2,1)S(1)}, u32[]{:S(2)}, u32[]{:S(2)}) collective-permute-start(bf16[64,2048]{1,0:T(8,128)(2,1)S(1)} %get-tuple-element.65), channel_id=1, source_target_pairs={{0,14},{1,15},{2,0},{3,1},{4,2},{5,3},{6,4},{7,5},{8,6},{9,7},{10,... | collective-permute-start | bytes 786440 | tf_op jit(solution)/shard_map/ppermute | solution.py:25
  93.8 10.5 %collective-permute-start.18 = (bf16[64,2048]{1,0:T(8,128)(2,1)S(1)}, bf16[64,2048]{1,0:T(8,128)(2,1)S(1)}, u32[]{:S(2)}, u32[]{:S(2)}) collective-permute-start(bf16[64,2048]{1,0:T(8,128)(2,1)S(1)} %get-tuple-element.57.refs_10_), channel_id=1, source_target_pairs={{0,2},{1,3},{2,4},{3,5},{4,6},{5,7},{6,8},{7,9},{8,10},{9,11},{10,... | collective-permute-start | bytes 786440 | tf_op jit(solution)/shard_map/ppermute | solution.py:25
  95.6 13.9 %collective-permute-start.25 = (bf16[64,2048]{1,0:T(8,128)(2,1)S(1)}, bf16[64,2048]{1,0:T(8,128)(2,1)S(1)}, u32[]{:S(2)}, u32[]{:S(2)}) collective-permute-start(bf16[64,2048]{1,0:T(8,128)(2,1)S(1)} %get-tuple-element.62), channel_id=1, source_target_pairs={{0,2},{1,3},{2,4},{3,5},{4,6},{5,7},{6,8},{7,9},{8,10},{9,11},{10,... | collective-permute-start | bytes 786440 | tf_op jit(solution)/shard_map/ppermute | solution.py:25
  96.1 14.1 %collective-permute-start.22 = (bf16[64,2048]{1,0:T(8,128)(2,1)S(1)}, bf16[64,2048]{1,0:T(8,128)(2,1)S(1)}, u32[]{:S(2)}, u32[]{:S(2)}) collective-permute-start(bf16[64,2048]{1,0:T(8,128)(2,1)S(1)} %get-tuple-element.56.refs_8_), channel_id=1, source_target_pairs={{0,14},{1,15},{2,0},{3,1},{4,2},{5,3},{6,4},{7,5},{8,6},{9,7},{10,... | collective-permute-start | bytes 786440 | tf_op jit(solution)/shard_map/ppermute | solution.py:25
  102.9 11.2 %collective-permute-start.29 = (bf16[64,2048]{1,0:T(8,128)(2,1)S(1)}, bf16[64,2048]{1,0:T(8,128)(2,1)S(1)}, u32[]{:S(2)}, u32[]{:S(2)}) collective-permute-start(bf16[64,2048]{1,0:T(8,128)(2,1)S(1)} %shard_map.143), channel_id=1, source_target_pairs={{0,14},{1,15},{2,0},{3,1},{4,2},{5,3},{6,4},{7,5},{8,6},{9,7},{10,... | collective-permute-start | bytes 786440 | tf_op jit(solution)/shard_map/ppermute | solution.py:25
  104.4 11.2 %collective-permute-start.19 = (bf16[64,2048]{1,0:T(8,128)(2,1)S(1)}, bf16[64,2048]{1,0:T(8,128)(2,1)S(1)}, u32[]{:S(2)}, u32[]{:S(2)}) collective-permute-start(bf16[64,2048]{1,0:T(8,128)(2,1)S(1)} %shard_map.135), channel_id=1, source_target_pairs={{0,2},{1,3},{2,4},{3,5},{4,6},{5,7},{6,8},{7,9},{8,10},{9,11},{10,... | collective-permute-start | bytes 786440 | tf_op jit(solution)/shard_map/ppermute | solution.py:25
  109.6 11.2 %collective-permute-start.26 = (bf16[64,2048]{1,0:T(8,128)(2,1)S(1)}, bf16[64,2048]{1,0:T(8,128)(2,1)S(1)}, u32[]{:S(2)}, u32[]{:S(2)}) collective-permute-start(bf16[64,2048]{1,0:T(8,128)(2,1)S(1)} %shard_map.141), channel_id=1, source_target_pairs={{0,2},{1,3},{2,4},{3,5},{4,6},{5,7},{6,8},{7,9},{8,10},{9,11},{10,... | collective-permute-start | bytes 786440 | tf_op jit(solution)/shard_map/ppermute | solution.py:25
  110.2 11.2 %collective-permute-start.23 = (bf16[64,2048]{1,0:T(8,128)(2,1)S(1)}, bf16[64,2048]{1,0:T(8,128)(2,1)S(1)}, u32[]{:S(2)}, u32[]{:S(2)}) collective-permute-start(bf16[64,2048]{1,0:T(8,128)(2,1)S(1)} %shard_map.139), channel_id=1, source_target_pairs={{0,14},{1,15},{2,0},{3,1},{4,2},{5,3},{6,4},{7,5},{8,6},{9,7},{10,... | collective-permute-start | bytes 786440 | tf_op jit(solution)/shard_map/ppermute | solution.py:25
  114.1 10.8 %collective-permute-start.30 = (bf16[64,2048]{1,0:T(8,128)(2,1)S(1)}, bf16[64,2048]{1,0:T(8,128)(2,1)S(1)}, u32[]{:S(2)}, u32[]{:S(2)}) collective-permute-start(bf16[64,2048]{1,0:T(8,128)(2,1)S(1)} %shard_map.144), channel_id=1, source_target_pairs={{0,14},{1,15},{2,0},{3,1},{4,2},{5,3},{6,4},{7,5},{8,6},{9,7},{10,... | collective-permute-start | bytes 786440 | tf_op jit(solution)/shard_map/ppermute | solution.py:25
  115.7 12.0 %collective-permute-start.20 = (bf16[64,2048]{1,0:T(8,128)(2,1)S(1)}, bf16[64,2048]{1,0:T(8,128)(2,1)S(1)}, u32[]{:S(2)}, u32[]{:S(2)}) collective-permute-start(bf16[64,2048]{1,0:T(8,128)(2,1)S(1)} %shard_map.136), channel_id=1, source_target_pairs={{0,2},{1,3},{2,4},{3,5},{4,6},{5,7},{6,8},{7,9},{8,10},{9,11},{10,... | collective-permute-start | bytes 786440 | tf_op jit(solution)/shard_map/ppermute | solution.py:25
  120.8 9.7 %collective-permute-start.27 = (bf16[64,2048]{1,0:T(8,128)(2,1)S(1)}, bf16[64,2048]{1,0:T(8,128)(2,1)S(1)}, u32[]{:S(2)}, u32[]{:S(2)}) collective-permute-start(bf16[64,2048]{1,0:T(8,128)(2,1)S(1)} %shard_map.142), channel_id=1, source_target_pairs={{0,2},{1,3},{2,4},{3,5},{4,6},{5,7},{6,8},{7,9},{8,10},{9,11},{10,... | collective-permute-start | bytes 786440 | tf_op jit(solution)/shard_map/ppermute | solution.py:25
  121.5 9.0 %collective-permute-start.24 = (bf16[64,2048]{1,0:T(8,128)(2,1)S(1)}, bf16[64,2048]{1,0:T(8,128)(2,1)S(1)}, u32[]{:S(2)}, u32[]{:S(2)}) collective-permute-start(bf16[64,2048]{1,0:T(8,128)(2,1)S(1)} %shard_map.140), channel_id=1, source_target_pairs={{0,14},{1,15},{2,0},{3,1},{4,2},{5,3},{6,4},{7,5},{8,6},{9,7},{10,... | collective-permute-start | bytes 786440 | tf_op jit(solution)/shard_map/ppermute | solution.py:25
  125.0 6.6 %collective-permute-start.31 = (bf16[64,2048]{1,0:T(8,128)(2,1)S(1)}, bf16[64,2048]{1,0:T(8,128)(2,1)S(1)}, u32[]{:S(2)}, u32[]{:S(2)}) collective-permute-start(bf16[64,2048]{1,0:T(8,128)(2,1)S(1)} %shard_map.145), channel_id=1, source_target_pairs={{0,14},{1,15},{2,0},{3,1},{4,2},{5,3},{6,4},{7,5},{8,6},{9,7},{10,... | collective-permute-start | bytes 786440 | tf_op jit(solution)/shard_map/ppermute | solution.py:25
  127.7 7.7 %collective-permute-start.21 = (bf16[64,2048]{1,0:T(8,128)(2,1)S(1)}, bf16[64,2048]{1,0:T(8,128)(2,1)S(1)}, u32[]{:S(2)}, u32[]{:S(2)}) collective-permute-start(bf16[64,2048]{1,0:T(8,128)(2,1)S(1)} %shard_map.138), channel_id=1, source_target_pairs={{0,2},{1,3},{2,4},{3,5},{4,6},{5,7},{6,8},{7,9},{8,10},{9,11},{10,... | collective-permute-start | bytes 786440 | tf_op jit(solution)/shard_map/ppermute | solution.py:25

commit v4 on v3

--- a/solution.py
+++ b/solution.py
@@ -113,16 +113,10 @@
     return jnp.concatenate([taps[...], taps[...]], axis=1)
 
 
-def conv_main_kernel(far_value, far_gate, far_taps, out, laid, value, gate, taps, arrived):
-    pairs = ((far_value, value), (far_gate, gate), (far_taps, taps))
-    fetches = [pltpu.make_async_copy(*pair, arrived.at[i]) for i, pair in enumerate(pairs)]
-    for fetch in fetches:
-        fetch.start()
-    for fetch in fetches:
-        fetch.wait()
+def conv_main_kernel(line, taps, out, laid):
     blocks, rows, _ = out.shape
     both = twice(taps)
-    line = gated(value[...], gate[...]).astype(f32)
+    line = line[...].astype(f32)
     line = jnp.concatenate([line, jnp.zeros((line.shape[0], TILE), f32)], axis=1)
     laid[...] = position_major(line)
     lead = both.shape[0] - 1
@@ -133,41 +127,34 @@
         out[block, :, :] = tap_sum(window, rows - lead, rows, both)
 
 
-def conv_first_kernel(rim, value, gate, taps, _, out, laid):
+def conv_first_kernel(rim, line, taps, _, out, laid):
     rows = out.shape[1]
     both = twice(taps)
-    line = gated(value[...], gate[...]).astype(f32)
+    line = line[...].astype(f32)
     line = jnp.concatenate([rim[...].astype(f32), line, jnp.zeros_like(line)], axis=1)
     laid[...] = position_major(line)
     lead = both.shape[0] - 1
     out[0, :, :] = tap_sum(laid, rim.shape[1] - lead, rows, both)
 
 
-def convolve(conv_value, conv_gate, taps, rim, blocks):
-    channels, length = conv_value.shape
+def convolve(line, taps, rim, blocks):
+    channels, length = line.shape
     rows = length // blocks // 2
     shape = jax.ShapeDtypeStruct((blocks, rows, 2 * channels), bf16)
     main = pl.pallas_call(
         conv_main_kernel,
-        in_specs=[pl.BlockSpec(memory_space=pltpu.HBM)] * 3,
+        in_specs=in_vmem(2),
         out_specs=in_vmem(1)[0],
         out_shape=shape,
-        scratch_shapes=[
-            pltpu.VMEM((length, 2 * channels), f32),
-            pltpu.VMEM(conv_value.shape, bf16),
-            pltpu.VMEM(conv_gate.shape, bf16),
-            pltpu.VMEM(taps.shape, f32),
-            pltpu.SemaphoreType.DMA((3,)),
-        ],
+        scratch_shapes=[pltpu.VMEM((length, 2 * channels), f32)],
         compiler_params=pltpu.CompilerParams(vmem_limit_bytes=4 << 20),
         cost_estimate=pl.CostEstimate(flops=5 << 28, bytes_accessed=1 << 20, transcendentals=0),
-    )(conv_value, conv_gate, taps)
+    )(line, taps)
     return pl.pallas_call(
         conv_first_kernel,
         grid=(1,),
         in_specs=[
             pl.BlockSpec(rim.shape, lambda i: (0, 0)),
-            pl.BlockSpec((channels, TILE), lambda i: (0, 0)),
             pl.BlockSpec((channels, TILE), lambda i: (0, 0)),
             pl.BlockSpec(taps.shape, lambda i: (0, 0)),
             pl.BlockSpec(memory_space=pl.ANY),
@@ -175,10 +162,10 @@
         out_specs=pl.BlockSpec((1, rows, 2 * channels), lambda i: (0, 0, 0)),
         out_shape=shape,
         scratch_shapes=[pltpu.VMEM((rim.shape[1] + TILE, 2 * channels), f32)],
-        input_output_aliases={4: 0},
+        input_output_aliases={3: 0},
         compiler_params=pltpu.CompilerParams(vmem_limit_bytes=4 << 20),
         cost_estimate=pl.CostEstimate(flops=1 << 27, bytes_accessed=1 << 16, transcendentals=0),
-    )(rim, conv_value, conv_gate, taps, main)
+    )(rim, line, taps, main)
 
 
 def token_kernel(
@@ -335,10 +322,10 @@
     expert_down,
 ):
     run_len = conv_value.shape[1]
-    rim = gated(conv_value[:, run_len - TILE :], conv_gate[:, run_len - TILE :])
-    rim = shifted(rim, "sp", 1)
+    line = lax.optimization_barrier(gated(conv_value, conv_gate))
+    rim = shifted(line[:, run_len - TILE :], "sp", 1)
     blocks = lax.axis_size("tp")
-    conv_out = convolve(conv_value, conv_gate, conv_taps.T, rim, blocks)
+    conv_out = convolve(line, conv_taps.T, rim, blocks)
     tok_rows = stream.shape[0]
     width = stream.shape[1]
     top_count = routes.shape[1]

time: 151 us -> 149 us (0.987)
  local copies, waits for them, and re-layouts: 2.57 us -> 0.77 us
    unnamed x26 -> x22, local copies, waits for them, and re-layouts: 2.57 us -> 0.77 us
where the time goes in v4:
time: 149 us
  blocking collectives  48.4 us (32%)
  starting transfers between devices  41.8 us (28%)
  waiting for transfers between devices  32.1 us (22%)
  Pallas kernels  23.3 us (16%)
    ppermute x28, starting transfers between devices, z_shift(): lax.ppermute(value, 'tp', [(i, (i + 2 * steps) % count) for i in range(co...  36.7 us
    ppermute x28, waiting for transfers between devices, z_shift(): lax.ppermute(value, 'tp', [(i, (i + 2 * steps) % count) for i in range(co...  32.1 us
    pallas_call x5, Pallas kernels, expert(): pl.pallas_call(functools.partial(expert_kernel, sizes, hidden // 2, len(t...  19 us
    all_to_all x1, blocking collectives, per_device(): lax.all_to_all(send_rows, 'sp', split_axis=0, concat_axis=0, tiled=True)  17.3 us
    all_to_all x1, blocking collectives, per_device(): lax.all_to_all(conv_out, 'tp', split_axis=0, concat_axis=0, tiled=True)  17 us
    all_to_all x1, blocking collectives, per_device(): lax.all_to_all(result, 'sp', split_axis=0, concat_axis=0, tiled=True)  14.1 us
    ppermute x1, starting transfers between devices, shifted(): lax.ppermute(value, axis, [(source, source + steps) for source in range(i...  3.4 us
  transfers between devices with their start and end apart: 32, of which 13 were waited for; matrix products, arithmetic and copies ran while one was open for 0% of the time, Pallas kernels for 12%

profile of v4, /device:TPU:2, one launch (start us, length us, event | category | flops | bytes accessed | tf_op | source)
XLA Modules:
  0.0 148.9 jit_solution(275537992795208386)
XLA Ops:
  0.0 1.0 multiply_convert_fusion.line
  1.1 3.4 %collective-permute-start = (bf16[64,128]{1,0:T(8,128)(2,1)S(1)}, bf16[64,128]{1,0:T(8,128)(2,1)S(1)}, u32[]{:S(2)}, u32[]{:S(2)}) collective-permute-start(bf16[64,128]{1,0:T(8,128)(2,1)S(1)} %slice.4), channel_id=1, source_target_pairs={{0,16},{16,32},{32,48},{48,64},{64,80},{80,96},{96,112},{112,128},... | collective-permute-start | bytes 49160 | tf_op jit(solution)/shard_map/ppermute | solution.py:20
  4.5 0.7 copy-done.5
  5.2 1.8 %shard_map.127._ = bf16[16,32,128]{2,1,0:T(8,128)(2,1)S(1)} custom-call(bf16[64,1024]{1,0:T(8,128)(2,1)S(1)} %multiply_convert_fusion.line, f32[31,64]{1,0:T(8,128)S(1)} %bitcast.46), custom_call_target="tpu_custom_call" | custom-call | flops 1342177280 | bytes 1048576 | tf_op jit(solution)/shard_map/pallas_call | solution.py:144
  7.3 17.0 %all_to_all.15.conv = bf16[16,32,128]{2,1,0:T(8,128)(2,1)S(1)} all-to-all(bf16[16,32,128]{2,1,0:T(8,128)(2,1)S(1)} %shard_map.128), channel_id=1, replica_groups=mesh['sp'=16,'tp'=16] {'tp'}, dimensions={0} | all-to-all | bytes 262144 | tf_op jit(solution)/shard_map/all_to_all | solution.py:334
  24.4 1.5 %shard_map.129 = (bf16[128,2048]{1,0:T(8,128)(2,1)S(1)}, bf16[64,2048]{1,0:T(8,128)(2,1)S(1)}, bf16[128,64]{1,0:T(8,128)(2,1)S(1)}, bf16[128,64]{1,0:T(8,128)(2,1)S(1)}) custom-call(bf16[16,32,128]{2,1,0:T(8,128)(2,1)S(1)} %all_to_all.15.conv, f32[1,1024]{1,0:T(1,128)S(1)} %bitcast.49, f32[1,1024]{1,0:T(1,128)S(1)} %bitcast.50, ...), custom_call_target="tpu_custom_call" | custom-call | flops 1610612736 | bytes 5242880 | tf_op jit(solution)/shard_map/pallas_call | solution.py:234
  25.9 0.7 collective-permute-start.1
  27.1 0.6 collective-permute-start.3
  27.6 17.3 %all_to_all.16 = bf16[16,8,2048]{2,1,0:T(8,128)(2,1)S(1)} all-to-all(bf16[16,8,2048]{2,1,0:T(8,128)(2,1)S(1)} %bitcast.45), channel_id=1, replica_groups=mesh['sp'=16,'tp'=16] {'sp'}, dimensions={0} | all-to-all | bytes 1048576 | tf_op jit(solution)/shard_map/all_to_all | solution.py:349
  45.4 1.7 %collective-permute-start.4 = (bf16[64,2048]{1,0:T(8,128)(2,1)S(1)}, bf16[64,2048]{1,0:T(8,128)(2,1)S(1)}, u32[]{:S(2)}, u32[]{:S(2)}) collective-permute-start(bf16[64,2048]{1,0:T(8,128)(2,1)S(1)} %get-tuple-element.46.refs_0_), channel_id=1, source_target_pairs={{0,2},{1,3},{2,4},{3,5},{4,6},{5,7},{6,8},{7,9},{8,10},{9,11},{10,... | collective-permute-start | bytes 786440 | tf_op jit(solution)/shard_map/ppermute | solution.py:25
  47.1 0.6 collective-permute-start.12
  47.6 2.7 %collective-permute-start.15 = (bf16[64,2048]{1,0:T(8,128)(2,1)S(1)}, bf16[64,2048]{1,0:T(8,128)(2,1)S(1)}, u32[]{:S(2)}, u32[]{:S(2)}) collective-permute-start(bf16[64,2048]{1,0:T(8,128)(2,1)S(1)} %get-tuple-element.46.refs_0_), channel_id=1, source_target_pairs={{0,14},{1,15},{2,0},{3,1},{4,2},{5,3},{6,4},{7,5},{8,6},{9,7},{10,... | collective-permute-start | bytes 786440 | tf_op jit(solution)/shard_map/ppermute | solution.py:25
  50.3 3.9 %collective-permute-done.8.refs_3_ = bf16[64,2048]{1,0:T(8,128)(2,1)S(1)} collective-permute-done((bf16[64,2048]{1,0:T(8,128)(2,1)S(1)}, bf16[64,2048]{1,0:T(8,128)(2,1)S(1)}, u32[]{:S(2)}, u32[]{:S(2)}) %collective-permute-start.8) | collective-permute-done | bytes 262176 | tf_op jit(solution)/shard_map/ppermute | solution.py:25
  54.2 0.7 collective-permute-start.9
  55.0 0.8 collective-permute-done.4.refs_0_
  55.8 0.5 collective-permute-start.5
  56.3 5.1 %collective-permute-done.12.refs_1_ = bf16[64,2048]{1,0:T(8,128)(2,1)S(1)} collective-permute-done((bf16[64,2048]{1,0:T(8,128)(2,1)S(1)}, bf16[64,2048]{1,0:T(8,128)(2,1)S(1)}, u32[]{:S(2)}, u32[]{:S(2)}) %collective-permute-start.12) | collective-permute-done | bytes 262176 | tf_op jit(solution)/shard_map/ppermute | solution.py:25
  61.9 2.8 %collective-permute-start.16 = (bf16[64,2048]{1,0:T(8,128)(2,1)S(1)}, bf16[64,2048]{1,0:T(8,128)(2,1)S(1)}, u32[]{:S(2)}, u32[]{:S(2)}) collective-permute-start(bf16[64,2048]{1,0:T(8,128)(2,1)S(1)} %collective-permute-done.15.refs_2_), channel_id=1, source_target_pairs={{0,14},{1,15},{2,0},{3,1},{4,2},{5,3},{6,4},{7,5},{8,6},{9,7},{10,... | collective-permute-start | bytes 786440 | tf_op jit(solution)/shard_map/ppermute | solution.py:25
  64.6 3.3 %shard_map.131 = (bf16[64,2048]{1,0:T(8,128)(2,1)S(1)}, bf16[64,2048]{1,0:T(8,128)(2,1)S(1)}) custom-call(bf16[64,2048]{1,0:T(8,128)(2,1)S(1)} %get-tuple-element.46.refs_0_, bf16[64,2048]{1,0:T(8,128)(2,1)S(1)} %get-tuple-element.47.refs_1_, bf16[448,2048]{1,0:T(8,128)(2,1)S(1)} %bitcast.26, bf16[448,2048]{1,0:T(8,128)(2,1)S(1)} %collective-permute-done.1.refs_3_.refs_5_, ...), custom_call_target="tpu_custom_call" | custom-call | flops 1409286144 | bytes 1048576 | tf_op jit(solution)/shard_map/pallas_call | solution.py:77
  68.1 2.0 %collective-permute-start.6 = (bf16[64,2048]{1,0:T(8,128)(2,1)S(1)}, bf16[64,2048]{1,0:T(8,128)(2,1)S(1)}, u32[]{:S(2)}, u32[]{:S(2)}) collective-permute-start(bf16[64,2048]{1,0:T(8,128)(2,1)S(1)} %collective-permute-done.5.refs_0_), channel_id=1, source_target_pairs={{0,2},{1,3},{2,4},{3,5},{4,6},{5,7},{6,8},{7,9},{8,10},{9,11},{10,... | collective-permute-start | bytes 786440 | tf_op jit(solution)/shard_map/ppermute | solution.py:25
  70.1 2.5 %collective-permute-done.13.refs_1_ = bf16[64,2048]{1,0:T(8,128)(2,1)S(1)} collective-permute-done((bf16[64,2048]{1,0:T(8,128)(2,1)S(1)}, bf16[64,2048]{1,0:T(8,128)(2,1)S(1)}, u32[]{:S(2)}, u32[]{:S(2)}) %collective-permute-start.13) | collective-permute-done | bytes 262176 | tf_op jit(solution)/shard_map/ppermute | solution.py:25
  73.1 2.8 %collective-permute-start.17 = (bf16[64,2048]{1,0:T(8,128)(2,1)S(1)}, bf16[64,2048]{1,0:T(8,128)(2,1)S(1)}, u32[]{:S(2)}, u32[]{:S(2)}) collective-permute-start(bf16[64,2048]{1,0:T(8,128)(2,1)S(1)} %collective-permute-done.16.refs_2_), channel_id=1, source_target_pairs={{0,14},{1,15},{2,0},{3,1},{4,2},{5,3},{6,4},{7,5},{8,6},{9,7},{10,... | collective-permute-start | bytes 786440 | tf_op jit(solution)/shard_map/ppermute | solution.py:25
  75.9 4.1 %shard_map.132 = (bf16[64,2048]{1,0:T(8,128)(2,1)S(1)}, bf16[64,2048]{1,0:T(8,128)(2,1)S(1)}, bf16[64,2048]{1,0:T(8,128)(2,1)S(1)}, bf16[64,2048]{1,0:T(8,128)(2,1)S(1)}) custom-call(bf16[64,2048]{1,0:T(8,128)(2,1)S(1)} %collective-permute-done.5.refs_0_, bf16[64,2048]{1,0:T(8,128)(2,1)S(1)} %collective-permute-done.13.refs_1_, ...), custom_call_target="tpu_custom_call" | custom-call | flops 2818572288 | bytes 1048576 | tf_op jit(solution)/shard_map/pallas_call | solution.py:77
  80.1 2.0 %collective-permute-start.7 = (bf16[64,2048]{1,0:T(8,128)(2,1)S(1)}, bf16[64,2048]{1,0:T(8,128)(2,1)S(1)}, u32[]{:S(2)}, u32[]{:S(2)}) collective-permute-start(bf16[64,2048]{1,0:T(8,128)(2,1)S(1)} %collective-permute-done.6.refs_0_), channel_id=1, source_target_pairs={{0,2},{1,3},{2,4},{3,5},{4,6},{5,7},{6,8},{7,9},{8,10},{9,11},{10,... | collective-permute-start | bytes 786440 | tf_op jit(solution)/shard_map/ppermute | solution.py:25
  82.1 2.0 %collective-permute-done.14.refs_1_ = bf16[64,2048]{1,0:T(8,128)(2,1)S(1)} collective-permute-done((bf16[64,2048]{1,0:T(8,128)(2,1)S(1)}, bf16[64,2048]{1,0:T(8,128)(2,1)S(1)}, u32[]{:S(2)}, u32[]{:S(2)}) %collective-permute-start.14) | collective-permute-done | bytes 262176 | tf_op jit(solution)/shard_map/ppermute | solution.py:25
  84.1 4.1 %shard_map.133 = (bf16[64,2048]{1,0:T(8,128)(2,1)S(1)}, bf16[64,2048]{1,0:T(8,128)(2,1)S(1)}, bf16[64,2048]{1,0:T(8,128)(2,1)S(1)}, bf16[64,2048]{1,0:T(8,128)(2,1)S(1)}) custom-call(bf16[64,2048]{1,0:T(8,128)(2,1)S(1)} %collective-permute-done.6.refs_0_, bf16[64,2048]{1,0:T(8,128)(2,1)S(1)} %collective-permute-done.14.refs_1_, ...), custom_call_target="tpu_custom_call" | custom-call | flops 2818572288 | bytes 1048576 | tf_op jit(solution)/shard_map/pallas_call | solution.py:77
  88.2 3.3 %shard_map.134 = (bf16[64,2048]{1,0:T(8,128)(2,1)S(1)}, bf16[64,2048]{1,0:T(8,128)(2,1)S(1)}) custom-call(bf16[64,2048]{1,0:T(8,128)(2,1)S(1)} %collective-permute-done.7.refs_0_, bf16[64,2048]{1,0:T(8,128)(2,1)S(1)} %collective-permute-done.11.refs_1_, bf16[448,2048]{1,0:T(8,128)(2,1)S(1)} %bitcast.29, ...), custom_call_target="tpu_custom_call" | custom-call | flops 1409286144 | bytes 1048576 | tf_op jit(solution)/shard_map/pallas_call | solution.py:77
  91.9 1.8 %collective-permute-start.18 = (bf16[64,2048]{1,0:T(8,128)(2,1)S(1)}, bf16[64,2048]{1,0:T(8,128)(2,1)S(1)}, u32[]{:S(2)}, u32[]{:S(2)}) collective-permute-start(bf16[64,2048]{1,0:T(8,128)(2,1)S(1)} %get-tuple-element.57.refs_10_), channel_id=1, source_target_pairs={{0,2},{1,3},{2,4},{3,5},{4,6},{5,7},{6,8},{7,9},{8,10},{9,11},{10,... | collective-permute-start | bytes 786440 | tf_op jit(solution)/shard_map/ppermute | solution.py:25
  94.1 2.8 %collective-permute-start.22 = (bf16[64,2048]{1,0:T(8,128)(2,1)S(1)}, bf16[64,2048]{1,0:T(8,128)(2,1)S(1)}, u32[]{:S(2)}, u32[]{:S(2)}) collective-permute-start(bf16[64,2048]{1,0:T(8,128)(2,1)S(1)} %get-tuple-element.56.refs_8_), channel_id=1, source_target_pairs={{0,14},{1,15},{2,0},{3,1},{4,2},{5,3},{6,4},{7,5},{8,6},{9,7},{10,... | collective-permute-start | bytes 786440 | tf_op jit(solution)/shard_map/ppermute | solution.py:25
  96.9 3.9 %collective-permute-done.28.a = bf16[64,2048]{1,0:T(8,128)(2,1)S(1)} collective-permute-done((bf16[64,2048]{1,0:T(8,128)(2,1)S(1)}, bf16[64,2048]{1,0:T(8,128)(2,1)S(1)}, u32[]{:S(2)}, u32[]{:S(2)}) %collective-permute-start.28) | collective-permute-done | bytes 262176 | tf_op jit(solution)/shard_map/ppermute | solution.py:25
  100.9 1.5 %collective-permute-start.29 = (bf16[64,2048]{1,0:T(8,128)(2,1)S(1)}, bf16[64,2048]{1,0:T(8,128)(2,1)S(1)}, u32[]{:S(2)}, u32[]{:S(2)}) collective-permute-start(bf16[64,2048]{1,0:T(8,128)(2,1)S(1)} %shard_map.143), channel_id=1, source_target_pairs={{0,14},{1,15},{2,0},{3,1},{4,2},{5,3},{6,4},{7,5},{8,6},{9,7},{10,... | collective-permute-start | bytes 786440 | tf_op jit(solution)/shard_map/ppermute | solution.py:25
  102.5 0.9 collective-permute-start.19
  103.3 4.2 %collective-permute-done.25.a = bf16[64,2048]{1,0:T(8,128)(2,1)S(1)} collective-permute-done((bf16[64,2048]{1,0:T(8,128)(2,1)S(1)}, bf16[64,2048]{1,0:T(8,128)(2,1)S(1)}, u32[]{:S(2)}, u32[]{:S(2)}) %collective-permute-start.25) | collective-permute-done | bytes 262176 | tf_op jit(solution)/shard_map/ppermute | solution.py:25
  107.6 0.6 collective-permute-start.26
  108.3 2.8 %collective-permute-start.23 = (bf16[64,2048]{1,0:T(8,128)(2,1)S(1)}, bf16[64,2048]{1,0:T(8,128)(2,1)S(1)}, u32[]{:S(2)}, u32[]{:S(2)}) collective-permute-start(bf16[64,2048]{1,0:T(8,128)(2,1)S(1)} %shard_map.139), channel_id=1, source_target_pairs={{0,14},{1,15},{2,0},{3,1},{4,2},{5,3},{6,4},{7,5},{8,6},{9,7},{10,... | collective-permute-start | bytes 786440 | tf_op jit(solution)/shard_map/ppermute | solution.py:25
  111.1 1.0 collective-permute-done.29.a
  112.1 1.5 %collective-permute-start.30 = (bf16[64,2048]{1,0:T(8,128)(2,1)S(1)}, bf16[64,2048]{1,0:T(8,128)(2,1)S(1)}, u32[]{:S(2)}, u32[]{:S(2)}) collective-permute-start(bf16[64,2048]{1,0:T(8,128)(2,1)S(1)} %shard_map.144), channel_id=1, source_target_pairs={{0,14},{1,15},{2,0},{3,1},{4,2},{5,3},{6,4},{7,5},{8,6},{9,7},{10,... | collective-permute-start | bytes 786440 | tf_op jit(solution)/shard_map/ppermute | solution.py:25
  113.7 0.6 collective-permute-start.20
  114.4 4.1 %shard_map.137 = (bf16[64,2048]{1,0:T(8,128)(2,1)S(1)}, bf16[64,2048]{1,0:T(8,128)(2,1)S(1)}, bf16[64,2048]{1,0:T(8,128)(2,1)S(1)}, bf16[64,2048]{1,0:T(8,128)(2,1)S(1)}) custom-call(bf16[64,2048]{1,0:T(8,128)(2,1)S(1)} %collective-permute-done.4.refs_0_, bf16[64,2048]{1,0:T(8,128)(2,1)S(1)} %collective-permute-done.12.refs_1_, ...), custom_call_target="tpu_custom_call" | custom-call | flops 2818572288 | bytes 1048576 | tf_op jit(solution)/shard_map/pallas_call | solution.py:77
  118.9 0.6 collective-permute-start.27
  119.5 2.8 %collective-permute-start.24 = (bf16[64,2048]{1,0:T(8,128)(2,1)S(1)}, bf16[64,2048]{1,0:T(8,128)(2,1)S(1)}, u32[]{:S(2)}, u32[]{:S(2)}) collective-permute-start(bf16[64,2048]{1,0:T(8,128)(2,1)S(1)} %shard_map.140), channel_id=1, source_target_pairs={{0,14},{1,15},{2,0},{3,1},{4,2},{5,3},{6,4},{7,5},{8,6},{9,7},{10,... | collective-permute-start | bytes 786440 | tf_op jit(solution)/shard_map/ppermute | solution.py:25
  122.3 0.6 collective-permute-done.30.a
  123.0 2.7 %collective-permute-start.31 = (bf16[64,2048]{1,0:T(8,128)(2,1)S(1)}, bf16[64,2048]{1,0:T(8,128)(2,1)S(1)}, u32[]{:S(2)}, u32[]{:S(2)}) collective-permute-start(bf16[64,2048]{1,0:T(8,128)(2,1)S(1)} %shard_map.145), channel_id=1, source_target_pairs={{0,14},{1,15},{2,0},{3,1},{4,2},{5,3},{6,4},{7,5},{8,6},{9,7},{10,... | collective-permute-start | bytes 786440 | tf_op jit(solution)/shard_map/ppermute | solution.py:25
  125.9 2.7 %collective-permute-done.27.right_b = bf16[64,2048]{1,0:T(8,128)(2,1)S(1)} collective-permute-done((bf16[64,2048]{1,0:T(8,128)(2,1)S(1)}, bf16[64,2048]{1,0:T(8,128)(2,1)S(1)}, u32[]{:S(2)}, u32[]{:S(2)}) %collective-permute-start.27) | collective-permute-done | bytes 262176 | tf_op jit(solution)/shard_map/ppermute | solution.py:25
  128.5 1.1 collective-permute-done.31.left_b
  129.6 3.8 %collective-permute-done.21.right_a = bf16[64,2048]{1,0:T(8,128)(2,1)S(1)} collective-permute-done((bf16[64,2048]{1,0:T(8,128)(2,1)S(1)}, bf16[64,2048]{1,0:T(8,128)(2,1)S(1)}, u32[]{:S(2)}, u32[]{:S(2)}) %collective-permute-start.21) | collective-permute-done | bytes 262176 | tf_op jit(solution)/shard_map/ppermute | solution.py:25
  133.6 14.1 %all_to_all.17 = bf16[16,8,2048]{2,1,0:T(8,128)(2,1)S(1)} all-to-all(bf16[16,8,2048]{2,1,0:T(8,128)(2,1)S(1)} %bitcast.44), channel_id=1, replica_groups=mesh['sp'=16,'tp'=16] {'sp'}, dimensions={0} | all-to-all | bytes 1048576 | tf_op jit(solution)/shard_map/all_to_all | solution.py:389
  148.0 1.0 add_convert_fusion
  (65 shorter events, 4.6 us)
Async XLA Ops:
  1.1 6.0 %collective-permute-start = (bf16[64,128]{1,0:T(8,128)(2,1)S(1)}, bf16[64,128]{1,0:T(8,128)(2,1)S(1)}, u32[]{:S(2)}, u32[]{:S(2)}) collective-permute-start(bf16[64,128]{1,0:T(8,128)(2,1)S(1)} %slice.4), channel_id=1, source_target_pairs={{0,16},{16,32},{32,48},{48,64},{64,80},{80,96},{96,112},{112,128},... | collective-permute-start | bytes 49160 | tf_op jit(solution)/shard_map/ppermute | solution.py:20
  4.5 0.7 copy-start.5
  5.2 19.1 %copy-start.3 = (bf16[1024,2048]{1,0:T(8,128)(2,1)S(1)}, bf16[1024,2048]{1,0:T(8,128)(2,1)}, u32[]{:S(2)}) copy-start(bf16[1024,2048]{1,0:T(8,128)(2,1)} %out_weight.1) | copy-start | bytes 12582916
  5.2 19.1 %copy-start.4 = (bf16[64,2048]{1,0:T(8,128)(2,1)S(1)}, bf16[64,2048]{1,0:T(8,128)(2,1)}, u32[]{:S(2)}) copy-start(bf16[64,2048]{1,0:T(8,128)(2,1)} %stream.1) | copy-start | bytes 786436
  5.2 19.1 %copy-start.6 = (f32[2048]{0:T(1024)S(1)}, f32[2048]{0:T(1024)}, u32[]{:S(2)}) copy-start(f32[2048]{0:T(1024)} %param.22) | copy-start | bytes 24580
  5.2 19.1 %copy-start.7 = (f32[1024]{0:T(1024)S(1)}, f32[1024]{0:T(1024)}, u32[]{:S(2)}) copy-start(f32[1024]{0:T(1024)} %param.16) | copy-start | bytes 12292
  5.2 19.1 %copy-start.8 = (f32[1024]{0:T(1024)S(1)}, f32[1024]{0:T(1024)}, u32[]{:S(2)}) copy-start(f32[1024]{0:T(1024)} %param.17) | copy-start | bytes 12292
  5.2 19.1 %copy-start.9 = (s32[64,2]{0,1:T(2,128)S(1)}, s32[64,2]{0,1:T(2,128)}, u32[]{:S(2)}) copy-start(s32[64,2]{0,1:T(2,128)} %param.20) | copy-start | bytes 1540
  5.2 19.1 %copy-start.10 = (f32[64,2]{0,1:T(2,128)S(1)}, f32[64,2]{0,1:T(2,128)}, u32[]{:S(2)}) copy-start(f32[64,2]{0,1:T(2,128)} %param.21) | copy-start | bytes 1540
  24.4 1.5 %copy-start = (bf16[1,2048,448]{1,2,0:T(8,128)(2,1)S(1)}, bf16[1,2048,448]{1,2,0:T(8,128)(2,1)}, u32[]{:S(2)}) copy-start(bf16[1,2048,448]{1,2,0:T(8,128)(2,1)} %param.23) | copy-start | bytes 5505028
  24.4 2.3 %copy-start.1 = (bf16[1,2048,448]{1,2,0:T(8,128)(2,1)S(1)}, bf16[1,2048,448]{1,2,0:T(8,128)(2,1)}, u32[]{:S(2)}) copy-start(bf16[1,2048,448]{1,2,0:T(8,128)(2,1)} %param.24) | copy-start | bytes 5505028
  24.4 2.7 %copy-start.2 = (bf16[1,448,2048]{2,1,0:T(8,128)(2,1)S(1)}, bf16[1,448,2048]{2,1,0:T(8,128)(2,1)}, u32[]{:S(2)}) copy-start(bf16[1,448,2048]{2,1,0:T(8,128)(2,1)} %param.25) | copy-start | bytes 5505028
  25.9 19.0 %collective-permute-start.1 = (bf16[448,2048]{1,0:T(8,128)(2,1)S(1)}, bf16[448,2048]{1,0:T(8,128)(2,1)S(1)}, u32[]{:S(2)}, u32[]{:S(2)}) collective-permute-start(bf16[448,2048]{1,0:T(8,128)(2,1)S(1)} %bitcast.25), channel_id=1, source_target_pairs={{0,1},{1,0},{2,3},{3,2},{4,5},{5,4},{6,7},{7,6},{8,9},{9,8},{10,11... | collective-permute-start | bytes 5505032 | tf_op jit(solution)/shard_map/ppermute | solution.py:30
  26.6 18.3 %collective-permute-start.2 = (bf16[448,2048]{1,0:T(8,128)(2,1)S(1)}, bf16[448,2048]{1,0:T(8,128)(2,1)S(1)}, u32[]{:S(2)}, u32[]{:S(2)}) collective-permute-start(bf16[448,2048]{1,0:T(8,128)(2,1)S(1)} %bitcast.31), channel_id=1, source_target_pairs={{0,1},{1,0},{2,3},{3,2},{4,5},{5,4},{6,7},{7,6},{8,9},{9,8},{10,11... | collective-permute-start | bytes 5505032 | tf_op jit(solution)/shard_map/ppermute | solution.py:30
  27.1 17.9 %collective-permute-start.3 = (bf16[448,2048]{1,0:T(8,128)(2,1)S(1)}, bf16[448,2048]{1,0:T(8,128)(2,1)S(1)}, u32[]{:S(2)}, u32[]{:S(2)}) collective-permute-start(bf16[448,2048]{1,0:T(8,128)(2,1)S(1)} %bitcast.37), channel_id=1, source_target_pairs={{0,1},{1,0},{2,3},{3,2},{4,5},{5,4},{6,7},{7,6},{8,9},{9,8},{10,11... | collective-permute-start | bytes 5505032 | tf_op jit(solution)/shard_map/ppermute | solution.py:30
  45.0 9.3 %collective-permute-start.8 = (bf16[64,2048]{1,0:T(8,128)(2,1)S(1)}, bf16[64,2048]{1,0:T(8,128)(2,1)S(1)}, u32[]{:S(2)}, u32[]{:S(2)}) collective-permute-start(bf16[64,2048]{1,0:T(8,128)(2,1)S(1)} %get-tuple-element.47.refs_1_), channel_id=1, source_target_pairs={{0,14},{1,15},{2,0},{3,1},{4,2},{5,3},{6,4},{7,5},{8,6},{9,7},{10,... | collective-permute-start | bytes 786440 | tf_op jit(solution)/shard_map/ppermute | solution.py:25
  45.4 10.4 %collective-permute-start.4 = (bf16[64,2048]{1,0:T(8,128)(2,1)S(1)}, bf16[64,2048]{1,0:T(8,128)(2,1)S(1)}, u32[]{:S(2)}, u32[]{:S(2)}) collective-permute-start(bf16[64,2048]{1,0:T(8,128)(2,1)S(1)} %get-tuple-element.46.refs_0_), channel_id=1, source_target_pairs={{0,2},{1,3},{2,4},{3,5},{4,6},{5,7},{6,8},{7,9},{8,10},{9,11},{10,... | collective-permute-start | bytes 786440 | tf_op jit(solution)/shard_map/ppermute | solution.py:25
  47.1 14.3 %collective-permute-start.12 = (bf16[64,2048]{1,0:T(8,128)(2,1)S(1)}, bf16[64,2048]{1,0:T(8,128)(2,1)S(1)}, u32[]{:S(2)}, u32[]{:S(2)}) collective-permute-start(bf16[64,2048]{1,0:T(8,128)(2,1)S(1)} %get-tuple-element.47.refs_1_), channel_id=1, source_target_pairs={{0,2},{1,3},{2,4},{3,5},{4,6},{5,7},{6,8},{7,9},{8,10},{9,11},{10,... | collective-permute-start | bytes 786440 | tf_op jit(solution)/shard_map/ppermute | solution.py:25
  47.6 14.2 %collective-permute-start.15 = (bf16[64,2048]{1,0:T(8,128)(2,1)S(1)}, bf16[64,2048]{1,0:T(8,128)(2,1)S(1)}, u32[]{:S(2)}, u32[]{:S(2)}) collective-permute-start(bf16[64,2048]{1,0:T(8,128)(2,1)S(1)} %get-tuple-element.46.refs_0_), channel_id=1, source_target_pairs={{0,14},{1,15},{2,0},{3,1},{4,2},{5,3},{6,4},{7,5},{8,6},{9,7},{10,... | collective-permute-start | bytes 786440 | tf_op jit(solution)/shard_map/ppermute | solution.py:25
  54.2 13.7 %collective-permute-start.9 = (bf16[64,2048]{1,0:T(8,128)(2,1)S(1)}, bf16[64,2048]{1,0:T(8,128)(2,1)S(1)}, u32[]{:S(2)}, u32[]{:S(2)}) collective-permute-start(bf16[64,2048]{1,0:T(8,128)(2,1)S(1)} %collective-permute-done.8.refs_3_), channel_id=1, source_target_pairs={{0,14},{1,15},{2,0},{3,1},{4,2},{5,3},{6,4},{7,5},{8,6},{9,7},{10,... | collective-permute-start | bytes 786440 | tf_op jit(solution)/shard_map/ppermute | solution.py:25
  55.8 12.3 %collective-permute-start.5 = (bf16[64,2048]{1,0:T(8,128)(2,1)S(1)}, bf16[64,2048]{1,0:T(8,128)(2,1)S(1)}, u32[]{:S(2)}, u32[]{:S(2)}) collective-permute-start(bf16[64,2048]{1,0:T(8,128)(2,1)S(1)} %collective-permute-done.4.refs_0_), channel_id=1, source_target_pairs={{0,2},{1,3},{2,4},{3,5},{4,6},{5,7},{6,8},{7,9},{8,10},{9,11},{10,... | collective-permute-start | bytes 786440 | tf_op jit(solution)/shard_map/ppermute | solution.py:25
  61.4 11.2 %collective-permute-start.13 = (bf16[64,2048]{1,0:T(8,128)(2,1)S(1)}, bf16[64,2048]{1,0:T(8,128)(2,1)S(1)}, u32[]{:S(2)}, u32[]{:S(2)}) collective-permute-start(bf16[64,2048]{1,0:T(8,128)(2,1)S(1)} %collective-permute-done.12.refs_1_), channel_id=1, source_target_pairs={{0,2},{1,3},{2,4},{3,5},{4,6},{5,7},{6,8},{7,9},{8,10},{9,11},{10,... | collective-permute-start | bytes 786440 | tf_op jit(solution)/shard_map/ppermute | solution.py:25
  61.9 11.2 %collective-permute-start.16 = (bf16[64,2048]{1,0:T(8,128)(2,1)S(1)}, bf16[64,2048]{1,0:T(8,128)(2,1)S(1)}, u32[]{:S(2)}, u32[]{:S(2)}) collective-permute-start(bf16[64,2048]{1,0:T(8,128)(2,1)S(1)} %collective-permute-done.15.refs_2_), channel_id=1, source_target_pairs={{0,14},{1,15},{2,0},{3,1},{4,2},{5,3},{6,4},{7,5},{8,6},{9,7},{10,... | collective-permute-start | bytes 786440 | tf_op jit(solution)/shard_map/ppermute | solution.py:25
  68.0 12.0 %collective-permute-start.10 = (bf16[64,2048]{1,0:T(8,128)(2,1)S(1)}, bf16[64,2048]{1,0:T(8,128)(2,1)S(1)}, u32[]{:S(2)}, u32[]{:S(2)}) collective-permute-start(bf16[64,2048]{1,0:T(8,128)(2,1)S(1)} %collective-permute-done.9.refs_3_), channel_id=1, source_target_pairs={{0,14},{1,15},{2,0},{3,1},{4,2},{5,3},{6,4},{7,5},{8,6},{9,7},{10,... | collective-permute-start | bytes 786440 | tf_op jit(solution)/shard_map/ppermute | solution.py:25
  68.1 12.0 %collective-permute-start.6 = (bf16[64,2048]{1,0:T(8,128)(2,1)S(1)}, bf16[64,2048]{1,0:T(8,128)(2,1)S(1)}, u32[]{:S(2)}, u32[]{:S(2)}) collective-permute-start(bf16[64,2048]{1,0:T(8,128)(2,1)S(1)} %collective-permute-done.5.refs_0_), channel_id=1, source_target_pairs={{0,2},{1,3},{2,4},{3,5},{4,6},{5,7},{6,8},{7,9},{8,10},{9,11},{10,... | collective-permute-start | bytes 786440 | tf_op jit(solution)/shard_map/ppermute | solution.py:25
  72.6 11.4 %collective-permute-start.14 = (bf16[64,2048]{1,0:T(8,128)(2,1)S(1)}, bf16[64,2048]{1,0:T(8,128)(2,1)S(1)}, u32[]{:S(2)}, u32[]{:S(2)}) collective-permute-start(bf16[64,2048]{1,0:T(8,128)(2,1)S(1)} %collective-permute-done.13.refs_1_), channel_id=1, source_target_pairs={{0,2},{1,3},{2,4},{3,5},{4,6},{5,7},{6,8},{7,9},{8,10},{9,11},{10,... | collective-permute-start | bytes 786440 | tf_op jit(solution)/shard_map/ppermute | solution.py:25
  73.1 11.0 %collective-permute-start.17 = (bf16[64,2048]{1,0:T(8,128)(2,1)S(1)}, bf16[64,2048]{1,0:T(8,128)(2,1)S(1)}, u32[]{:S(2)}, u32[]{:S(2)}) collective-permute-start(bf16[64,2048]{1,0:T(8,128)(2,1)S(1)} %collective-permute-done.16.refs_2_), channel_id=1, source_target_pairs={{0,14},{1,15},{2,0},{3,1},{4,2},{5,3},{6,4},{7,5},{8,6},{9,7},{10,... | collective-permute-start | bytes 786440 | tf_op jit(solution)/shard_map/ppermute | solution.py:25
  80.0 8.2 %collective-permute-start.11 = (bf16[64,2048]{1,0:T(8,128)(2,1)S(1)}, bf16[64,2048]{1,0:T(8,128)(2,1)S(1)}, u32[]{:S(2)}, u32[]{:S(2)}) collective-permute-start(bf16[64,2048]{1,0:T(8,128)(2,1)S(1)} %collective-permute-done.10.refs_3_), channel_id=1, source_target_pairs={{0,14},{1,15},{2,0},{3,1},{4,2},{5,3},{6,4},{7,5},{8,6},{9,7},{10,... | collective-permute-start | bytes 786440 | tf_op jit(solution)/shard_map/ppermute | solution.py:25
  80.1 8.1 %collective-permute-start.7 = (bf16[64,2048]{1,0:T(8,128)(2,1)S(1)}, bf16[64,2048]{1,0:T(8,128)(2,1)S(1)}, u32[]{:S(2)}, u32[]{:S(2)}) collective-permute-start(bf16[64,2048]{1,0:T(8,128)(2,1)S(1)} %collective-permute-done.6.refs_0_), channel_id=1, source_target_pairs={{0,2},{1,3},{2,4},{3,5},{4,6},{5,7},{6,8},{7,9},{8,10},{9,11},{10,... | collective-permute-start | bytes 786440 | tf_op jit(solution)/shard_map/ppermute | solution.py:25
  91.5 9.3 %collective-permute-start.28 = (bf16[64,2048]{1,0:T(8,128)(2,1)S(1)}, bf16[64,2048]{1,0:T(8,128)(2,1)S(1)}, u32[]{:S(2)}, u32[]{:S(2)}) collective-permute-start(bf16[64,2048]{1,0:T(8,128)(2,1)S(1)} %get-tuple-element.65), channel_id=1, source_target_pairs={{0,14},{1,15},{2,0},{3,1},{4,2},{5,3},{6,4},{7,5},{8,6},{9,7},{10,... | collective-permute-start | bytes 786440 | tf_op jit(solution)/shard_map/ppermute | solution.py:25
  91.9 10.5 %collective-permute-start.18 = (bf16[64,2048]{1,0:T(8,128)(2,1)S(1)}, bf16[64,2048]{1,0:T(8,128)(2,1)S(1)}, u32[]{:S(2)}, u32[]{:S(2)}) collective-permute-start(bf16[64,2048]{1,0:T(8,128)(2,1)S(1)} %get-tuple-element.57.refs_10_), channel_id=1, source_target_pairs={{0,2},{1,3},{2,4},{3,5},{4,6},{5,7},{6,8},{7,9},{8,10},{9,11},{10,... | collective-permute-start | bytes 786440 | tf_op jit(solution)/shard_map/ppermute | solution.py:25
  93.6 13.9 %collective-permute-start.25 = (bf16[64,2048]{1,0:T(8,128)(2,1)S(1)}, bf16[64,2048]{1,0:T(8,128)(2,1)S(1)}, u32[]{:S(2)}, u32[]{:S(2)}) collective-permute-start(bf16[64,2048]{1,0:T(8,128)(2,1)S(1)} %get-tuple-element.62), channel_id=1, source_target_pairs={{0,2},{1,3},{2,4},{3,5},{4,6},{5,7},{6,8},{7,9},{8,10},{9,11},{10,... | collective-permute-start | bytes 786440 | tf_op jit(solution)/shard_map/ppermute | solution.py:25
  94.1 14.1 %collective-permute-start.22 = (bf16[64,2048]{1,0:T(8,128)(2,1)S(1)}, bf16[64,2048]{1,0:T(8,128)(2,1)S(1)}, u32[]{:S(2)}, u32[]{:S(2)}) collective-permute-start(bf16[64,2048]{1,0:T(8,128)(2,1)S(1)} %get-tuple-element.56.refs_8_), channel_id=1, source_target_pairs={{0,14},{1,15},{2,0},{3,1},{4,2},{5,3},{6,4},{7,5},{8,6},{9,7},{10,... | collective-permute-start | bytes 786440 | tf_op jit(solution)/shard_map/ppermute | solution.py:25
  100.9 11.2 %collective-permute-start.29 = (bf16[64,2048]{1,0:T(8,128)(2,1)S(1)}, bf16[64,2048]{1,0:T(8,128)(2,1)S(1)}, u32[]{:S(2)}, u32[]{:S(2)}) collective-permute-start(bf16[64,2048]{1,0:T(8,128)(2,1)S(1)} %shard_map.143), channel_id=1, source_target_pairs={{0,14},{1,15},{2,0},{3,1},{4,2},{5,3},{6,4},{7,5},{8,6},{9,7},{10,... | collective-permute-start | bytes 786440 | tf_op jit(solution)/shard_map/ppermute | solution.py:25
  102.5 11.2 %collective-permute-start.19 = (bf16[64,2048]{1,0:T(8,128)(2,1)S(1)}, bf16[64,2048]{1,0:T(8,128)(2,1)S(1)}, u32[]{:S(2)}, u32[]{:S(2)}) collective-permute-start(bf16[64,2048]{1,0:T(8,128)(2,1)S(1)} %shard_map.135), channel_id=1, source_target_pairs={{0,2},{1,3},{2,4},{3,5},{4,6},{5,7},{6,8},{7,9},{8,10},{9,11},{10,... | collective-permute-start | bytes 786440 | tf_op jit(solution)/shard_map/ppermute | solution.py:25
  107.6 11.2 %collective-permute-start.26 = (bf16[64,2048]{1,0:T(8,128)(2,1)S(1)}, bf16[64,2048]{1,0:T(8,128)(2,1)S(1)}, u32[]{:S(2)}, u32[]{:S(2)}) collective-permute-start(bf16[64,2048]{1,0:T(8,128)(2,1)S(1)} %shard_map.141), channel_id=1, source_target_pairs={{0,2},{1,3},{2,4},{3,5},{4,6},{5,7},{6,8},{7,9},{8,10},{9,11},{10,... | collective-permute-start | bytes 786440 | tf_op jit(solution)/shard_map/ppermute | solution.py:25
  108.3 11.2 %collective-permute-start.23 = (bf16[64,2048]{1,0:T(8,128)(2,1)S(1)}, bf16[64,2048]{1,0:T(8,128)(2,1)S(1)}, u32[]{:S(2)}, u32[]{:S(2)}) collective-permute-start(bf16[64,2048]{1,0:T(8,128)(2,1)S(1)} %shard_map.139), channel_id=1, source_target_pairs={{0,14},{1,15},{2,0},{3,1},{4,2},{5,3},{6,4},{7,5},{8,6},{9,7},{10,... | collective-permute-start | bytes 786440 | tf_op jit(solution)/shard_map/ppermute | solution.py:25
  112.1 10.9 %collective-permute-start.30 = (bf16[64,2048]{1,0:T(8,128)(2,1)S(1)}, bf16[64,2048]{1,0:T(8,128)(2,1)S(1)}, u32[]{:S(2)}, u32[]{:S(2)}) collective-permute-start(bf16[64,2048]{1,0:T(8,128)(2,1)S(1)} %shard_map.144), channel_id=1, source_target_pairs={{0,14},{1,15},{2,0},{3,1},{4,2},{5,3},{6,4},{7,5},{8,6},{9,7},{10,... | collective-permute-start | bytes 786440 | tf_op jit(solution)/shard_map/ppermute | solution.py:25
  113.7 12.0 %collective-permute-start.20 = (bf16[64,2048]{1,0:T(8,128)(2,1)S(1)}, bf16[64,2048]{1,0:T(8,128)(2,1)S(1)}, u32[]{:S(2)}, u32[]{:S(2)}) collective-permute-start(bf16[64,2048]{1,0:T(8,128)(2,1)S(1)} %shard_map.136), channel_id=1, source_target_pairs={{0,2},{1,3},{2,4},{3,5},{4,6},{5,7},{6,8},{7,9},{8,10},{9,11},{10,... | collective-permute-start | bytes 786440 | tf_op jit(solution)/shard_map/ppermute | solution.py:25
  118.9 9.7 %collective-permute-start.27 = (bf16[64,2048]{1,0:T(8,128)(2,1)S(1)}, bf16[64,2048]{1,0:T(8,128)(2,1)S(1)}, u32[]{:S(2)}, u32[]{:S(2)}) collective-permute-start(bf16[64,2048]{1,0:T(8,128)(2,1)S(1)} %shard_map.142), channel_id=1, source_target_pairs={{0,2},{1,3},{2,4},{3,5},{4,6},{5,7},{6,8},{7,9},{8,10},{9,11},{10,... | collective-permute-start | bytes 786440 | tf_op jit(solution)/shard_map/ppermute | solution.py:25
  119.5 9.0 %collective-permute-start.24 = (bf16[64,2048]{1,0:T(8,128)(2,1)S(1)}, bf16[64,2048]{1,0:T(8,128)(2,1)S(1)}, u32[]{:S(2)}, u32[]{:S(2)}) collective-permute-start(bf16[64,2048]{1,0:T(8,128)(2,1)S(1)} %shard_map.140), channel_id=1, source_target_pairs={{0,14},{1,15},{2,0},{3,1},{4,2},{5,3},{6,4},{7,5},{8,6},{9,7},{10,... | collective-permute-start | bytes 786440 | tf_op jit(solution)/shard_map/ppermute | solution.py:25
  123.0 6.6 %collective-permute-start.31 = (bf16[64,2048]{1,0:T(8,128)(2,1)S(1)}, bf16[64,2048]{1,0:T(8,128)(2,1)S(1)}, u32[]{:S(2)}, u32[]{:S(2)}) collective-permute-start(bf16[64,2048]{1,0:T(8,128)(2,1)S(1)} %shard_map.145), channel_id=1, source_target_pairs={{0,14},{1,15},{2,0},{3,1},{4,2},{5,3},{6,4},{7,5},{8,6},{9,7},{10,... | collective-permute-start | bytes 786440 | tf_op jit(solution)/shard_map/ppermute | solution.py:25
  125.8 7.7 %collective-permute-start.21 = (bf16[64,2048]{1,0:T(8,128)(2,1)S(1)}, bf16[64,2048]{1,0:T(8,128)(2,1)S(1)}, u32[]{:S(2)}, u32[]{:S(2)}) collective-permute-start(bf16[64,2048]{1,0:T(8,128)(2,1)S(1)} %shard_map.138), channel_id=1, source_target_pairs={{0,2},{1,3},{2,4},{3,5},{4,6},{5,7},{6,8},{7,9},{8,10},{9,11},{10,... | collective-permute-start | bytes 786440 | tf_op jit(solution)/shard_map/ppermute | solution.py:25

commit v5 on v4

--- a/solution.py
+++ b/solution.py
@@ -5,6 +5,7 @@
 from jax.experimental import pallas as pl
 from jax.experimental.pallas import tpu as pltpu
 from jax.sharding import PartitionSpec as P
+
 
 epsilon = 1e-06
 f32 = jnp.float32
@@ -342,12 +343,11 @@
         routes.T,
         route_weights.T,
     )
-    mine = (expert_gate[0].T, expert_up[0].T, expert_down[0])
-    send_rows, gone = lax.optimization_barrier((send_rows, mine))
-    weights = [w for pair in zip(mine, map(other_core, gone)) for w in pair]
     send_rows = send_rows.reshape(experts, capacity, width)
     received = lax.all_to_all(send_rows, "sp", split_axis=0, concat_axis=0, tiled=True)
-    received, weights = lax.optimization_barrier((received, weights))
+    weights = []
+    for mine in (expert_gate[0].T, expert_up[0].T, expert_down[0]):
+        weights += [mine, other_core(mine)]
     own = received.reshape(-1, width)
 
     far = lax.axis_size("tp") // 4
@@ -363,9 +363,8 @@
         from_left[k] = (left_a, left_b)
         from_right[k] = (right_a, right_b)
 
-    part_own = expert(from_left[0], weights)
     part_left, part_right = {}, {}
-    token = part_own[0]
+    token = None
     for k in range(2, far):
         parts = expert((*from_left[k], *from_right[k]), weights, token)
         part_left[k], part_right[k] = parts[0:2], parts[2:4]
@@ -378,6 +377,7 @@
     left_b = z_shift(antipode[1], -1)
     parts = expert((*from_left[1], *from_right[1]), weights, antipode[0])
     part_left[1], part_right[1] = parts[0:2], parts[2:4]
+    part_own = expert(from_left[0], weights, parts[0])
     for k in range(far - 1, 0, -1):
         if k < far - 1:
             right_b = z_shift(add(right_b, part_right[k][1]), 1)

time: 149 us -> 173 us (1.16)
  blocking collectives: 48.4 us -> 31.3 us
  Pallas kernels: 23.3 us -> 37.6 us
  waiting for transfers between devices: 32.1 us -> 44.7 us
  starting transfers between devices: 41.8 us -> 53.4 us
  local copies, waits for them, and re-layouts: 0.77 us -> 2.94 us
    all_to_all x1 -> x0, blocking collectives: 17 us -> none  [per_device(): lax.all_to_all(conv_out, 'tp', split_axis=0, concat_axis=0, tiled=True)]
    pallas_call x5, Pallas kernels: 19 us -> 32 us  [expert(): pl.pallas_call(functools.partial(expert_kernel, sizes, hidden // 2, len(t...]
    all_to_all x0 -> x1, starting transfers between devices: none -> 8.57 us  [per_device(): lax.all_to_all(conv_out, 'tp', split_axis=0, concat_axis=0, tiled=True)]
    all_to_all x0 -> x1, waiting for transfers between devices: none -> 7.72 us  [per_device(): lax.all_to_all(conv_out, 'tp', split_axis=0, concat_axis=0, tiled=True)]
    ppermute x28, waiting for transfers between devices: 32.1 us -> 36.9 us  [z_shift(): lax.ppermute(value, 'tp', [(i, (i + 2 * steps) % count) for i in range(co...]
    ppermute x28, starting transfers between devices: 36.7 us -> 40.5 us  [z_shift(): lax.ppermute(value, 'tp', [(i, (i + 2 * steps) % count) for i in range(co...]
    unnamed x22, local copies, waits for them, and re-layouts: 0.77 us -> 2.94 us
  transfers between devices with their start and end apart: 32 -> 33, of which waited for: 13 -> 13; matrix products, arithmetic and copies ran while one was open for 0% -> 0% of each run, Pallas kernels for 12% -> 18%
where the time goes in v5:
time: 173 us
  starting transfers between devices  53.4 us (31%)
  waiting for transfers between devices  44.7 us (26%)
  Pallas kernels  37.6 us (22%)
  blocking collectives  31.3 us (18%)
  local copies, waits for them, and re-layouts  2.94 us (2%)
    ppermute x28, starting transfers between devices, z_shift(): lax.ppermute(value, 'tp', [(i, (i + 2 * steps) % count) for i in range(co...  40.5 us
    ppermute x28, waiting for transfers between devices, z_shift(): lax.ppermute(value, 'tp', [(i, (i + 2 * steps) % count) for i in range(co...  36.9 us
    pallas_call x5, Pallas kernels, expert(): pl.pallas_call(functools.partial(expert_kernel, sizes, hidden // 2, len(t...  32 us
    all_to_all x1, blocking collectives, per_device(): lax.all_to_all(send_rows, 'sp', split_axis=0, concat_axis=0, tiled=True)  18 us
    all_to_all x1, blocking collectives, per_device(): lax.all_to_all(result, 'sp', split_axis=0, concat_axis=0, tiled=True)  13.4 us
    all_to_all x1, starting transfers between devices, per_device(): lax.all_to_all(conv_out, 'tp', split_axis=0, concat_axis=0, tiled=True)  8.57 us
    all_to_all x1, waiting for transfers between devices, per_device(): lax.all_to_all(conv_out, 'tp', split_axis=0, concat_axis=0, tiled=True)  7.72 us
  transfers between devices with their start and end apart: 33, of which 13 were waited for; matrix products, arithmetic and copies ran while one was open for 0% of the time, Pallas kernels for 18%

profile of v5, /device:TPU:2, one launch (start us, length us, event | category | flops | bytes accessed | tf_op | source)
XLA Modules:
  0.0 172.6 jit_solution(6096380803127056751)
XLA Ops:
  0.0 1.0 multiply_convert_fusion.line
  1.1 3.4 %collective-permute-start = (bf16[64,128]{1,0:T(8,128)(2,1)S(1)}, bf16[64,128]{1,0:T(8,128)(2,1)S(1)}, u32[]{:S(2)}, u32[]{:S(2)}) collective-permute-start(bf16[64,128]{1,0:T(8,128)(2,1)S(1)} %slice.4), channel_id=1, source_target_pairs={{0,16},{16,32},{32,48},{48,64},{64,80},{80,96},{96,112},{112,128},... | collective-permute-start | bytes 49160 | tf_op jit(solution)/shard_map/ppermute | solution.py:21
  4.5 0.7 copy-done.5
  5.2 2.5 %shard_map.127._ = bf16[16,32,128]{2,1,0:T(8,128)(2,1)} custom-call(bf16[64,1024]{1,0:T(8,128)(2,1)S(1)} %multiply_convert_fusion.line, f32[31,64]{1,0:T(8,128)S(1)} %bitcast.46), custom_call_target="tpu_custom_call" | custom-call | flops 1342177280 | bytes 1048576 | tf_op jit(solution)/shard_map/pallas_call | solution.py:145
  7.7 0.8 shard_map.128
  8.5 8.6 %all-to-all-start = ((bf16[16,32,128]{2,1,0:T(8,128)(2,1)}), bf16[16,32,128]{2,1,0:T(8,128)(2,1)S(1)}, u32[]{:S(2)}, u32[]{:S(2)}) async-start(bf16[16,32,128]{2,1,0:T(8,128)(2,1)} %shard_map.128), calls=%async_computation | async-start | bytes 262144 | tf_op jit(solution)/shard_map/all_to_all | solution.py:335
  17.1 0.4 collective-permute-start.10
  17.7 0.3 collective-permute-start.9
  18.0 7.7 %all-to-all-done.conv = bf16[16,32,128]{2,1,0:T(8,128)(2,1)S(1)} async-done(((bf16[16,32,128]{2,1,0:T(8,128)(2,1)}), bf16[16,32,128]{2,1,0:T(8,128)(2,1)S(1)}, u32[]{:S(2)}, u32[]{:S(2)}) %all-to-all-start) | async-done | bytes 131104 | tf_op jit(solution)/shard_map/all_to_all | solution.py:335
  25.8 2.2 %copy-done.3 = bf16[1024,2048]{1,0:T(8,128)(2,1)S(1)} copy-done((bf16[1024,2048]{1,0:T(8,128)(2,1)S(1)}, bf16[1024,2048]{1,0:T(8,128)(2,1)}, u32[]{:S(2)}) %copy-start.3) | copy-done | bytes 4194328
  28.0 1.5 shard_map.129
  29.5 18.0 %all_to_all.15 = bf16[16,8,2048]{2,1,0:T(8,128)(2,1)S(1)} all-to-all(bf16[16,8,2048]{2,1,0:T(8,128)(2,1)S(1)} %bitcast.45), channel_id=1, replica_groups=mesh['sp'=16,'tp'=16] {'sp'}, dimensions={0} | all-to-all | bytes 1048576 | tf_op jit(solution)/shard_map/all_to_all | solution.py:347
  47.5 0.6 collective-permute-start.12
  48.1 2.7 %collective-permute-start.15 = (bf16[64,2048]{1,0:T(8,128)(2,1)S(1)}, bf16[64,2048]{1,0:T(8,128)(2,1)S(1)}, u32[]{:S(2)}, u32[]{:S(2)}) collective-permute-start(bf16[64,2048]{1,0:T(8,128)(2,1)S(1)} %get-tuple-element.30.refs_0_), channel_id=1, source_target_pairs={{0,14},{1,15},{2,0},{3,1},{4,2},{5,3},{6,4},{7,5},{8,6},{9,7},{10,... | collective-permute-start | bytes 786440 | tf_op jit(solution)/shard_map/ppermute | solution.py:26
  50.8 5.4 %collective-permute-done.12.refs_1_ = bf16[64,2048]{1,0:T(8,128)(2,1)S(1)} collective-permute-done((bf16[64,2048]{1,0:T(8,128)(2,1)S(1)}, bf16[64,2048]{1,0:T(8,128)(2,1)S(1)}, u32[]{:S(2)}, u32[]{:S(2)}) %collective-permute-start.12) | collective-permute-done | bytes 262176 | tf_op jit(solution)/shard_map/ppermute | solution.py:26
  56.2 3.2 %collective-permute-start.5 = (bf16[64,2048]{1,0:T(8,128)(2,1)S(1)}, bf16[64,2048]{1,0:T(8,128)(2,1)S(1)}, u32[]{:S(2)}, u32[]{:S(2)}) collective-permute-start(bf16[64,2048]{1,0:T(8,128)(2,1)S(1)} %get-tuple-element.31.refs_1_), channel_id=1, source_target_pairs={{0,14},{1,15},{2,0},{3,1},{4,2},{5,3},{6,4},{7,5},{8,6},{9,7},{10,... | collective-permute-start | bytes 786440 | tf_op jit(solution)/shard_map/ppermute | solution.py:26
  59.4 4.5 %collective-permute-done.1.refs_0_ = bf16[64,2048]{1,0:T(8,128)(2,1)S(1)} collective-permute-done((bf16[64,2048]{1,0:T(8,128)(2,1)S(1)}, bf16[64,2048]{1,0:T(8,128)(2,1)S(1)}, u32[]{:S(2)}, u32[]{:S(2)}) %collective-permute-start.1) | collective-permute-done | bytes 262176 | tf_op jit(solution)/shard_map/ppermute | solution.py:26
  64.0 3.2 %collective-permute-start.16 = (bf16[64,2048]{1,0:T(8,128)(2,1)S(1)}, bf16[64,2048]{1,0:T(8,128)(2,1)S(1)}, u32[]{:S(2)}, u32[]{:S(2)}) collective-permute-start(bf16[64,2048]{1,0:T(8,128)(2,1)S(1)} %collective-permute-done.15.refs_2_), channel_id=1, source_target_pairs={{0,14},{1,15},{2,0},{3,1},{4,2},{5,3},{6,4},{7,5},{8,6},{9,7},{10,... | collective-permute-start | bytes 786440 | tf_op jit(solution)/shard_map/ppermute | solution.py:26
  67.2 4.3 %collective-permute-done.13.refs_1_ = bf16[64,2048]{1,0:T(8,128)(2,1)S(1)} collective-permute-done((bf16[64,2048]{1,0:T(8,128)(2,1)S(1)}, bf16[64,2048]{1,0:T(8,128)(2,1)S(1)}, u32[]{:S(2)}, u32[]{:S(2)}) %collective-permute-start.13) | collective-permute-done | bytes 262176 | tf_op jit(solution)/shard_map/ppermute | solution.py:26
  71.5 3.4 %collective-permute-start.6 = (bf16[64,2048]{1,0:T(8,128)(2,1)S(1)}, bf16[64,2048]{1,0:T(8,128)(2,1)S(1)}, u32[]{:S(2)}, u32[]{:S(2)}) collective-permute-start(bf16[64,2048]{1,0:T(8,128)(2,1)S(1)} %collective-permute-done.5.refs_3_), channel_id=1, source_target_pairs={{0,14},{1,15},{2,0},{3,1},{4,2},{5,3},{6,4},{7,5},{8,6},{9,7},{10,... | collective-permute-start | bytes 786440 | tf_op jit(solution)/shard_map/ppermute | solution.py:26
  74.9 5.2 %collective-permute-done.2.refs_0_ = bf16[64,2048]{1,0:T(8,128)(2,1)S(1)} collective-permute-done((bf16[64,2048]{1,0:T(8,128)(2,1)S(1)}, bf16[64,2048]{1,0:T(8,128)(2,1)S(1)}, u32[]{:S(2)}, u32[]{:S(2)}) %collective-permute-start.2) | collective-permute-done | bytes 262176 | tf_op jit(solution)/shard_map/ppermute | solution.py:26
  80.1 3.6 %collective-permute-start.7 = (bf16[64,2048]{1,0:T(8,128)(2,1)S(1)}, bf16[64,2048]{1,0:T(8,128)(2,1)S(1)}, u32[]{:S(2)}, u32[]{:S(2)}) collective-permute-start(bf16[64,2048]{1,0:T(8,128)(2,1)S(1)} %collective-permute-done.6.refs_3_), channel_id=1, source_target_pairs={{0,14},{1,15},{2,0},{3,1},{4,2},{5,3},{6,4},{7,5},{8,6},{9,7},{10,... | collective-permute-start | bytes 786440 | tf_op jit(solution)/shard_map/ppermute | solution.py:26
  83.8 6.1 %collective-permute-done.3.refs_0_ = bf16[64,2048]{1,0:T(8,128)(2,1)S(1)} collective-permute-done((bf16[64,2048]{1,0:T(8,128)(2,1)S(1)}, bf16[64,2048]{1,0:T(8,128)(2,1)S(1)}, u32[]{:S(2)}, u32[]{:S(2)}) %collective-permute-start.3) | collective-permute-done | bytes 262176 | tf_op jit(solution)/shard_map/ppermute | solution.py:26
  90.1 3.7 %collective-permute-start.17 = (bf16[64,2048]{1,0:T(8,128)(2,1)S(1)}, bf16[64,2048]{1,0:T(8,128)(2,1)S(1)}, u32[]{:S(2)}, u32[]{:S(2)}) collective-permute-start(bf16[64,2048]{1,0:T(8,128)(2,1)S(1)} %collective-permute-done.16.refs_2_), channel_id=1, source_target_pairs={{0,14},{1,15},{2,0},{3,1},{4,2},{5,3},{6,4},{7,5},{8,6},{9,7},{10,... | collective-permute-start | bytes 786440 | tf_op jit(solution)/shard_map/ppermute | solution.py:26
  93.8 3.2 %collective-permute-start.8 = (bf16[64,2048]{1,0:T(8,128)(2,1)S(1)}, bf16[64,2048]{1,0:T(8,128)(2,1)S(1)}, u32[]{:S(2)}, u32[]{:S(2)}) collective-permute-start(bf16[64,2048]{1,0:T(8,128)(2,1)S(1)} %collective-permute-done.7.refs_3_), channel_id=1, source_target_pairs={{0,14},{1,15},{2,0},{3,1},{4,2},{5,3},{6,4},{7,5},{8,6},{9,7},{10,... | collective-permute-start | bytes 786440 | tf_op jit(solution)/shard_map/ppermute | solution.py:26
  97.0 6.7 %shard_map.131 = (bf16[64,2048]{1,0:T(8,128)(2,1)S(1)}, bf16[64,2048]{1,0:T(8,128)(2,1)S(1)}, bf16[64,2048]{1,0:T(8,128)(2,1)S(1)}, bf16[64,2048]{1,0:T(8,128)(2,1)S(1)}) custom-call(bf16[64,2048]{1,0:T(8,128)(2,1)S(1)} %collective-permute-done.2.refs_0_, bf16[64,2048]{1,0:T(8,128)(2,1)S(1)} %collective-permute-done.13.refs_1_, ...), custom_call_target="tpu_custom_call" | custom-call | flops 2818572288 | bytes 1048576 | tf_op jit(solution)/shard_map/pallas_call | solution.py:78
  103.8 6.7 %shard_map.132 = (bf16[64,2048]{1,0:T(8,128)(2,1)S(1)}, bf16[64,2048]{1,0:T(8,128)(2,1)S(1)}, bf16[64,2048]{1,0:T(8,128)(2,1)S(1)}, bf16[64,2048]{1,0:T(8,128)(2,1)S(1)}) custom-call(bf16[64,2048]{1,0:T(8,128)(2,1)S(1)} %collective-permute-done.3.refs_0_, bf16[64,2048]{1,0:T(8,128)(2,1)S(1)} %collective-permute-done.14.refs_1_, ...), custom_call_target="tpu_custom_call" | custom-call | flops 2818572288 | bytes 1048576 | tf_op jit(solution)/shard_map/pallas_call | solution.py:78
  110.5 5.9 %shard_map.133 = (bf16[64,2048]{1,0:T(8,128)(2,1)S(1)}, bf16[64,2048]{1,0:T(8,128)(2,1)S(1)}) custom-call(bf16[64,2048]{1,0:T(8,128)(2,1)S(1)} %collective-permute-done.4.refs_0_, bf16[64,2048]{1,0:T(8,128)(2,1)S(1)} %collective-permute-done.8.refs_1_, bf16[448,2048]{1,0:T(8,128)(2,1)S(1)} %bitcast.28, ...), custom_call_target="tpu_custom_call" | custom-call | flops 1409286144 | bytes 1048576 | tf_op jit(solution)/shard_map/pallas_call | solution.py:78
  116.5 2.0 %collective-permute-start.18 = (bf16[64,2048]{1,0:T(8,128)(2,1)S(1)}, bf16[64,2048]{1,0:T(8,128)(2,1)S(1)}, u32[]{:S(2)}, u32[]{:S(2)}) collective-permute-start(bf16[64,2048]{1,0:T(8,128)(2,1)S(1)} %get-tuple-element.34.refs_10_), channel_id=1, source_target_pairs={{0,2},{1,3},{2,4},{3,5},{4,6},{5,7},{6,8},{7,9},{8,10},{9,11},{10,... | collective-permute-start | bytes 786440 | tf_op jit(solution)/shard_map/ppermute | solution.py:26
  118.6 3.2 %collective-permute-start.22 = (bf16[64,2048]{1,0:T(8,128)(2,1)S(1)}, bf16[64,2048]{1,0:T(8,128)(2,1)S(1)}, u32[]{:S(2)}, u32[]{:S(2)}) collective-permute-start(bf16[64,2048]{1,0:T(8,128)(2,1)S(1)} %get-tuple-element.33.refs_8_), channel_id=1, source_target_pairs={{0,14},{1,15},{2,0},{3,1},{4,2},{5,3},{6,4},{7,5},{8,6},{9,7},{10,... | collective-permute-start | bytes 786440 | tf_op jit(solution)/shard_map/ppermute | solution.py:26
  121.8 3.9 %collective-permute-done.28.a = bf16[64,2048]{1,0:T(8,128)(2,1)S(1)} collective-permute-done((bf16[64,2048]{1,0:T(8,128)(2,1)S(1)}, bf16[64,2048]{1,0:T(8,128)(2,1)S(1)}, u32[]{:S(2)}, u32[]{:S(2)}) %collective-permute-start.28) | collective-permute-done | bytes 262176 | tf_op jit(solution)/shard_map/ppermute | solution.py:26
  125.9 1.1 collective-permute-done.18.a
  127.1 0.9 collective-permute-start.19
  128.0 3.7 %collective-permute-done.25.a = bf16[64,2048]{1,0:T(8,128)(2,1)S(1)} collective-permute-done((bf16[64,2048]{1,0:T(8,128)(2,1)S(1)}, bf16[64,2048]{1,0:T(8,128)(2,1)S(1)}, u32[]{:S(2)}, u32[]{:S(2)}) %collective-permute-start.25) | collective-permute-done | bytes 262176 | tf_op jit(solution)/shard_map/ppermute | solution.py:26
  131.8 0.3 collective-permute-start.26
  132.2 3.3 %collective-permute-start.23 = (bf16[64,2048]{1,0:T(8,128)(2,1)S(1)}, bf16[64,2048]{1,0:T(8,128)(2,1)S(1)}, u32[]{:S(2)}, u32[]{:S(2)}) collective-permute-start(bf16[64,2048]{1,0:T(8,128)(2,1)S(1)} %shard_map.138), channel_id=1, source_target_pairs={{0,14},{1,15},{2,0},{3,1},{4,2},{5,3},{6,4},{7,5},{8,6},{9,7},{10,... | collective-permute-start | bytes 786440 | tf_op jit(solution)/shard_map/ppermute | solution.py:26
  135.5 0.9 collective-permute-done.29.a
  136.6 0.9 collective-permute-done.19.a
  137.5 1.2 collective-permute-start.20
  138.7 6.7 %shard_map.136 = (bf16[64,2048]{1,0:T(8,128)(2,1)S(1)}, bf16[64,2048]{1,0:T(8,128)(2,1)S(1)}, bf16[64,2048]{1,0:T(8,128)(2,1)S(1)}, bf16[64,2048]{1,0:T(8,128)(2,1)S(1)}) custom-call(bf16[64,2048]{1,0:T(8,128)(2,1)S(1)} %collective-permute-done.1.refs_0_, bf16[64,2048]{1,0:T(8,128)(2,1)S(1)} %collective-permute-done.12.refs_1_, ...), custom_call_target="tpu_custom_call" | custom-call | flops 2818572288 | bytes 1048576 | tf_op jit(solution)/shard_map/pallas_call | solution.py:78
  145.7 3.3 %collective-permute-start.24 = (bf16[64,2048]{1,0:T(8,128)(2,1)S(1)}, bf16[64,2048]{1,0:T(8,128)(2,1)S(1)}, u32[]{:S(2)}, u32[]{:S(2)}) collective-permute-start(bf16[64,2048]{1,0:T(8,128)(2,1)S(1)} %shard_map.139), channel_id=1, source_target_pairs={{0,14},{1,15},{2,0},{3,1},{4,2},{5,3},{6,4},{7,5},{8,6},{9,7},{10,... | collective-permute-start | bytes 786440 | tf_op jit(solution)/shard_map/ppermute | solution.py:26
  149.0 1.0 collective-permute-start.31
  150.1 1.2 collective-permute-start.21
  151.3 5.9 %shard_map.140 = (bf16[64,2048]{1,0:T(8,128)(2,1)S(1)}, bf16[64,2048]{1,0:T(8,128)(2,1)S(1)}) custom-call(bf16[64,2048]{1,0:T(8,128)(2,1)S(1)} %get-tuple-element.30.refs_0_, bf16[64,2048]{1,0:T(8,128)(2,1)S(1)} %get-tuple-element.31.refs_1_, bf16[448,2048]{1,0:T(8,128)(2,1)S(1)} %bitcast.30, bf16[448,2048]{1,0:T(8,128)(2,1)} %collective-permute-done.9.refs_5_.refs_3_, ...), custom_call_target="tpu_custom_call" | custom-call | flops 1409286144 | bytes 1048576 | tf_op jit(solution)/shard_map/pallas_call | solution.py:78
  157.3 0.5 collective-permute-done.21.right_a
  158.0 13.4 %all_to_all.16 = bf16[16,8,2048]{2,1,0:T(8,128)(2,1)S(1)} all-to-all(bf16[16,8,2048]{2,1,0:T(8,128)(2,1)S(1)} %bitcast.44), channel_id=1, replica_groups=mesh['sp'=16,'tp'=16] {'sp'}, dimensions={0} | all-to-all | bytes 1048576 | tf_op jit(solution)/shard_map/all_to_all | solution.py:389
  171.3 0.2 fusion
  171.6 1.0 add_convert_fusion
  (66 shorter events, 1.8 us)
Async XLA Ops:
  1.1 6.6 %collective-permute-start = (bf16[64,128]{1,0:T(8,128)(2,1)S(1)}, bf16[64,128]{1,0:T(8,128)(2,1)S(1)}, u32[]{:S(2)}, u32[]{:S(2)}) collective-permute-start(bf16[64,128]{1,0:T(8,128)(2,1)S(1)} %slice.4), channel_id=1, source_target_pairs={{0,16},{16,32},{32,48},{48,64},{64,80},{80,96},{96,112},{112,128},... | collective-permute-start | bytes 49160 | tf_op jit(solution)/shard_map/ppermute | solution.py:21
  4.5 0.7 copy-start.5
  5.2 12.5 %copy-start = (bf16[1,2048,448]{1,2,0:T(8,128)(2,1)S(1)}, bf16[1,2048,448]{1,2,0:T(8,128)(2,1)}, u32[]{:S(2)}) copy-start(bf16[1,2048,448]{1,2,0:T(8,128)(2,1)} %param.23) | copy-start | bytes 5505028
  5.2 20.6 %copy-start.4 = (bf16[64,2048]{1,0:T(8,128)(2,1)S(1)}, bf16[64,2048]{1,0:T(8,128)(2,1)}, u32[]{:S(2)}) copy-start(bf16[64,2048]{1,0:T(8,128)(2,1)} %stream.1) | copy-start | bytes 786436
  5.2 20.6 %copy-start.6 = (f32[2048]{0:T(1024)S(1)}, f32[2048]{0:T(1024)}, u32[]{:S(2)}) copy-start(f32[2048]{0:T(1024)} %param.22) | copy-start | bytes 24580
  5.2 20.6 %copy-start.7 = (f32[1024]{0:T(1024)S(1)}, f32[1024]{0:T(1024)}, u32[]{:S(2)}) copy-start(f32[1024]{0:T(1024)} %param.16) | copy-start | bytes 12292
  5.2 20.6 %copy-start.8 = (f32[1024]{0:T(1024)S(1)}, f32[1024]{0:T(1024)}, u32[]{:S(2)}) copy-start(f32[1024]{0:T(1024)} %param.17) | copy-start | bytes 12292
  5.2 20.6 %copy-start.9 = (s32[64,2]{0,1:T(2,128)S(1)}, s32[64,2]{0,1:T(2,128)}, u32[]{:S(2)}) copy-start(s32[64,2]{0,1:T(2,128)} %param.20) | copy-start | bytes 1540
  5.2 20.6 %copy-start.10 = (f32[64,2]{0,1:T(2,128)S(1)}, f32[64,2]{0,1:T(2,128)}, u32[]{:S(2)}) copy-start(f32[64,2]{0,1:T(2,128)} %param.21) | copy-start | bytes 1540
  8.5 17.2 %all-to-all-start = ((bf16[16,32,128]{2,1,0:T(8,128)(2,1)}), bf16[16,32,128]{2,1,0:T(8,128)(2,1)S(1)}, u32[]{:S(2)}, u32[]{:S(2)}) async-start(bf16[16,32,128]{2,1,0:T(8,128)(2,1)} %shard_map.128), calls=%async_computation | async-start | bytes 262144 | tf_op jit(solution)/shard_map/all_to_all | solution.py:335
  17.1 76.7 %collective-permute-start.10 = (bf16[448,2048]{1,0:T(8,128)(2,1)}, bf16[448,2048]{1,0:T(8,128)(2,1)}, u32[]{:S(2)}, u32[]{:S(2)}) collective-permute-start(bf16[448,2048]{1,0:T(8,128)(2,1)} %bitcast.31), channel_id=1, source_target_pairs={{0,1},{1,0},{2,3},{3,2},{4,5},{5,4},{6,7},{7,6},{8,9},{9,8},{10,11... | collective-permute-start | bytes 5505032 | tf_op jit(solution)/shard_map/ppermute | solution.py:31
  17.5 76.3 %collective-permute-start.11 = (bf16[448,2048]{1,0:T(8,128)(2,1)}, bf16[448,2048]{1,0:T(8,128)(2,1)}, u32[]{:S(2)}, u32[]{:S(2)}) collective-permute-start(bf16[448,2048]{1,0:T(8,128)(2,1)} %bitcast.37), channel_id=1, source_target_pairs={{0,1},{1,0},{2,3},{3,2},{4,5},{5,4},{6,7},{7,6},{8,9},{9,8},{10,11... | collective-permute-start | bytes 5505032 | tf_op jit(solution)/shard_map/ppermute | solution.py:31
  17.7 79.3 %collective-permute-start.9 = (bf16[448,2048]{1,0:T(8,128)(2,1)S(1)}, bf16[448,2048]{1,0:T(8,128)(2,1)}, u32[]{:S(2)}, u32[]{:S(2)}) collective-permute-start(bf16[448,2048]{1,0:T(8,128)(2,1)S(1)} %bitcast.25), channel_id=1, source_target_pairs={{0,1},{1,0},{2,3},{3,2},{4,5},{5,4},{6,7},{7,6},{8,9},{9,8},{10,11... | collective-permute-start | bytes 5505032 | tf_op jit(solution)/shard_map/ppermute | solution.py:31
  25.8 2.2 %copy-start.3 = (bf16[1024,2048]{1,0:T(8,128)(2,1)S(1)}, bf16[1024,2048]{1,0:T(8,128)(2,1)}, u32[]{:S(2)}) copy-start(bf16[1024,2048]{1,0:T(8,128)(2,1)} %out_weight.1) | copy-start | bytes 12582916
  28.0 69.0 %copy-start.1 = (bf16[1,2048,448]{1,2,0:T(8,128)(2,1)S(1)}, bf16[1,2048,448]{1,2,0:T(8,128)(2,1)}, u32[]{:S(2)}) copy-start(bf16[1,2048,448]{1,2,0:T(8,128)(2,1)} %param.24) | copy-start | bytes 5505028
  28.0 69.0 %copy-start.2 = (bf16[1,448,2048]{2,1,0:T(8,128)(2,1)S(1)}, bf16[1,448,2048]{2,1,0:T(8,128)(2,1)}, u32[]{:S(2)}) copy-start(bf16[1,448,2048]{2,1,0:T(8,128)(2,1)} %param.25) | copy-start | bytes 5505028
  47.5 8.7 %collective-permute-start.12 = (bf16[64,2048]{1,0:T(8,128)(2,1)S(1)}, bf16[64,2048]{1,0:T(8,128)(2,1)S(1)}, u32[]{:S(2)}, u32[]{:S(2)}) collective-permute-start(bf16[64,2048]{1,0:T(8,128)(2,1)S(1)} %get-tuple-element.31.refs_1_), channel_id=1, source_target_pairs={{0,2},{1,3},{2,4},{3,5},{4,6},{5,7},{6,8},{7,9},{8,10},{9,11},{10,... | collective-permute-start | bytes 786440 | tf_op jit(solution)/shard_map/ppermute | solution.py:26
  48.1 8.1 %collective-permute-start.15 = (bf16[64,2048]{1,0:T(8,128)(2,1)S(1)}, bf16[64,2048]{1,0:T(8,128)(2,1)S(1)}, u32[]{:S(2)}, u32[]{:S(2)}) collective-permute-start(bf16[64,2048]{1,0:T(8,128)(2,1)S(1)} %get-tuple-element.30.refs_0_), channel_id=1, source_target_pairs={{0,14},{1,15},{2,0},{3,1},{4,2},{5,3},{6,4},{7,5},{8,6},{9,7},{10,... | collective-permute-start | bytes 786440 | tf_op jit(solution)/shard_map/ppermute | solution.py:26
  56.2 7.8 %collective-permute-start.1 = (bf16[64,2048]{1,0:T(8,128)(2,1)S(1)}, bf16[64,2048]{1,0:T(8,128)(2,1)S(1)}, u32[]{:S(2)}, u32[]{:S(2)}) collective-permute-start(bf16[64,2048]{1,0:T(8,128)(2,1)S(1)} %get-tuple-element.30.refs_0_), channel_id=1, source_target_pairs={{0,2},{1,3},{2,4},{3,5},{4,6},{5,7},{6,8},{7,9},{8,10},{9,11},{10,... | collective-permute-start | bytes 786440 | tf_op jit(solution)/shard_map/ppermute | solution.py:26
  56.2 7.8 %collective-permute-start.5 = (bf16[64,2048]{1,0:T(8,128)(2,1)S(1)}, bf16[64,2048]{1,0:T(8,128)(2,1)S(1)}, u32[]{:S(2)}, u32[]{:S(2)}) collective-permute-start(bf16[64,2048]{1,0:T(8,128)(2,1)S(1)} %get-tuple-element.31.refs_1_), channel_id=1, source_target_pairs={{0,14},{1,15},{2,0},{3,1},{4,2},{5,3},{6,4},{7,5},{8,6},{9,7},{10,... | collective-permute-start | bytes 786440 | tf_op jit(solution)/shard_map/ppermute | solution.py:26
  64.0 7.6 %collective-permute-start.13 = (bf16[64,2048]{1,0:T(8,128)(2,1)S(1)}, bf16[64,2048]{1,0:T(8,128)(2,1)S(1)}, u32[]{:S(2)}, u32[]{:S(2)}) collective-permute-start(bf16[64,2048]{1,0:T(8,128)(2,1)S(1)} %collective-permute-done.12.refs_1_), channel_id=1, source_target_pairs={{0,2},{1,3},{2,4},{3,5},{4,6},{5,7},{6,8},{7,9},{8,10},{9,11},{10,... | collective-permute-start | bytes 786440 | tf_op jit(solution)/shard_map/ppermute | solution.py:26
  64.0 7.6 %collective-permute-start.16 = (bf16[64,2048]{1,0:T(8,128)(2,1)S(1)}, bf16[64,2048]{1,0:T(8,128)(2,1)S(1)}, u32[]{:S(2)}, u32[]{:S(2)}) collective-permute-start(bf16[64,2048]{1,0:T(8,128)(2,1)S(1)} %collective-permute-done.15.refs_2_), channel_id=1, source_target_pairs={{0,14},{1,15},{2,0},{3,1},{4,2},{5,3},{6,4},{7,5},{8,6},{9,7},{10,... | collective-permute-start | bytes 786440 | tf_op jit(solution)/shard_map/ppermute | solution.py:26
  71.5 8.6 %collective-permute-start.2 = (bf16[64,2048]{1,0:T(8,128)(2,1)S(1)}, bf16[64,2048]{1,0:T(8,128)(2,1)S(1)}, u32[]{:S(2)}, u32[]{:S(2)}) collective-permute-start(bf16[64,2048]{1,0:T(8,128)(2,1)S(1)} %collective-permute-done.1.refs_0_), channel_id=1, source_target_pairs={{0,2},{1,3},{2,4},{3,5},{4,6},{5,7},{6,8},{7,9},{8,10},{9,11},{10,... | collective-permute-start | bytes 786440 | tf_op jit(solution)/shard_map/ppermute | solution.py:26
  71.5 8.6 %collective-permute-start.6 = (bf16[64,2048]{1,0:T(8,128)(2,1)S(1)}, bf16[64,2048]{1,0:T(8,128)(2,1)S(1)}, u32[]{:S(2)}, u32[]{:S(2)}) collective-permute-start(bf16[64,2048]{1,0:T(8,128)(2,1)S(1)} %collective-permute-done.5.refs_3_), channel_id=1, source_target_pairs={{0,14},{1,15},{2,0},{3,1},{4,2},{5,3},{6,4},{7,5},{8,6},{9,7},{10,... | collective-permute-start | bytes 786440 | tf_op jit(solution)/shard_map/ppermute | solution.py:26
  80.1 9.7 %collective-permute-start.3 = (bf16[64,2048]{1,0:T(8,128)(2,1)S(1)}, bf16[64,2048]{1,0:T(8,128)(2,1)S(1)}, u32[]{:S(2)}, u32[]{:S(2)}) collective-permute-start(bf16[64,2048]{1,0:T(8,128)(2,1)S(1)} %collective-permute-done.2.refs_0_), channel_id=1, source_target_pairs={{0,2},{1,3},{2,4},{3,5},{4,6},{5,7},{6,8},{7,9},{8,10},{9,11},{10,... | collective-permute-start | bytes 786440 | tf_op jit(solution)/shard_map/ppermute | solution.py:26
  80.1 10.0 %collective-permute-start.7 = (bf16[64,2048]{1,0:T(8,128)(2,1)S(1)}, bf16[64,2048]{1,0:T(8,128)(2,1)S(1)}, u32[]{:S(2)}, u32[]{:S(2)}) collective-permute-start(bf16[64,2048]{1,0:T(8,128)(2,1)S(1)} %collective-permute-done.6.refs_3_), channel_id=1, source_target_pairs={{0,14},{1,15},{2,0},{3,1},{4,2},{5,3},{6,4},{7,5},{8,6},{9,7},{10,... | collective-permute-start | bytes 786440 | tf_op jit(solution)/shard_map/ppermute | solution.py:26
  89.8 13.9 %collective-permute-start.14 = (bf16[64,2048]{1,0:T(8,128)(2,1)S(1)}, bf16[64,2048]{1,0:T(8,128)(2,1)S(1)}, u32[]{:S(2)}, u32[]{:S(2)}) collective-permute-start(bf16[64,2048]{1,0:T(8,128)(2,1)S(1)} %collective-permute-done.13.refs_1_), channel_id=1, source_target_pairs={{0,2},{1,3},{2,4},{3,5},{4,6},{5,7},{6,8},{7,9},{8,10},{9,11},{10,... | collective-permute-start | bytes 786440 | tf_op jit(solution)/shard_map/ppermute | solution.py:26
  90.1 13.7 %collective-permute-start.17 = (bf16[64,2048]{1,0:T(8,128)(2,1)S(1)}, bf16[64,2048]{1,0:T(8,128)(2,1)S(1)}, u32[]{:S(2)}, u32[]{:S(2)}) collective-permute-start(bf16[64,2048]{1,0:T(8,128)(2,1)S(1)} %collective-permute-done.16.refs_2_), channel_id=1, source_target_pairs={{0,14},{1,15},{2,0},{3,1},{4,2},{5,3},{6,4},{7,5},{8,6},{9,7},{10,... | collective-permute-start | bytes 786440 | tf_op jit(solution)/shard_map/ppermute | solution.py:26
  93.8 16.7 %collective-permute-start.4 = (bf16[64,2048]{1,0:T(8,128)(2,1)S(1)}, bf16[64,2048]{1,0:T(8,128)(2,1)S(1)}, u32[]{:S(2)}, u32[]{:S(2)}) collective-permute-start(bf16[64,2048]{1,0:T(8,128)(2,1)S(1)} %collective-permute-done.3.refs_0_), channel_id=1, source_target_pairs={{0,2},{1,3},{2,4},{3,5},{4,6},{5,7},{6,8},{7,9},{8,10},{9,11},{10,... | collective-permute-start | bytes 786440 | tf_op jit(solution)/shard_map/ppermute | solution.py:26
  93.8 16.7 %collective-permute-start.8 = (bf16[64,2048]{1,0:T(8,128)(2,1)S(1)}, bf16[64,2048]{1,0:T(8,128)(2,1)S(1)}, u32[]{:S(2)}, u32[]{:S(2)}) collective-permute-start(bf16[64,2048]{1,0:T(8,128)(2,1)S(1)} %collective-permute-done.7.refs_3_), channel_id=1, source_target_pairs={{0,14},{1,15},{2,0},{3,1},{4,2},{5,3},{6,4},{7,5},{8,6},{9,7},{10,... | collective-permute-start | bytes 786440 | tf_op jit(solution)/shard_map/ppermute | solution.py:26
  116.5 9.3 %collective-permute-start.28 = (bf16[64,2048]{1,0:T(8,128)(2,1)S(1)}, bf16[64,2048]{1,0:T(8,128)(2,1)S(1)}, u32[]{:S(2)}, u32[]{:S(2)}) collective-permute-start(bf16[64,2048]{1,0:T(8,128)(2,1)S(1)} %get-tuple-element.43), channel_id=1, source_target_pairs={{0,14},{1,15},{2,0},{3,1},{4,2},{5,3},{6,4},{7,5},{8,6},{9,7},{10,... | collective-permute-start | bytes 786440 | tf_op jit(solution)/shard_map/ppermute | solution.py:26
  116.5 10.5 %collective-permute-start.18 = (bf16[64,2048]{1,0:T(8,128)(2,1)S(1)}, bf16[64,2048]{1,0:T(8,128)(2,1)S(1)}, u32[]{:S(2)}, u32[]{:S(2)}) collective-permute-start(bf16[64,2048]{1,0:T(8,128)(2,1)S(1)} %get-tuple-element.34.refs_10_), channel_id=1, source_target_pairs={{0,2},{1,3},{2,4},{3,5},{4,6},{5,7},{6,8},{7,9},{8,10},{9,11},{10,... | collective-permute-start | bytes 786440 | tf_op jit(solution)/shard_map/ppermute | solution.py:26
  118.6 13.2 %collective-permute-start.25 = (bf16[64,2048]{1,0:T(8,128)(2,1)S(1)}, bf16[64,2048]{1,0:T(8,128)(2,1)S(1)}, u32[]{:S(2)}, u32[]{:S(2)}) collective-permute-start(bf16[64,2048]{1,0:T(8,128)(2,1)S(1)} %get-tuple-element.40), channel_id=1, source_target_pairs={{0,2},{1,3},{2,4},{3,5},{4,6},{5,7},{6,8},{7,9},{8,10},{9,11},{10,... | collective-permute-start | bytes 786440 | tf_op jit(solution)/shard_map/ppermute | solution.py:26
  118.6 13.6 %collective-permute-start.22 = (bf16[64,2048]{1,0:T(8,128)(2,1)S(1)}, bf16[64,2048]{1,0:T(8,128)(2,1)S(1)}, u32[]{:S(2)}, u32[]{:S(2)}) collective-permute-start(bf16[64,2048]{1,0:T(8,128)(2,1)S(1)} %get-tuple-element.33.refs_8_), channel_id=1, source_target_pairs={{0,14},{1,15},{2,0},{3,1},{4,2},{5,3},{6,4},{7,5},{8,6},{9,7},{10,... | collective-permute-start | bytes 786440 | tf_op jit(solution)/shard_map/ppermute | solution.py:26
  125.8 10.6 %collective-permute-start.29 = (bf16[64,2048]{1,0:T(8,128)(2,1)S(1)}, bf16[64,2048]{1,0:T(8,128)(2,1)S(1)}, u32[]{:S(2)}, u32[]{:S(2)}) collective-permute-start(bf16[64,2048]{1,0:T(8,128)(2,1)S(1)} %shard_map.143), channel_id=1, source_target_pairs={{0,14},{1,15},{2,0},{3,1},{4,2},{5,3},{6,4},{7,5},{8,6},{9,7},{10,... | collective-permute-start | bytes 786440 | tf_op jit(solution)/shard_map/ppermute | solution.py:26
  127.1 10.4 %collective-permute-start.19 = (bf16[64,2048]{1,0:T(8,128)(2,1)S(1)}, bf16[64,2048]{1,0:T(8,128)(2,1)S(1)}, u32[]{:S(2)}, u32[]{:S(2)}) collective-permute-start(bf16[64,2048]{1,0:T(8,128)(2,1)S(1)} %shard_map.134), channel_id=1, source_target_pairs={{0,2},{1,3},{2,4},{3,5},{4,6},{5,7},{6,8},{7,9},{8,10},{9,11},{10,... | collective-permute-start | bytes 786440 | tf_op jit(solution)/shard_map/ppermute | solution.py:26
  131.8 13.6 %collective-permute-start.26 = (bf16[64,2048]{1,0:T(8,128)(2,1)S(1)}, bf16[64,2048]{1,0:T(8,128)(2,1)S(1)}, u32[]{:S(2)}, u32[]{:S(2)}) collective-permute-start(bf16[64,2048]{1,0:T(8,128)(2,1)S(1)} %shard_map.141), channel_id=1, source_target_pairs={{0,2},{1,3},{2,4},{3,5},{4,6},{5,7},{6,8},{7,9},{8,10},{9,11},{10,... | collective-permute-start | bytes 786440 | tf_op jit(solution)/shard_map/ppermute | solution.py:26
  132.2 13.4 %collective-permute-start.23 = (bf16[64,2048]{1,0:T(8,128)(2,1)S(1)}, bf16[64,2048]{1,0:T(8,128)(2,1)S(1)}, u32[]{:S(2)}, u32[]{:S(2)}) collective-permute-start(bf16[64,2048]{1,0:T(8,128)(2,1)S(1)} %shard_map.138), channel_id=1, source_target_pairs={{0,14},{1,15},{2,0},{3,1},{4,2},{5,3},{6,4},{7,5},{8,6},{9,7},{10,... | collective-permute-start | bytes 786440 | tf_op jit(solution)/shard_map/ppermute | solution.py:26
  136.5 12.5 %collective-permute-start.30 = (bf16[64,2048]{1,0:T(8,128)(2,1)S(1)}, bf16[64,2048]{1,0:T(8,128)(2,1)S(1)}, u32[]{:S(2)}, u32[]{:S(2)}) collective-permute-start(bf16[64,2048]{1,0:T(8,128)(2,1)S(1)} %shard_map.144), channel_id=1, source_target_pairs={{0,14},{1,15},{2,0},{3,1},{4,2},{5,3},{6,4},{7,5},{8,6},{9,7},{10,... | collective-permute-start | bytes 786440 | tf_op jit(solution)/shard_map/ppermute | solution.py:26
  137.5 12.5 %collective-permute-start.20 = (bf16[64,2048]{1,0:T(8,128)(2,1)S(1)}, bf16[64,2048]{1,0:T(8,128)(2,1)S(1)}, u32[]{:S(2)}, u32[]{:S(2)}) collective-permute-start(bf16[64,2048]{1,0:T(8,128)(2,1)S(1)} %shard_map.135), channel_id=1, source_target_pairs={{0,2},{1,3},{2,4},{3,5},{4,6},{5,7},{6,8},{7,9},{8,10},{9,11},{10,... | collective-permute-start | bytes 786440 | tf_op jit(solution)/shard_map/ppermute | solution.py:26
  145.5 11.7 %collective-permute-start.27 = (bf16[64,2048]{1,0:T(8,128)(2,1)S(1)}, bf16[64,2048]{1,0:T(8,128)(2,1)S(1)}, u32[]{:S(2)}, u32[]{:S(2)}) collective-permute-start(bf16[64,2048]{1,0:T(8,128)(2,1)S(1)} %shard_map.142), channel_id=1, source_target_pairs={{0,2},{1,3},{2,4},{3,5},{4,6},{5,7},{6,8},{7,9},{8,10},{9,11},{10,... | collective-permute-start | bytes 786440 | tf_op jit(solution)/shard_map/ppermute | solution.py:26
  145.7 11.6 %collective-permute-start.24 = (bf16[64,2048]{1,0:T(8,128)(2,1)S(1)}, bf16[64,2048]{1,0:T(8,128)(2,1)S(1)}, u32[]{:S(2)}, u32[]{:S(2)}) collective-permute-start(bf16[64,2048]{1,0:T(8,128)(2,1)S(1)} %shard_map.139), channel_id=1, source_target_pairs={{0,14},{1,15},{2,0},{3,1},{4,2},{5,3},{6,4},{7,5},{8,6},{9,7},{10,... | collective-permute-start | bytes 786440 | tf_op jit(solution)/shard_map/ppermute | solution.py:26
  149.0 8.2 %collective-permute-start.31 = (bf16[64,2048]{1,0:T(8,128)(2,1)S(1)}, bf16[64,2048]{1,0:T(8,128)(2,1)S(1)}, u32[]{:S(2)}, u32[]{:S(2)}) collective-permute-start(bf16[64,2048]{1,0:T(8,128)(2,1)S(1)} %shard_map.145), channel_id=1, source_target_pairs={{0,14},{1,15},{2,0},{3,1},{4,2},{5,3},{6,4},{7,5},{8,6},{9,7},{10,... | collective-permute-start | bytes 786440 | tf_op jit(solution)/shard_map/ppermute | solution.py:26
  150.1 7.7 %collective-permute-start.21 = (bf16[64,2048]{1,0:T(8,128)(2,1)S(1)}, bf16[64,2048]{1,0:T(8,128)(2,1)S(1)}, u32[]{:S(2)}, u32[]{:S(2)}) collective-permute-start(bf16[64,2048]{1,0:T(8,128)(2,1)S(1)} %shard_map.137), channel_id=1, source_target_pairs={{0,2},{1,3},{2,4},{3,5},{4,6},{5,7},{6,8},{7,9},{8,10},{9,11},{10,... | collective-permute-start | bytes 786440 | tf_op jit(solution)/shard_map/ppermute | solution.py:26
